TPU v7x, 128 devices: a whole 4x4x4 slice. The times are simulated.
128 devices in a mesh: sp: 32 (over z, y, core), tp: 4 (over x).
Axes of the slice: x: 4, y: 4, z: 4, core: 2. Of those that a mesh axis runs over, the one named last changes fastest.
Arguments:
- tokens: bfloat16 [8192, 2048], P('sp'), may hold values from -6 to 6
- input_norm_gain: float32 [2048], replicated, may hold values from 0.1 to 1.9
- convolution_value_weight: bfloat16 [2048, 512], P(None, 'tp'), may hold values from -0.125 to 0.125
- convolution_gate_weight: bfloat16 [2048, 512], P(None, 'tp'), may hold values from -0.125 to 0.125
- depthwise_taps_weight: float32 [31, 512], P(None, 'tp'), may hold values from -1 to 1
- convolution_group_gain: float32 [512], P('tp'), may hold values from 0.1 to 1.9
- convolution_group_shift: float32 [512], P('tp'), may hold values from -3 to 3
- receptance_weight: bfloat16 [2048, 1024], P(None, 'tp'), may hold values from -0.125 to 0.125
- key_weight: bfloat16 [2048, 1024], P(None, 'tp'), may hold values from -0.125 to 0.125
- value_weight: bfloat16 [2048, 1024], P(None, 'tp'), may hold values from -0.125 to 0.125
- decay_weight: bfloat16 [2048, 1024], P(None, 'tp'), may hold values from -0.0625 to 0.0625
- correction_rate_weight: bfloat16 [2048, 1024], P(None, 'tp'), may hold values from -0.125 to 0.125
- output_gate_weight: bfloat16 [2048, 1024], P(None, 'tp'), may hold values from -0.125 to 0.125
- key_prenorm_gain: float32 [1024], P('tp'), may hold values from 0.04 to 8
- decay_offset_bias: float32 [1024], P('tp'), may hold values from -30 to 0
- position_decay_shift: float32 [8192, 1024], P('sp', 'tp'), may hold values from -1 to 1
- extra_log_decay: float32 [8192, 1024], P('sp', 'tp'), may hold values from -0.7 to 0
- head_norm_gain: float32 [1024], P('tp'), may hold values from 0.1 to 1.9
- convolution_output_weight: bfloat16 [512, 2048], replicated, may hold values from -0.15625 to 0.15625
- attention_output_weight: bfloat16 [1024, 2048], replicated, may hold values from -0.15625 to 0.15625
Outputs:
- mixed: bfloat16 [8192, 2048], P(('sp', 'tp'))
All inputs are finite; a program needn't handle non-finite values.
Results may differ from a plain program's by a relative error of at most 0.0063.
The roundings to bfloat16 on the way count: a program that leaves them out, or rounds other values in their place, can miss the bound.
Values may be sent and summed in bfloat16 or wider, within the bound.
No kernel may reach another device: no remote copies, remote signals or barrier semaphores. Data moves between devices by JAX's collectives and lax.ppermute only.
A program may use at most 128 MiB of HBM per device.

v0:
```python
import math

import jax
import jax.numpy as jnp
from jax import lax
from jax.sharding import Mesh
from jax.sharding import PartitionSpec as P

HEAD = 64
SP = ("sp_0", "sp_1", "sp_2")
SP_TP = ("sp_0", "sp_1", "sp_2", "tp")


NORM_EPS = 1e-06
GROUP_EPS = 1e-05
HEAD_EPS = 0.00064
KEY_EPS = 1e-06
HIGHEST = lax.Precision.HIGHEST


def from_behind(value, axis, steps):
    count = lax.axis_size(axis)
    leading, last = (max(0, -steps), min(count, count - steps))
    return lax.ppermute(value, axis, [(source, source + steps) for source in range(leading, last)])


def neutral_like(value, identity):
    return jax.tree.map(
        lambda part, zero: jnp.zeros_like(part) + jnp.asarray(zero, part.dtype), value, identity
    )


def entering_2(value, axes, combine, identity):
    before = start = neutral_like(value, identity)
    running = value
    for axis in reversed(axes):
        length, mine = (lax.axis_size(axis), lax.axis_index(axis))
        pieces = jax.tree.map(lambda part: lax.all_gather(part, axis), running)
        inside, running = (start, start)
        for k in range(length):
            passed = k < mine
            running = combine(running, jax.tree.map(lambda part: part[k], pieces))
            inside = jax.tree.map(lambda new, old: jnp.where(passed, new, old), running, inside)
        before = combine(inside, before)
    return before


def stored(values):
    return lax.optimization_barrier(values.astype(jnp.bfloat16)).astype(jnp.float32)


def einsum_exact(form, left, right):
    return jnp.einsum(form, left, right, precision=HIGHEST)


def to_blocks(values, span_len):
    tok_rows, width = values.shape
    return values.reshape(tok_rows // span_len, span_len, width // HEAD, HEAD).transpose(2, 0, 1, 3)


def block_pass(receptance, decay_logarithm, key_rows, value_rows, unit_key, erase_dir):
    span_len = receptance.shape[2]
    cumulate = jnp.cumsum(decay_logarithm, axis=2)
    before = cumulate - decay_logarithm
    final = cumulate[:, :, -1:, :]
    query_unit = unit_key * jnp.exp(before)
    query_read = receptance * jnp.exp(cumulate)
    scaled_erase = erase_dir * jnp.exp(-cumulate)
    scaled_key = key_rows * jnp.exp(-cumulate)
    strict = jnp.tril(jnp.ones((span_len, span_len), jnp.float32), -1)
    inclusive = jnp.tril(jnp.ones((span_len, span_len), jnp.float32))
    erase_mix = einsum_exact("hbsn,hbjn->hbsj", query_unit, scaled_erase) * strict
    key_mix = einsum_exact("hbsn,hbjn->hbsj", query_unit, scaled_key) * strict
    right_side = jnp.concatenate(
        [-einsum_exact("hbsj,hbjn->hbsn", key_mix, value_rows), -query_unit], axis=-1
    )
    system = erase_mix + jnp.eye(span_len, dtype=jnp.float32)
    removed = jax.scipy.linalg.solve_triangular(system, right_side, lower=True, unit_diagonal=True)
    read_erase = einsum_exact("hbtn,hbjn->hbtj", query_read, scaled_erase) * inclusive
    read_key = einsum_exact("hbtn,hbjn->hbtj", query_read, scaled_key) * inclusive
    readout = einsum_exact("hbtj,hbjr->hbtr", read_erase, removed) + jnp.concatenate(
        [einsum_exact("hbtj,hbjn->hbtn", read_key, value_rows), query_read], axis=-1
    )
    kept_erase = erase_dir * jnp.exp(final - cumulate)
    kept_key = key_rows * jnp.exp(final - cumulate)
    from_removed = einsum_exact("hbjr,hbjn->hbrn", removed, kept_erase)
    local_base = from_removed[:, :, :HEAD] + einsum_exact("hbjv,hbjn->hbvn", value_rows, kept_key)
    transfer = from_removed[:, :, HEAD:] + jnp.eye(HEAD, dtype=jnp.float32) * jnp.exp(final)
    return (readout[..., :HEAD], readout[..., HEAD:], transfer, local_base)


def compose(carry, block):
    trans_now, base_now = carry
    block_trans, block_base = block
    joined = (
        einsum_exact("hij,hjk->hik", trans_now, block_trans),
        einsum_exact("hij,hjk->hik", base_now, block_trans) + block_base,
    )
    return (joined, carry)


def chain(earlier, later):
    return (
        einsum_exact("hij,hjk->hik", earlier[0], later[0]),
        einsum_exact("hij,hjk->hik", earlier[1], later[0]) + later[1],
    )


def local(
    tokens,
    input_norm_gain,
    convolution_value_weight,
    convolution_gate_weight,
    depthwise_taps_weight,
    convolution_group_gain,
    convolution_group_shift,
    receptance_weight,
    key_weight,
    value_weight,
    decay_weight,
    correction_rate_weight,
    output_gate_weight,
    key_prenorm_gain,
    decay_offset_bias,
    position_decay_shift,
    extra_log_decay,
    head_norm_gain,
    convolution_output_weight,
    attention_output_weight,
):
    tok_rows = tokens.shape[0]
    float_rows = tokens.astype(jnp.float32)
    normed = (
        float_rows
        * lax.rsqrt(jnp.mean(float_rows * float_rows, axis=-1, keepdims=True) + NORM_EPS)
        * input_norm_gain
    ).astype(jnp.bfloat16)

    def project(weight):
        return stored(jnp.dot(normed, weight, preferred_element_type=jnp.float32))

    conv_input = (
        project(convolution_value_weight) * jax.nn.sigmoid(project(convolution_gate_weight))
    ).astype(jnp.bfloat16)
    tap_count = depthwise_taps_weight.shape[0]
    earlier_rows = from_behind(conv_input[tok_rows - tap_count + 1 :], SP, 1)
    extended = jnp.concatenate([earlier_rows, conv_input], axis=0).astype(jnp.float32)
    conv_sum = jnp.zeros((tok_rows, conv_input.shape[1]), jnp.float32)
    for offset in range(tap_count):
        conv_sum = conv_sum + depthwise_taps_weight[offset] * extended[offset : offset + tok_rows]
    channels = conv_input.shape[1]
    grouped = conv_sum.reshape(tok_rows, channels // 64, 64)
    centred = grouped - jnp.mean(grouped, axis=-1, keepdims=True)
    grouped = centred * lax.rsqrt(jnp.mean(centred * centred, axis=-1, keepdims=True) + GROUP_EPS)
    conv_out = jax.nn.silu(
        grouped.reshape(tok_rows, channels) * convolution_group_gain + convolution_group_shift
    ).astype(jnp.bfloat16)
    span_len = math.gcd(64, tok_rows)
    receptance = project(receptance_weight)
    key_all = project(key_weight)
    value_all = project(value_weight)
    decay_logits = project(decay_weight) + decay_offset_bias + position_decay_shift
    decay_logarithm = -jnp.exp(-jax.nn.softplus(-decay_logits) - 0.5) + extra_log_decay
    erase_rate = jax.nn.sigmoid(project(correction_rate_weight))
    out_gate = jax.nn.sigmoid(project(output_gate_weight))
    unit_key = to_blocks(key_all * key_prenorm_gain, span_len)
    unit_key = unit_key * lax.rsqrt(jnp.sum(unit_key * unit_key, axis=-1, keepdims=True) + KEY_EPS)
    erase_dir = unit_key * to_blocks(erase_rate, span_len)
    local_read, carried_read, transfer, local_base = block_pass(
        to_blocks(receptance, span_len),
        to_blocks(decay_logarithm, span_len),
        to_blocks(key_all, span_len),
        to_blocks(value_all, span_len),
        unit_key,
        erase_dir,
    )
    head_count = transfer.shape[0]
    identity = jnp.broadcast_to(jnp.eye(HEAD, dtype=jnp.float32), (head_count, HEAD, HEAD))
    empty = jnp.zeros((head_count, HEAD, HEAD), jnp.float32)
    totals, priors = lax.scan(
        compose, (identity, empty), (jnp.moveaxis(transfer, 1, 0), jnp.moveaxis(local_base, 1, 0))
    )
    total_trans, total_base = totals
    prior_trans, prior_base = priors
    prefix = entering_2((total_trans, total_base), SP, chain, (identity, empty))
    incoming = prefix[1]
    entering = einsum_exact("hij,bhjk->hbik", incoming, prior_trans) + jnp.moveaxis(
        prior_base, 0, 1
    )
    readout = local_read + einsum_exact("hbtk,hbik->hbti", carried_read, entering)
    centred_read = readout - jnp.mean(readout, axis=-1, keepdims=True)
    normed_read = centred_read * lax.rsqrt(
        jnp.mean(centred_read * centred_read, axis=-1, keepdims=True) + HEAD_EPS
    )
    mix_rows = normed_read.transpose(1, 2, 0, 3).reshape(tok_rows, head_count * HEAD)
    mix_out = (mix_rows * head_norm_gain * out_gate).astype(jnp.bfloat16)
    conv_full, mix_full = (
        lax.all_to_all(conv_out, "tp", split_axis=0, concat_axis=1, tiled=True),
        lax.all_to_all(mix_out, "tp", split_axis=0, concat_axis=1, tiled=True),
    )
    projected = jnp.dot(
        conv_full, convolution_output_weight, preferred_element_type=jnp.float32
    ) + jnp.dot(mix_full, attention_output_weight, preferred_element_type=jnp.float32)
    return projected.astype(jnp.bfloat16)


def solution(mesh):
    split = Mesh(mesh.devices.reshape(4, 4, 2, mesh.shape["tp"]), ("sp_0", "sp_1", "sp_2", "tp"))
    placed = (
        P(SP, None),
        P(),
        P(None, "tp"),
        P(None, "tp"),
        P(None, "tp"),
        P("tp"),
        P("tp"),
        P(None, "tp"),
        P(None, "tp"),
        P(None, "tp"),
        P(None, "tp"),
        P(None, "tp"),
        P(None, "tp"),
        P("tp"),
        P("tp"),
        P(SP, "tp"),
        P(SP, "tp"),
        P("tp"),
        P(),
        P(),
    )
    return jax.shard_map(
        local, mesh=split, in_specs=placed, out_specs=P(SP_TP, None), check_vma=False
    )
```

profile of v0, /device:TPU:0, one launch (start us, length us, event | category | flops | bytes accessed | tf_op | source)
XLA Modules:
  0.0 242.4 jit_solution(9391969910535645362)
XLA Ops:
  0.0 1.7 fusion.12
  1.7 2.0 convolution_convert_fusion.7
  4.3 1.4 collective-permute-start
  7.9 2.0 convolution_convert_fusion.3
  10.0 1.1 reshape.123
  11.5 2.0 convolution_convert_fusion.2
  13.7 1.1 reshape.122
  14.7 2.0 convolution_convert_fusion.5
  16.8 1.1 reshape.126
  17.8 1.5 reduce_window_sum.11
  19.4 2.6 %fusion.160 = (f32[4,4,64,64]{3,2,1,0:T(8,128)}, f32[4,4,64,64]{3,2,1,0:T(8,128)S(1)}, f32[4,4,64,64]{3,2,1,0:T(8,128)S(1)}, f32[4,4,64,64]{3,2,1,0:T(8,128)S(1)}) fusion(f32[4,4,64,64]{3,2,1,0:T(8,128)S(1)} %reduce_window_sum.11, f32[4,64,4,64]{3,2,1,0:T(4,128)} %copy-done.5, f32[4,4,64]{2,1,0:T(4,128)S(1)} %add_rsqrt_fusion.1, ...), kind=kLoop, calls=%fused_computation.282 | loop fusion | flops 393216 | bytes 2363392 | tf_op jit(solution)/shard_map/neg | solution.py:75
  22.0 1.8 convolution_multiply_fusion.3
  23.8 1.8 convolution_multiply_fusion
  25.6 1.8 convolution_multiply_fusion.1
  27.4 1.8 fusion.18
  29.3 80.0 %custom-call.4 = f32[4,4,1,64,64]{3,4,2,1,0:T(8,128)} custom-call(f32[4,4,1,64,64]{4,3,2,1,0:T(8,128)} %fusion.18), custom_call_target="InvertDiagBlocksLowerTriangular" | custom-call | tf_op jit(solution)/shard_map/jit(_solve_triangular)/vmap(vmap())/triangular_solve | solution.py:78
  109.3 2.0 convolution_convert_fusion.1
  112.2 1.1 copy.111
  113.4 1.7 convolution_negate_fusion
  115.1 2.4 fusion.25
  117.5 1.0 fusion.32
  118.5 1.4 fusion.20
  120.3 1.0 copy.117
  121.3 1.1 add_bitcast_fusion
  122.4 9.9 %while.17 = (s32[]{:T(128)}, f32[4,64,64]{1,2,0:T(8,128)S(1)}, f32[4,64,64]{1,2,0:T(8,128)S(1)}, f32[4,4,64,64]{2,3,1,0:T(8,128)}, f32[4,4,64,64]{2,3,1,0:T(8,12...) while((s32[]{:T(128)}, f32[4,64,64]{1,2,0:T(8,128)S(1)}, ...), condition=%wide.region_6.7_spmd.clone, body=%wide.region_5.6_spmd.clone.sunk | while | flops 25214980 | bytes 1443436 | solution.py:180
  123.2 1.3 fusion.211
  125.6 1.3 fusion.211
  128.1 1.3 fusion.211
  130.6 1.3 fusion.211
  132.4 4.0 %all-gather = f32[8,64,64]{2,1,0:T(8,128)S(1)} all-gather(f32[4,64,64]{2,1,0:T(8,128)S(1)} %copy.95), channel_id=2, replica_groups=mesh['sp_0'=4,'sp_1'=4,'sp_2'=2,'tp'=4] {'sp_2'}, dimensions={0}, use_global_device_ids=true | all-gather | bytes 196608 | tf_op jit(solution)/shard_map/all_gather | solution.py:38
  138.1 13.1 %all-gather.1 = f32[16,64,64]{2,1,0:T(8,128)S(1)} all-gather(f32[4,64,64]{2,1,0:T(8,128)S(1)} %fusion.112), channel_id=3, replica_groups=mesh['sp_0'=4,'sp_1'=4,'sp_2'=2,'tp'=4] {'sp_1'}, dimensions={0}, use_global_device_ids=true | all-gather | bytes 327680 | tf_op jit(solution)/shard_map/all_gather | solution.py:38
  152.0 2.2 all-gather.3
  154.2 1.1 convolution_add_fusion.12
  155.3 1.2 convolution_add_fusion.11
  156.6 13.3 %all-gather.4 = f32[16,64,64]{2,1,0:T(8,128)S(1)} all-gather(f32[4,64,64]{2,1,0:T(8,128)S(1)} %convolution_add_fusion.11), channel_id=6, replica_groups=mesh['sp_0'=4,'sp_1'=4,'sp_2'=2,'tp'=4] {'sp_1'}, dimensions={0}, use_global_device_ids=true | all-gather | bytes 327680 | tf_op jit(solution)/shard_map/all_gather | solution.py:38
  174.5 1.2 fusion.106
  176.2 15.1 %all-gather.2 = f32[16,64,64]{2,1,0:T(8,128)} all-gather(f32[4,64,64]{2,1,0:T(8,128)S(1)} %fusion.100), channel_id=4, replica_groups=mesh['sp_0'=4,'sp_1'=4,'sp_2'=2,'tp'=4] {'sp_0'}, dimensions={0}, use_global_device_ids=true | all-gather | bytes 327680 | tf_op jit(solution)/shard_map/all_gather | solution.py:38
  191.6 0.9 fusion.95
  193.5 13.8 %all-gather.5 = f32[16,64,64]{2,1,0:T(8,128)} all-gather(f32[4,64,64]{2,1,0:T(8,128)S(1)} %copy-done.25), channel_id=7, replica_groups=mesh['sp_0'=4,'sp_1'=4,'sp_2'=2,'tp'=4] {'sp_0'}, dimensions={0}, use_global_device_ids=true | all-gather | bytes 327680 | tf_op jit(solution)/shard_map/all_gather | solution.py:38
  207.4 1.7 fusion.42
  209.1 1.2 convolution_add_fusion.14
  210.3 1.2 convolution_add_fusion.7
  218.0 1.1 multiply_convert_fusion.1
  219.0 4.3 %all-to-all-start = ((bf16[4,64,128]{2,1,0:T(8,128)(2,1)}), bf16[4,64,128]{2,1,0:T(8,128)(2,1)S(1)}, u32[]{:S(2)}, u32[]{:S(2)}) async-start(bf16[4,64,128]{2,1,0:T(8,128)(2,1)} %bitcast.34), calls=%async_computation | async-start | bytes 131072 | tf_op jit(solution)/shard_map/all_to_all | solution.py:198
  224.1 5.2 %all-to-all-done = bf16[4,64,128]{2,1,0:T(8,128)(2,1)S(1)} async-done(((bf16[4,64,128]{2,1,0:T(8,128)(2,1)}), bf16[4,64,128]{2,1,0:T(8,128)(2,1)S(1)}, u32[]{:S(2)}, u32[]{:S(2)}) %all-to-all-start) | async-done | bytes 65568 | tf_op jit(solution)/shard_map/all_to_all | solution.py:198
  229.3 3.3 %all-to-all-start.1 = ((bf16[4,64,256]{2,1,0:T(8,128)(2,1)}), bf16[4,64,256]{2,1,0:T(8,128)(2,1)S(1)}, u32[]{:S(2)}, u32[]{:S(2)}) async-start(bf16[4,64,256]{2,1,0:T(8,128)(2,1)} %bitcast.56), calls=%async_computation.1 | async-start | bytes 262144 | tf_op jit(solution)/shard_map/all_to_all | solution.py:199
  233.1 5.4 %all-to-all-done.1 = bf16[4,64,256]{2,1,0:T(8,128)(2,1)S(1)} async-done(((bf16[4,64,256]{2,1,0:T(8,128)(2,1)}), bf16[4,64,256]{2,1,0:T(8,128)(2,1)S(1)}, u32[]{:S(2)}, u32[]{:S(2)}) %all-to-all-start.1) | async-done | bytes 131104 | tf_op jit(solution)/shard_map/all_to_all | solution.py:199
  238.6 3.7 %fusion.11 = bf16[64,2048]{1,0:T(8,128)(2,1)} fusion(f32[64,2048]{1,0:T(8,128)S(1)} %fusion.118, bf16[64,1024]{1,0:T(8,128)(2,1)S(1)} %bitcast.216, bf16[1024,2048]{1,0:T(8,128)(2,1)} %param.41), kind=kOutput, calls=%fused_computation.18 | convolution fusion | flops 268697600 | bytes 5111808 | tf_op jit(solution)/shard_map/dot_general | solution.py:203
  (196 shorter events, 24.9 us)
Async XLA Ops:
  0.0 232.7 %copy-start = (bf16[512,2048]{1,0:T(8,128)(2,1)S(1)}, bf16[512,2048]{1,0:T(8,128)(2,1)}, u32[]{:S(2)}) copy-start(bf16[512,2048]{1,0:T(8,128)(2,1)} %param.40) | copy-start | bytes 6291460
  0.0 3.7 %copy-start.32 = (bf16[256,2048]{1,0:T(8,128)(2,1)S(1)}, bf16[256,2048]{1,0:T(8,128)(2,1)}, u32[]{:S(2)}) copy-start(bf16[256,2048]{1,0:T(8,128)(2,1)} %param.22) | copy-start | bytes 3145732
  0.0 3.7 %copy-start.53 = (f32[2048]{0:T(1024)S(1)}, f32[2048]{0:T(1024)}, u32[]{:S(2)}) copy-start(f32[2048]{0:T(1024)} %param.23) | copy-start | bytes 24580
  0.0 3.7 %copy-start.52 = (bf16[2048,128]{1,0:T(8,128)(2,1)S(1)}, bf16[2048,128]{1,0:T(8,128)(2,1)}, u32[]{:S(2)}) copy-start(bf16[2048,128]{1,0:T(8,128)(2,1)} %param.25) | copy-start | bytes 1572868
  1.7 107.6 %copy-start.45 = (f32[256]{0:T(256)}, f32[256]{0:T(256)S(1)}, u32[]{:S(2)}) copy-start(f32[256]{0:T(256)S(1)} %add_rsqrt_fusion.3) | copy-start | bytes 3076
  1.7 4.3 %copy-start.50 = (bf16[2048,256]{1,0:T(8,128)(2,1)S(1)}, bf16[2048,256]{1,0:T(8,128)(2,1)}, u32[]{:S(2)}) copy-start(bf16[2048,256]{1,0:T(8,128)(2,1)} %param.32) | copy-start | bytes 3145732
  4.2 2.3 copy-start.40
  4.2 2.3 copy-start.41
  4.2 2.3 copy-start.47
  4.3 1.5 copy-start.38
  4.3 212.8 %collective-permute-start = (bf16[30,128]{1,0:T(8,128)(2,1)S(1)}, bf16[30,128]{1,0:T(8,128)(2,1)S(1)}, u32[]{:S(2)}, u32[]{:S(2)}) collective-permute-start(bf16[30,128]{1,0:T(8,128)(2,1)S(1)} %slice.378), channel_id=1, source_target_pairs={{0,4},{4,8},{8,12},{12,16},{16,20},{20,24},{24,28},{28,32},{32,36}... | collective-permute-start | bytes 23048 | tf_op jit(solution)/shard_map/ppermute | solution.py:24
  5.8 164.1 %copy-start.11 = (f32[64,64]{1,0:T(8,128)}, f32[64,64]{1,0:T(8,128)S(1)}, u32[]{:S(2)}) copy-start(f32[64,64]{1,0:T(8,128)S(1)} %get-tuple-element.150) | copy-start | bytes 49156
  7.0 3.0 %copy-start.5 = (f32[4,64,4,64]{3,2,1,0:T(4,128)}, f32[4,64,4,64]{3,2,1,0:T(4,128)S(1)}, u32[]{:S(2)}) copy-start(f32[4,64,4,64]{3,2,1,0:T(4,128)S(1)} %reshape.120) | copy-start | bytes 786436
  7.9 3.1 %copy-start.43 = (f32[256]{0:T(256)S(1)}, f32[256]{0:T(256)}, u32[]{:S(2)}) copy-start(f32[256]{0:T(256)} %param.35) | copy-start | bytes 3076
  11.3 3.4 %copy-start.6 = (f32[4,64,4,64]{3,2,1,0:T(4,128)}, f32[4,64,4,64]{3,2,1,0:T(4,128)S(1)}, u32[]{:S(2)}) copy-start(f32[4,64,4,64]{3,2,1,0:T(4,128)S(1)} %reshape.121) | copy-start | bytes 786436
  22.0 5.5 %copy-start.3 = (f32[4,4,64,64]{3,2,1,0:T(8,128)}, f32[4,4,64,64]{3,2,1,0:T(8,128)S(1)}, u32[]{:S(2)}) copy-start(f32[4,4,64,64]{3,2,1,0:T(8,128)S(1)} %get-tuple-element.112) | copy-start | bytes 786436
  22.0 1.8 copy-start.1
  113.3 5.2 %copy-start.9 = (bf16[4,64,4,64]{1,3,0,2:T(8,128)(2,1)}, bf16[4,64,4,64]{1,3,0,2:T(8,128)(2,1)S(1)}, u32[]{:S(2)}) copy-start(bf16[4,64,4,64]{1,3,0,2:T(8,128)(2,1)S(1)} %copy.111) | copy-start | bytes 393220
  113.3 4.1 %copy-start.4 = (f32[4,4,64,64]{3,2,1,0:T(8,128)S(1)}, f32[4,4,64,64]{3,2,1,0:T(8,128)}, u32[]{:S(2)}) copy-start(f32[4,4,64,64]{3,2,1,0:T(8,128)} %copy-done.3) | copy-start | bytes 786436
  115.1 3.5 %copy-start.2 = (f32[4,64,4,64]{3,2,1,0:T(4,128)S(1)}, f32[4,64,4,64]{3,2,1,0:T(4,128)}, u32[]{:S(2)}) copy-start(f32[4,64,4,64]{3,2,1,0:T(4,128)} %reshape.123) | copy-start | bytes 786436
  117.5 2.5 %copy-start.7 = (f32[4,4,64,128]{3,2,1,0:T(8,128)}, f32[4,4,64,128]{3,2,1,0:T(8,128)S(1)}, u32[]{:S(2)}) copy-start(f32[4,4,64,128]{3,2,1,0:T(8,128)S(1)} %fusion.25) | copy-start | bytes 1572868
  138.1 34.8 %copy-start.18 = (f32[4,64,64]{2,1,0:T(8,128)}, f32[4,64,64]{2,1,0:T(8,128)S(1)}, u32[]{:S(2)}) copy-start(f32[4,64,64]{2,1,0:T(8,128)S(1)} %fusion.112) | copy-start | bytes 196612
  155.3 14.6 %copy-start.21 = (f32[4,64,64]{2,1,0:T(8,128)}, f32[4,64,64]{2,1,0:T(8,128)S(1)}, u32[]{:S(2)}) copy-start(f32[4,64,64]{2,1,0:T(8,128)S(1)} %convolution_add_fusion.12) | copy-start | bytes 196612
  156.6 14.2 %copy-start.23 = (f32[4,64,64]{2,1,0:T(8,128)}, f32[4,64,64]{2,1,0:T(8,128)S(1)}, u32[]{:S(2)}) copy-start(f32[4,64,64]{2,1,0:T(8,128)S(1)} %convolution_add_fusion.11) | copy-start | bytes 196612
  170.8 20.6 %copy-start.12 = (f32[64,64]{1,0:T(8,128)S(1)}, f32[64,64]{1,0:T(8,128)}, u32[]{:S(2)}) copy-start(f32[64,64]{1,0:T(8,128)} %copy-done.11) | copy-start | bytes 49156
  174.4 17.2 %copy-start.20 = (f32[4,64,64]{2,1,0:T(8,128)S(1)}, f32[4,64,64]{2,1,0:T(8,128)}, u32[]{:S(2)}) copy-start(f32[4,64,64]{2,1,0:T(8,128)} %fusion.109) | copy-start | bytes 196612
  174.4 18.1 %copy-start.25 = (f32[4,64,64]{2,1,0:T(8,128)S(1)}, f32[4,64,64]{2,1,0:T(8,128)}, u32[]{:S(2)}) copy-start(f32[4,64,64]{2,1,0:T(8,128)} %convolution_add_fusion.8) | copy-start | bytes 196612
  174.4 18.1 %copy-start.27 = (f32[4,64,64]{2,1,0:T(8,128)S(1)}, f32[4,64,64]{2,1,0:T(8,128)}, u32[]{:S(2)}) copy-start(f32[4,64,64]{2,1,0:T(8,128)} %copy-done.26) | copy-start | bytes 196612
  174.4 18.1 %copy-start.29 = (f32[4,64,64]{2,1,0:T(8,128)S(1)}, f32[4,64,64]{2,1,0:T(8,128)}, u32[]{:S(2)}) copy-start(f32[4,64,64]{2,1,0:T(8,128)} %copy-done.28) | copy-start | bytes 196612
  174.4 18.1 %copy-start.31 = (f32[4,64,64]{2,1,0:T(8,128)S(1)}, f32[4,64,64]{2,1,0:T(8,128)}, u32[]{:S(2)}) copy-start(f32[4,64,64]{2,1,0:T(8,128)} %copy-done.30) | copy-start | bytes 196612
  175.7 31.7 %copy-start.10 = (bf16[4,64,4,64]{1,3,0,2:T(8,128)(2,1)S(1)}, bf16[4,64,4,64]{1,3,0,2:T(8,128)(2,1)}, u32[]{:S(2)}) copy-start(bf16[4,64,4,64]{1,3,0,2:T(8,128)(2,1)} %copy-done.9) | copy-start | bytes 393220
  192.6 19.3 %copy-start.8 = (f32[4,4,64,128]{3,2,1,0:T(8,128)S(1)}, f32[4,4,64,128]{3,2,1,0:T(8,128)}, u32[]{:S(2)}) copy-start(f32[4,4,64,128]{3,2,1,0:T(8,128)} %copy-done.7) | copy-start | bytes 1572868
  207.4 4.2 %copy-start.16 = (f32[16,64,64]{2,1,0:T(8,128)S(1)}, f32[16,64,64]{2,1,0:T(8,128)}, u32[]{:S(2)}) copy-start(f32[16,64,64]{2,1,0:T(8,128)} %all-gather.2) | copy-start | bytes 786436
  207.4 4.2 %copy-start.17 = (f32[16,64,64]{2,1,0:T(8,128)S(1)}, f32[16,64,64]{2,1,0:T(8,128)}, u32[]{:S(2)}) copy-start(f32[16,64,64]{2,1,0:T(8,128)} %all-gather.5) | copy-start | bytes 786436
  207.4 4.5 %copy-start.15 = (f32[4,4,64,64]{3,2,1,0:T(8,128)S(1)}, f32[4,4,64,64]{3,2,1,0:T(8,128)}, u32[]{:S(2)}) copy-start(f32[4,4,64,64]{3,2,1,0:T(8,128)} %convolution_multiply_fusion.3) | copy-start | bytes 786436
  211.6 1.6 copy-start.13
  211.6 1.6 copy-start.22
  211.6 1.6 copy-start.24
  211.6 1.6 copy-start.37
  211.9 1.6 copy-start.35
  211.9 1.6 copy-start.36
  213.5 2.3 copy-start.33
  213.5 2.3 copy-start.46
  213.5 2.3 copy-start.51
  213.5 2.3 copy-start.54
  217.9 5.4 %copy-start.44 = (f32[256]{0:T(256)S(1)}, f32[256]{0:T(256)}, u32[]{:S(2)}) copy-start(f32[256]{0:T(256)} %param.39) | copy-start | bytes 3076
  219.0 10.3 %all-to-all-start = ((bf16[4,64,128]{2,1,0:T(8,128)(2,1)}), bf16[4,64,128]{2,1,0:T(8,128)(2,1)S(1)}, u32[]{:S(2)}, u32[]{:S(2)}) async-start(bf16[4,64,128]{2,1,0:T(8,128)(2,1)} %bitcast.34), calls=%async_computation | async-start | bytes 131072 | tf_op jit(solution)/shard_map/all_to_all | solution.py:198
  229.3 9.3 %all-to-all-start.1 = ((bf16[4,64,256]{2,1,0:T(8,128)(2,1)}), bf16[4,64,256]{2,1,0:T(8,128)(2,1)S(1)}, u32[]{:S(2)}, u32[]{:S(2)}) async-start(bf16[4,64,256]{2,1,0:T(8,128)(2,1)} %bitcast.56), calls=%async_computation.1 | async-start | bytes 262144 | tf_op jit(solution)/shard_map/all_to_all | solution.py:199
  (10 other events, 8.4 us)
where the time goes:
time: 243 us; the launch traced here: 242 us
  other arithmetic  93.6 us (39%)
  blocking collectives  61.6 us (25%)
  matrix products  53 us (22%)
  local copies, waits for them, and re-layouts  13.1 us (5%)
  waiting for transfers between devices  10.7 us (4%)
  starting transfers between devices  9.07 us (4%)
    another operation x6, other arithmetic, block_pass(): jax.scipy.linalg.solve_triangular(system, right_side, lower=True, unit_di...  80.1 us
    all_gather x6, blocking collectives, entering_2(): pieces = jax.tree.map(lambda part: lax.all_gather(part, axis), running)  61.6 us
    dot_general x40, matrix products, einsum_exact(): return jnp.einsum(form, left, right, precision=HIGHEST)  34.7 us
    dot_general x8, matrix products, project(): return stored(jnp.dot(normed, weight, preferred_element_type=jnp.float32))  11.6 us
    all_to_all x1, waiting for transfers between devices, local(): lax.all_to_all(mix_out, 'tp', split_axis=0, concat_axis=1, tiled=True)  5.45 us
    all_to_all x1, waiting for transfers between devices, local(): lax.all_to_all(conv_out, 'tp', split_axis=0, concat_axis=1, tiled=True)  5.24 us
  transfers between devices with their start and end apart: 3, of which 2 were waited for; matrix products, arithmetic and copies ran while one was open for 60% of the time, Pallas kernels for 0%

commit v1 on v0

v1 whole, which is shorter than its diff:
```python
import jax
import jax.numpy as jnp
from jax import lax
from jax.experimental import pallas as pl
from jax.experimental.pallas import tpu as pltpu
from jax.sharding import Mesh
from jax.sharding import PartitionSpec as P

HEAD = 64
ROWS = 256
LANES = 256
CONV = 128
SPAN = 64
CHUNKS = ROWS // SPAN
HALO = 32
TAPS = 31
PACK = 2 * HEAD + HALO // 2
SP = ("z", "y", "c")
SP_TP = ("z", "y", "c", "x")

NORM_EPS = 1e-06
GROUP_EPS = 1e-05
HEAD_EPS = 0.00064
KEY_EPS = 1e-06
EXP_HALF = 0.6065306597126334

F32 = jnp.float32
BF16 = jnp.bfloat16
NN = (((1,), (0,)), ((), ()))
NT = (((1,), (1,)), ((), ()))
TN = (((0,), (0,)), ((), ()))
VMEM = pl.BlockSpec(memory_space=pltpu.VMEM)
ANY = pl.BlockSpec(memory_space=pl.ANY)


def mm(left, right, dims=NN):
    return lax.dot_general(
        left.astype(BF16), right.astype(BF16), dims, preferred_element_type=F32
    )


def halves(value):
    high = value.astype(BF16)
    return high, (value - high.astype(F32)).astype(BF16)


def mm3(left, right, dims=NN):
    left_high, left_low = halves(left)
    right_high, right_low = halves(right)
    return mm(left_high, right_high, dims) + (
        mm(left_high, right_low, dims) + mm(left_low, right_high, dims)
    )


def iota(shape, dim):
    return lax.broadcasted_iota(jnp.int32, shape, dim)


def head_lanes(shape, head):
    return (iota(shape, 1) // HEAD) == head


def block_ones(size):
    shape = (size, size)
    return jnp.where(iota(shape, 0) // HEAD == iota(shape, 1) // HEAD, 1.0, 0.0).astype(BF16)


def group_sum(value, ones):
    high, low = halves(value)
    return mm(high, ones) + mm(low, ones)


def expand(compact):
    shape = (LANES, LANES)
    tall = jnp.concatenate([compact] * (LANES // HEAD), axis=0)
    return jnp.where(iota(shape, 0) // HEAD == iota(shape, 1) // HEAD, tall, 0.0)


def shrink(full):
    parts = [full[HEAD * h : HEAD * (h + 1)] for h in range(LANES // HEAD)]
    return (parts[0] + parts[1]) + (parts[2] + parts[3])


def unit_state():
    shape = (HEAD, LANES)
    eye = jnp.where(iota(shape, 0) == iota(shape, 1) % HEAD, 1.0, 0.0)
    return jnp.concatenate([eye, jnp.zeros(shape, F32)], axis=0)


def follow(earlier, trans, base):
    moved = mm3(earlier, expand(trans))
    return jnp.concatenate([moved[:HEAD], moved[HEAD:] + base], axis=0)


def per_chunk(rows):
    return jnp.concatenate([jnp.broadcast_to(row, (SPAN, LANES)) for row in rows], axis=0)


def swap_pair(value):
    return pltpu.roll(value, HEAD, 1)


def local_kernel(
    tokens_hbm,
    gain,
    key_hbm,
    rate_hbm,
    decay_hbm,
    value_hbm,
    conv_value_hbm,
    conv_gate_hbm,
    receptance_hbm,
    gate_hbm,
    key_gain,
    bias,
    shift,
    extra,
    pack_out,
    prior_out,
    local_out,
    query_out,
    gate_out,
    conv_out,
    tokens,
    w_key,
    w_rate,
    w_decay,
    w_value,
    w_conv_value,
    w_conv_gate,
    w_receptance,
    w_gate,
    sems,
):
    pairs = (
        (tokens_hbm, tokens),
        (key_hbm, w_key),
        (rate_hbm, w_rate),
        (decay_hbm, w_decay),
        (value_hbm, w_value),
        (conv_value_hbm, w_conv_value),
        (conv_gate_hbm, w_conv_gate),
        (receptance_hbm, w_receptance),
        (gate_hbm, w_gate),
    )
    copies = [
        pltpu.make_async_copy(source, target, sems.at[n])
        for n, (source, target) in enumerate(pairs)
    ]
    for copy in copies:
        copy.start()
    copies[0].wait()
    rows = tokens[...].astype(F32)
    scale = lax.rsqrt(jnp.mean(rows * rows, axis=-1, keepdims=True) + NORM_EPS)
    normed = (rows * scale * gain[...]).astype(BF16)

    def project(n):
        copies[n].wait()
        return (
            jnp.dot(normed, pairs[n][1][...], preferred_element_type=F32)
            .astype(BF16)
            .astype(F32)
        )

    square = (ROWS, LANES)
    row_at, lane_at = iota(square, 0), iota(square, 1)
    same_chunk = row_at // SPAN == lane_at // SPAN
    ones = block_ones(LANES)

    key = project(1)
    key_scaled = key * key_gain[...]
    unit = key_scaled * lax.rsqrt(group_sum(key_scaled * key_scaled, ones) + KEY_EPS)
    erase = unit * jax.nn.sigmoid(project(2))
    logits = project(3) + bias[...] + shift[...]
    log_decay = extra[...] - EXP_HALF * jax.nn.sigmoid(logits)
    lower = jnp.where(same_chunk & (lane_at <= row_at), 1.0, 0.0).astype(BF16)
    part_high, rest = halves(log_decay)
    part_mid = rest
    part_low = (log_decay - part_high.astype(F32) - rest.astype(F32)).astype(BF16)
    cumulate = mm(lower, part_high) + (mm(lower, part_mid) + mm(lower, part_low))
    before = cumulate - log_decay
    mids = [cumulate[SPAN * c + 31 : SPAN * c + 32] for c in range(CHUNKS)]
    finals = [cumulate[SPAN * c + 63 : SPAN * c + 64] for c in range(CHUNKS)]
    mid = per_chunk(mids)
    rise = jnp.exp(mid - cumulate)
    fall_read = jnp.exp(cumulate - mid)
    unit_s = unit * jnp.exp(before - mid)
    erase_s = erase * rise
    key_s = key * rise
    from_start = per_chunk([jnp.exp(m) for m in mids])
    to_end = per_chunk([jnp.exp(f - m) for f, m in zip(finals, mids)])
    unit_q = unit_s * from_start
    kept_erase = (erase_s * to_end).astype(BF16)
    kept_key = (key_s * to_end).astype(BF16)
    erase_b = erase_s.astype(BF16)
    key_b = key_s.astype(BF16)
    value = project(4)
    value_b = value.astype(BF16)
    value_swapped = [swap_pair(value[:, :128]), swap_pair(value[:, 128:])]

    strict = same_chunk & (lane_at < row_at)
    near = strict & (row_at // 8 == lane_at // 8)
    far = strict & (row_at // 8 != lane_at // 8)
    low_half = iota((ROWS, 128), 1) < HEAD
    solved = []
    for h in range(4):
        pair, own = h // 2, (low_half if h % 2 == 0 else ~low_half)
        span = slice(128 * pair, 128 * pair + 128)
        left = jnp.where(head_lanes(square, h), unit_s, 0.0).astype(BF16)
        erase_mix = mm(left, erase_b, NT)
        key_mix = jnp.where(strict, mm(left, key_b, NT), 0.0)
        d1 = jnp.where(near, erase_mix, 0.0)
        n1 = jnp.where(far, erase_mix, 0.0)
        d2 = mm(d1, d1)
        d4 = mm(d2, d2)
        g = d2 - d1 - mm(d1, d2)
        dinv = g + d4 + mm(g, d4)
        p1 = n1 + mm(dinv, n1)
        p2 = mm(p1, p1)
        p4 = mm(p2, p2)
        key_value = mm(key_mix, value_swapped[pair])
        right = jnp.where(own, unit_q[:, span], key_value)
        y = right + mm(dinv, right)
        y = y + mm(p4, y)
        y = y + mm(p2, y)
        y = mm(p1, y) - y
        solved.append(y)
    weave = []
    removed = []
    for pair in range(2):
        even, odd = solved[2 * pair], solved[2 * pair + 1]
        weave.append(jnp.where(low_half, even, odd))
        removed.append(swap_pair(jnp.where(low_half, odd, even)))
    weave = jnp.concatenate(weave, axis=1).astype(BF16)
    removed = jnp.concatenate(removed, axis=1).astype(BF16)

    same_head = row_at // HEAD == lane_at // HEAD
    eye = row_at == lane_at
    state = unit_state()
    for c in range(CHUNKS):
        here = slice(SPAN * c, SPAN * c + SPAN)
        prior_out[c] = state
        full = mm(weave[here], kept_erase[here], TN)
        trans = jnp.where(same_head, full, 0.0) + jnp.where(
            eye, jnp.broadcast_to(jnp.exp(finals[c]), square), 0.0
        )
        base = mm(removed[here], kept_erase[here], TN) + mm(value_b[here], kept_key[here], TN)
        base = shrink(jnp.where(same_head, base, 0.0))
        moved = mm3(state, trans)
        state = jnp.concatenate([moved[:HEAD], moved[HEAD:] + base], axis=0)
    pack_out[: 2 * HEAD] = state

    conv_input = (project(5) * jax.nn.sigmoid(project(6))).astype(BF16).astype(F32)
    conv_out[...] = conv_input
    pack_out[2 * HEAD :, :128] = conv_input[ROWS - 32 : ROWS - 16]
    pack_out[2 * HEAD :, 128:] = conv_input[ROWS - 16 :]

    receptance = project(7)
    gate_out[...] = jax.nn.sigmoid(project(8))
    read_s = receptance * fall_read
    read_q = read_s * from_start
    inclusive = same_chunk & (lane_at <= row_at)
    found = []
    for h in range(4):
        pair, own = h // 2, (low_half if h % 2 == 0 else ~low_half)
        left = jnp.where(head_lanes(square, h), read_s, 0.0).astype(BF16)
        read_erase = jnp.where(inclusive, mm(left, erase_b, NT), 0.0)
        read_key = jnp.where(inclusive, mm(left, key_b, NT), 0.0)
        mine = jnp.where(own, 0.0, value_swapped[pair])
        found.append(mm(read_erase, solved[h]) + mm(read_key, mine))
    query, local = [], []
    for pair in range(2):
        even, odd = found[2 * pair], found[2 * pair + 1]
        query.append(jnp.where(low_half, even, odd))
        local.append(swap_pair(jnp.where(low_half, odd, even)))
    query = jnp.concatenate(query, axis=1) + read_q
    local = jnp.concatenate(local, axis=1)
    for c in range(CHUNKS):
        here = slice(SPAN * c, SPAN * c + SPAN)
        if c == 0:
            local_out[here] = local[here]
            query_out[here] = query[here].astype(BF16)
        else:
            prior = prior_out[c]
            local_out[here] = local[here] + mm(query[here], expand(prior[HEAD:]), NT)
            query_out[here] = mm(query[here], expand(prior[:HEAD]), NT).astype(BF16)


def conv_kernel(conv_in, taps, gain, shift, done_out, part_out, padded):
    padded[:HALO] = jnp.zeros((HALO, CONV), F32)
    padded[HALO:] = conv_in[...]
    total = jnp.zeros((ROWS, CONV), F32)
    for j in range(TAPS):
        total = total + taps[j : j + 1] * padded[2 + j : 2 + j + ROWS]
    part_out[...] = total[:HALO]
    done_out[...] = finish_conv(total, gain[...], shift[...])


def finish_conv(total, gain, shift):
    ones = block_ones(CONV)
    centred = total - group_sum(total, ones) * (1.0 / HEAD)
    spread = group_sum(centred * centred, ones) * (1.0 / HEAD)
    scaled = centred * lax.rsqrt(spread + GROUP_EPS) * gain + shift
    return (scaled * jax.nn.sigmoid(scaled)).astype(BF16)


def core_kernel(mine, other, pack_out, prefix_out):
    first = lax.axis_index("c") == 0
    early = jnp.where(first, mine[...], other[...])
    late = jnp.where(first, other[...], mine[...])
    joined = follow(early[: 2 * HEAD], late[:HEAD], late[HEAD : 2 * HEAD])
    pack_out[: 2 * HEAD] = joined.astype(BF16)
    pack_out[2 * HEAD :] = late[2 * HEAD :].astype(BF16)
    prefix_out[...] = jnp.where(first, unit_state(), early[: 2 * HEAD])


def row_kernel(own, from_1, from_2, from_3, prefix, pack_out, prefix_out, slots):
    me = lax.axis_index("y")
    for n, ref in enumerate((own, from_1, from_2, from_3)):
        slots[n] = ref[...].astype(F32)
    state = unit_state()
    before = state
    for n in range(4):
        before = jnp.where(me == n, state, before)
        piece = slots[lax.rem(me - n + 4, 4)]
        if n == 0:
            state = piece[: 2 * HEAD]
        else:
            state = follow(state, piece[:HEAD], piece[HEAD : 2 * HEAD])
        if n == 3:
            pack_out[2 * HEAD :] = piece[2 * HEAD :].astype(BF16)
    pack_out[: 2 * HEAD] = state.astype(BF16)
    prefix_out[...] = follow(before, prefix[:HEAD], prefix[HEAD:])


def last_kernel(
    from_1,
    from_2,
    from_3,
    prefix,
    side_core,
    side_row,
    local,
    query,
    gate,
    head_gain,
    conv_done,
    conv_part,
    taps,
    conv_gain,
    conv_shift,
    out_0,
    out_1,
    out_2,
    out_3,
    slots,
    ready,
    padded,
):
    z, y, c, x = (lax.axis_index(name) for name in SP_TP)
    for n, ref in enumerate((from_1, from_2, from_3)):
        slots[n] = ref[: 2 * HEAD].astype(F32)
    state = jnp.zeros((HEAD, LANES), F32)
    for n in range(3):
        piece = slots[lax.rem(z - n + 3, 4)] if n else slots[jnp.maximum(z - 1, 0)]
        if n:
            piece = slots[jnp.clip(z - n - 1, 0, 2)]
            moved = mm3(state, expand(piece[:HEAD])) + piece[HEAD:]
        else:
            moved = piece[HEAD:]
        state = jnp.where(n < z, moved, state)
    state = mm3(state, expand(prefix[:HEAD])) + prefix[HEAD:]
    readout = local[...] + mm(query[...], expand(state), NT)
    ones = block_ones(LANES)
    centred = readout - group_sum(readout, ones) * (1.0 / HEAD)
    spread = group_sum(centred * centred, ones) * (1.0 / HEAD)
    mixed = centred * lax.rsqrt(spread + HEAD_EPS) * head_gain[...] * gate[...]
    ready[:, CONV:] = mixed.astype(BF16)
    ready[:, :CONV] = conv_done[...]

    far = jnp.where(y > 0, side_row[2 * HEAD :].astype(F32), from_1[2 * HEAD :].astype(F32))
    far = jnp.where((y == 0) & (z == 0), 0.0, far)
    side = jnp.where(c == 1, side_core[2 * HEAD :], far)
    padded[:16] = side[:, :128]
    padded[16:32] = side[:, 128:]
    padded[32:] = jnp.zeros((HALO, CONV), F32)
    total = conv_part[...]
    for j in range(TAPS):
        total = total + taps[j : j + 1] * padded[2 + j : 2 + j + HALO]
    ready[:HALO, :CONV] = finish_conv(total, conv_gain[...], conv_shift[...])
    for n, out in enumerate((out_0, out_1, out_2, out_3)):
        to = lax.rem(x + n, 4)
        out[...] = ready[pl.ds(pl.multiple_of(to * SPAN, SPAN), SPAN)]


def project_kernel(own, from_1, from_2, from_3, conv_hbm, mix_hbm, out, conv_w, mix_w, sems):
    x = lax.axis_index("x")
    copies = [
        pltpu.make_async_copy(conv_hbm, conv_w, sems.at[0]),
        pltpu.make_async_copy(mix_hbm, mix_w, sems.at[1]),
    ]
    for copy in copies:
        copy.start()
    for copy in copies:
        copy.wait()
    total = jnp.zeros((SPAN, 2048), F32)
    for n, ref in enumerate((own, from_1, from_2, from_3)):
        of = lax.rem(x - n + 4, 4)
        total = total + jnp.dot(
            ref[:, :CONV],
            conv_w[pl.ds(pl.multiple_of(of * CONV, CONV), CONV)],
            preferred_element_type=F32,
        )
        total = total + jnp.dot(
            ref[:, CONV:],
            mix_w[pl.ds(pl.multiple_of(of * LANES, LANES), LANES)],
            preferred_element_type=F32,
        )
    out[...] = total.astype(BF16)


def shifted(value, axis, steps):
    count = lax.axis_size(axis)
    return lax.ppermute(value, axis, [(s, (s + steps) % count) for s in range(count)])


def params():
    return pltpu.CompilerParams(vmem_limit_bytes=40 * 1024 * 1024)


def call(kernel, name, outs, arguments, specs=None, scratch=()):
    return pl.pallas_call(
        kernel,
        name=name,
        out_shape=[jax.ShapeDtypeStruct(*o) for o in outs],
        in_specs=specs or [VMEM] * len(arguments),
        out_specs=[VMEM] * len(outs),
        scratch_shapes=list(scratch),
        compiler_params=params(),
    )(*arguments)


def local(
    tokens,
    input_norm_gain,
    convolution_value_weight,
    convolution_gate_weight,
    depthwise_taps_weight,
    convolution_group_gain,
    convolution_group_shift,
    receptance_weight,
    key_weight,
    value_weight,
    decay_weight,
    correction_rate_weight,
    output_gate_weight,
    key_prenorm_gain,
    decay_offset_bias,
    position_decay_shift,
    extra_log_decay,
    head_norm_gain,
    convolution_output_weight,
    attention_output_weight,
):
    def as_row(value):
        return value.reshape(1, value.shape[0])

    conv_gain, conv_shift = as_row(convolution_group_gain), as_row(convolution_group_shift)
    wide = (2048, LANES)
    thin = (2048, CONV)
    pack, _, local_read, query, gate, conv_input = call(
        local_kernel,
        "local",
        [
            ((PACK, LANES), F32),
            ((CHUNKS, 2 * HEAD, LANES), F32),
            ((ROWS, LANES), F32),
            ((ROWS, LANES), BF16),
            ((ROWS, LANES), F32),
            ((ROWS, CONV), F32),
        ],
        (
            tokens,
            as_row(input_norm_gain),
            key_weight,
            correction_rate_weight,
            decay_weight,
            value_weight,
            convolution_value_weight,
            convolution_gate_weight,
            receptance_weight,
            output_gate_weight,
            as_row(key_prenorm_gain),
            as_row(decay_offset_bias),
            position_decay_shift,
            extra_log_decay,
        ),
        specs=[ANY, VMEM] + [ANY] * 8 + [VMEM] * 4,
        scratch=[pltpu.VMEM((ROWS, 2048), BF16)]
        + [pltpu.VMEM(wide, BF16)] * 4
        + [pltpu.VMEM(thin, BF16)] * 2
        + [pltpu.VMEM(wide, BF16)] * 2
        + [pltpu.SemaphoreType.DMA((9,))],
    )
    other = shifted(pack, "c", 1)
    conv_done, conv_part = call(
        conv_kernel,
        "conv",
        [((ROWS, CONV), BF16), ((HALO, CONV), F32)],
        (conv_input, depthwise_taps_weight, conv_gain, conv_shift),
        scratch=[pltpu.VMEM((HALO + ROWS, CONV), F32)],
    )
    pack_y, prefix_c = call(
        core_kernel,
        "core",
        [((PACK, LANES), BF16), ((2 * HEAD, LANES), F32)],
        (pack, other),
    )
    rows = [shifted(pack_y, "y", n) for n in (1, 2, 3)]
    pack_z, prefix = call(
        row_kernel,
        "row",
        [((PACK, LANES), BF16), ((2 * HEAD, LANES), F32)],
        (pack_y, *rows, prefix_c),
        scratch=[pltpu.VMEM((4, PACK, LANES), F32)],
    )
    planes = [shifted(pack_z, "z", n) for n in (1, 2, 3)]
    sends = call(
        last_kernel,
        "last",
        [((SPAN, CONV + LANES), BF16)] * 4,
        (
            *planes,
            prefix,
            other,
            rows[0],
            local_read,
            query,
            gate,
            as_row(head_norm_gain),
            conv_done,
            conv_part,
            depthwise_taps_weight,
            conv_gain,
            conv_shift,
        ),
        scratch=[
            pltpu.VMEM((3, 2 * HEAD, LANES), F32),
            pltpu.VMEM((ROWS, CONV + LANES), BF16),
            pltpu.VMEM((2 * HALO, CONV), F32),
        ],
    )
    arrived = [shifted(sends[n], "x", n) for n in (1, 2, 3)]
    (mixed,) = call(
        project_kernel,
        "project",
        [((SPAN, 2048), BF16)],
        (sends[0], *arrived, convolution_output_weight, attention_output_weight),
        specs=[VMEM] * 4 + [ANY] * 2,
        scratch=[
            pltpu.VMEM((512, 2048), BF16),
            pltpu.VMEM((1024, 2048), BF16),
            pltpu.SemaphoreType.DMA((2,)),
        ],
    )
    return mixed


def solution(mesh):
    split = Mesh(mesh.devices.reshape(4, 4, 2, mesh.shape["tp"]), SP_TP)
    placed = (
        P(SP, None),
        P(),
        P(None, "x"),
        P(None, "x"),
        P(None, "x"),
        P("x"),
        P("x"),
        P(None, "x"),
        P(None, "x"),
        P(None, "x"),
        P(None, "x"),
        P(None, "x"),
        P(None, "x"),
        P("x"),
        P("x"),
        P(SP, "x"),
        P(SP, "x"),
        P("x"),
        P(),
        P(),
    )
    return jax.shard_map(
        local, mesh=split, in_specs=placed, out_specs=P(SP_TP, None), check_vma=False
    )
```

time: 243 us -> 65.8 us (0.27)
  other arithmetic: 93.6 us -> 0 us
  blocking collectives: 61.6 us -> 0 us
  matrix products: 53 us -> 0 us
  Pallas kernels: 0 us -> 20.2 us
  starting transfers between devices: 9.07 us -> 16.2 us
  waiting for transfers between devices: 10.7 us -> 14 us
    another operation x7 -> x0, other arithmetic: 81.6 us -> none  [the longest x6 80.1 us: block_pass(): jax.scipy.linalg.solve_triangular(system, right_side, lower=True, unit_di...]
    all_gather x6 -> x0, blocking collectives: 61.6 us -> none  [entering_2(): pieces = jax.tree.map(lambda part: lax.all_gather(part, axis), running)]
    dot_general x50 -> x0, matrix products: 50.5 us -> none  [the longest x40 34.7 us: einsum_exact(): return jnp.einsum(form, left, right, precision=HIGHEST)]
    pallas_call x0 -> x6, Pallas kernels: none -> 20.2 us  [call(): pl.pallas_call(kernel, name=name, out_shape=[jax.ShapeDtypeStruct(*o) for...]
    ppermute x1 -> x10, starting transfers between devices: 1.42 us -> 16.2 us  [shifted(): lax.ppermute(value, axis, [(s, (s + steps) % count) for s in range(count)])]
    ppermute x1 -> x10, waiting for transfers between devices: 0.01 us -> 14 us  [shifted(): lax.ppermute(value, axis, [(s, (s + steps) % count) for s in range(count)])]
    all_to_all x2 -> x0, waiting for transfers between devices: 10.7 us -> none  [the longest x1 5.45 us: local(): lax.all_to_all(mix_out, 'tp', split_axis=0, concat_axis=1, tiled=True)]
    unnamed x112 -> x40, local copies, waits for them, and re-layouts: 4.32 us -> 14.6 us
  transfers between devices with their start and end apart: 3 -> 10, of which waited for: 2 -> 9; matrix products, arithmetic and copies ran while one was open for 60% -> 0% of each run, Pallas kernels for 0% -> 1%
where the time goes in v1:
time: 65.8 us; the launch traced here: 65.2 us
  Pallas kernels  20.2 us (31%)
  starting transfers between devices  16.2 us (25%)
  local copies, waits for them, and re-layouts  14.6 us (22%)
  waiting for transfers between devices  14 us (21%)
    pallas_call x6, Pallas kernels, call(): pl.pallas_call(kernel, name=name, out_shape=[jax.ShapeDtypeStruct(*o) for...  20.2 us
    ppermute x10, starting transfers between devices, shifted(): lax.ppermute(value, axis, [(s, (s + steps) % count) for s in range(count)])  16.2 us
    unnamed x40, local copies, waits for them, and re-layouts  14.6 us
    ppermute x10, waiting for transfers between devices, shifted(): lax.ppermute(value, axis, [(s, (s + steps) % count) for s in range(count)])  14 us
  transfers between devices with their start and end apart: 10, of which 9 were waited for; matrix products, arithmetic and copies ran while one was open for 0% of the time, Pallas kernels for 1%

profile of v1, /device:TPU:0, one launch (start us, length us, event | category | flops | bytes accessed | tf_op | source)
XLA Modules:
  0.0 65.2 jit_solution(15482822130130049383)
XLA Ops:
  0.0 1.2 %copy-done.2 = bf16[256,2048]{1,0:T(8,128)(2,1)S(1)} copy-done((bf16[256,2048]{1,0:T(8,128)(2,1)S(1)}, bf16[256,2048]{1,0:T(8,128)(2,1)}, u32[]{:S(2)}) %copy-start.2) | copy-done | bytes 1048600
  1.2 1.2 %copy-done.3 = bf16[2048,256]{1,0:T(8,128)(2,1)S(1)} copy-done((bf16[2048,256]{1,0:T(8,128)(2,1)S(1)}, bf16[2048,256]{1,0:T(8,128)(2,1)}, u32[]{:S(2)}) %copy-start.3) | copy-done | bytes 1048600
  2.5 1.2 %copy-done.4 = bf16[2048,256]{1,0:T(8,128)(2,1)S(1)} copy-done((bf16[2048,256]{1,0:T(8,128)(2,1)S(1)}, bf16[2048,256]{1,0:T(8,128)(2,1)}, u32[]{:S(2)}) %copy-start.4) | copy-done | bytes 1048600
  3.7 1.2 %copy-done.5 = bf16[2048,256]{1,0:T(8,128)(2,1)S(1)} copy-done((bf16[2048,256]{1,0:T(8,128)(2,1)S(1)}, bf16[2048,256]{1,0:T(8,128)(2,1)}, u32[]{:S(2)}) %copy-start.5) | copy-done | bytes 1048600
  4.9 1.2 %copy-done.6 = bf16[2048,256]{1,0:T(8,128)(2,1)S(1)} copy-done((bf16[2048,256]{1,0:T(8,128)(2,1)S(1)}, bf16[2048,256]{1,0:T(8,128)(2,1)}, u32[]{:S(2)}) %copy-start.6) | copy-done | bytes 1048600
  6.1 1.2 %copy-done.7 = bf16[2048,256]{1,0:T(8,128)(2,1)S(1)} copy-done((bf16[2048,256]{1,0:T(8,128)(2,1)S(1)}, bf16[2048,256]{1,0:T(8,128)(2,1)}, u32[]{:S(2)}) %copy-start.7) | copy-done | bytes 1048600
  7.4 1.2 %copy-done.8 = bf16[2048,256]{1,0:T(8,128)(2,1)S(1)} copy-done((bf16[2048,256]{1,0:T(8,128)(2,1)S(1)}, bf16[2048,256]{1,0:T(8,128)(2,1)}, u32[]{:S(2)}) %copy-start.8) | copy-done | bytes 1048600
  8.6 1.0 %copy-done.9 = bf16[2048,128]{1,0:T(8,128)(2,1)S(1)} copy-done((bf16[2048,128]{1,0:T(8,128)(2,1)S(1)}, bf16[2048,128]{1,0:T(8,128)(2,1)}, u32[]{:S(2)}) %copy-start.9) | copy-done | bytes 524312
  9.6 1.0 %copy-done.10 = bf16[2048,128]{1,0:T(8,128)(2,1)S(1)} copy-done((bf16[2048,128]{1,0:T(8,128)(2,1)S(1)}, bf16[2048,128]{1,0:T(8,128)(2,1)}, u32[]{:S(2)}) %copy-start.10) | copy-done | bytes 524312
  10.7 0.9 %copy-done.11 = f32[256,256]{1,0:T(8,128)S(1)} copy-done((f32[256,256]{1,0:T(8,128)S(1)}, f32[256,256]{1,0:T(8,128)}, u32[]{:S(2)}) %copy-start.11) | copy-done | bytes 262168
  11.6 0.9 %copy-done.12 = f32[256,256]{1,0:T(8,128)S(1)} copy-done((f32[256,256]{1,0:T(8,128)S(1)}, f32[256,256]{1,0:T(8,128)}, u32[]{:S(2)}) %copy-start.12) | copy-done | bytes 262168
  12.6 0.7 %copy-done.14 = f32[2048]{0:T(1024)S(1)} copy-done((f32[2048]{0:T(1024)S(1)}, f32[2048]{0:T(1024)}, u32[]{:S(2)}) %copy-start.14) | copy-done | bytes 8216
  13.3 0.7 %copy-done.17 = f32[256]{0:T(256)S(1)} copy-done((f32[256]{0:T(256)S(1)}, f32[256]{0:T(256)}, u32[]{:S(2)}) %copy-start.17) | copy-done | bytes 1048
  13.9 0.7 %copy-done.18 = f32[256]{0:T(256)S(1)} copy-done((f32[256]{0:T(256)S(1)}, f32[256]{0:T(256)}, u32[]{:S(2)}) %copy-start.18) | copy-done | bytes 1048
  14.6 0.0 copy-start
  14.6 0.0 copy-start.1
  14.7 14.9 %local.1 = (f32[144,256]{1,0:T(8,128)S(1)}, f32[4,128,256]{2,1,0:T(8,128)}, f32[256,256]{1,0:T(8,128)S(1)}, bf16[256,256]{1,0:T(8,128)(2,1)S(1)}, f32[256,256]{1,0:T(8,128)S(1)}, /*index=5*/f32[256,128]{1,0:T(8,128)S(1)}) custom-call(bf16[256,2048]{1,0:T(8,128)(2,1)S(1)} %copy-done.2, f32[1,2048]{1,0:T(1,128)S(1)} %bitcast.6, ...), custom_call_target="tpu_custom_call" | custom-call | tf_op jit(solution)/shard_map/local/pallas_call | solution.py:432
  29.6 0.1 collective-permute-start
  29.7 1.4 %collective-permute-done.other.side_core = f32[144,256]{1,0:T(8,128)S(1)} collective-permute-done((f32[144,256]{1,0:T(8,128)S(1)}, f32[144,256]{1,0:T(8,128)S(1)}, u32[]{:S(2)}, u32[]{:S(2)}) %collective-permute-start) | collective-permute-done | bytes 147488 | tf_op jit(solution)/shard_map/ppermute | solution.py:424
  31.0 0.2 core.1
  31.3 3.2 %collective-permute-start.3 = (bf16[144,256]{1,0:T(8,128)(2,1)S(1)}, bf16[144,256]{1,0:T(8,128)(2,1)S(1)}, u32[]{:S(2)}, u32[]{:S(2)}) collective-permute-start(bf16[144,256]{1,0:T(8,128)(2,1)S(1)} %get-tuple-element.21.own), channel_id=1, source_target_pairs={{0,24},{8,0},{16,8},{24,16},{1,25},{9,1},{17,9},{25,17},{2,26},{10... | collective-permute-start | bytes 221192 | tf_op jit(solution)/shard_map/ppermute | solution.py:424
  34.5 0.6 collective-permute-start.2
  35.1 1.0 %collective-permute-start.1 = (bf16[144,256]{1,0:T(8,128)(2,1)S(1)}, bf16[144,256]{1,0:T(8,128)(2,1)S(1)}, u32[]{:S(2)}, u32[]{:S(2)}) collective-permute-start(bf16[144,256]{1,0:T(8,128)(2,1)S(1)} %get-tuple-element.21.own), channel_id=1, source_target_pairs={{0,8},{8,16},{16,24},{24,0},{1,9},{9,17},{17,25},{25,1},{2,10},{10... | collective-permute-start | bytes 221192 | tf_op jit(solution)/shard_map/ppermute | solution.py:424
  36.1 1.8 %collective-permute-done.3.from_3 = bf16[144,256]{1,0:T(8,128)(2,1)S(1)} collective-permute-done((bf16[144,256]{1,0:T(8,128)(2,1)S(1)}, bf16[144,256]{1,0:T(8,128)(2,1)S(1)}, u32[]{:S(2)}, u32[]{:S(2)}) %collective-permute-start.3) | collective-permute-done | bytes 73760 | tf_op jit(solution)/shard_map/ppermute | solution.py:424
  37.9 2.9 %collective-permute-done.2.from_2 = bf16[144,256]{1,0:T(8,128)(2,1)S(1)} collective-permute-done((bf16[144,256]{1,0:T(8,128)(2,1)S(1)}, bf16[144,256]{1,0:T(8,128)(2,1)S(1)}, u32[]{:S(2)}, u32[]{:S(2)}) %collective-permute-start.2) | collective-permute-done | bytes 73760 | tf_op jit(solution)/shard_map/ppermute | solution.py:424
  40.8 0.8 %collective-permute-done.1.from_1.side_row = bf16[144,256]{1,0:T(8,128)(2,1)S(1)} collective-permute-done((bf16[144,256]{1,0:T(8,128)(2,1)S(1)}, bf16[144,256]{1,0:T(8,128)(2,1)S(1)}, u32[]{:S(2)}, u32[]{:S(2)}) %collective-permute-start.1) | collective-permute-done | bytes 73760 | tf_op jit(solution)/shard_map/ppermute | solution.py:424
  41.6 0.7 %row.1 = (bf16[144,256]{1,0:T(8,128)(2,1)S(1)}, f32[128,256]{1,0:T(8,128)S(1)}) custom-call(bf16[144,256]{1,0:T(8,128)(2,1)S(1)} %get-tuple-element.21.own, bf16[144,256]{1,0:T(8,128)(2,1)S(1)} %collective-permute-done.1.from_1.side_row, bf16[144,256]{1,0:T(8,128)(2,1)S(1)} %collective-permute-done.2.from_2, ...), custom_call_target="tpu_custom_call" | custom-call | tf_op jit(solution)/shard_map/row/pallas_call | solution.py:432
  42.3 4.3 %collective-permute-start.6 = (bf16[144,256]{1,0:T(8,128)(2,1)S(1)}, bf16[144,256]{1,0:T(8,128)(2,1)S(1)}, u32[]{:S(2)}, u32[]{:S(2)}) collective-permute-start(bf16[144,256]{1,0:T(8,128)(2,1)S(1)} %get-tuple-element.23), channel_id=1, source_target_pairs={{0,96},{32,0},{64,32},{96,64},{1,97},{33,1},{65,33},{97,65},{2,98}... | collective-permute-start | bytes 221192 | tf_op jit(solution)/shard_map/ppermute | solution.py:424
  46.6 0.0 collective-permute-start.5
  46.6 1.3 %collective-permute-start.4 = (bf16[144,256]{1,0:T(8,128)(2,1)S(1)}, bf16[144,256]{1,0:T(8,128)(2,1)S(1)}, u32[]{:S(2)}, u32[]{:S(2)}) collective-permute-start(bf16[144,256]{1,0:T(8,128)(2,1)S(1)} %get-tuple-element.23), channel_id=1, source_target_pairs={{0,32},{32,64},{64,96},{96,0},{1,33},{33,65},{65,97},{97,1},{2,34}... | collective-permute-start | bytes 221192 | tf_op jit(solution)/shard_map/ppermute | solution.py:424
  47.9 0.0 copy-done.13
  47.9 0.0 copy-done.15
  47.9 0.0 copy-done.16
  47.9 0.6 conv.1
  48.5 1.0 %collective-permute-done.6.from_3 = bf16[144,256]{1,0:T(8,128)(2,1)S(1)} collective-permute-done((bf16[144,256]{1,0:T(8,128)(2,1)S(1)}, bf16[144,256]{1,0:T(8,128)(2,1)S(1)}, u32[]{:S(2)}, u32[]{:S(2)}) %collective-permute-start.6) | collective-permute-done | bytes 73760 | tf_op jit(solution)/shard_map/ppermute | solution.py:424
  49.5 2.9 %collective-permute-done.5.from_2 = bf16[144,256]{1,0:T(8,128)(2,1)S(1)} collective-permute-done((bf16[144,256]{1,0:T(8,128)(2,1)S(1)}, bf16[144,256]{1,0:T(8,128)(2,1)S(1)}, u32[]{:S(2)}, u32[]{:S(2)}) %collective-permute-start.5) | collective-permute-done | bytes 73760 | tf_op jit(solution)/shard_map/ppermute | solution.py:424
  52.5 0.5 collective-permute-done.4.from_1
  53.0 0.0 copy-done.19
  53.0 1.3 %last.1 = (bf16[64,384]{1,0:T(8,128)(2,1)S(1)}, bf16[64,384]{1,0:T(8,128)(2,1)S(1)}, bf16[64,384]{1,0:T(8,128)(2,1)S(1)}, bf16[64,384]{1,0:T(8,128)(2,1)S(1)}) custom-call(bf16[144,256]{1,0:T(8,128)(2,1)S(1)} %collective-permute-done.4.from_1, bf16[144,256]{1,0:T(8,128)(2,1)S(1)} %collective-permute-done.5.from_2, ...), custom_call_target="tpu_custom_call" | custom-call | tf_op jit(solution)/shard_map/last/pallas_call | solution.py:432
  54.3 1.6 %collective-permute-start.7 = (bf16[64,384]{1,0:T(8,128)(2,1)S(1)}, bf16[64,384]{1,0:T(8,128)(2,1)S(1)}, u32[]{:S(2)}, u32[]{:S(2)}) collective-permute-start(bf16[64,384]{1,0:T(8,128)(2,1)S(1)} %get-tuple-element.32), channel_id=1, source_target_pairs={{0,1},{1,2},{2,3},{3,0},{4,5},{5,6},{6,7},{7,4},{8,9},{9,10},{10,1... | collective-permute-start | bytes 147464 | tf_op jit(solution)/shard_map/ppermute | solution.py:424
  55.9 2.7 %collective-permute-start.8 = (bf16[64,384]{1,0:T(8,128)(2,1)S(1)}, bf16[64,384]{1,0:T(8,128)(2,1)S(1)}, u32[]{:S(2)}, u32[]{:S(2)}) collective-permute-start(bf16[64,384]{1,0:T(8,128)(2,1)S(1)} %get-tuple-element.33), channel_id=1, source_target_pairs={{0,2},{1,3},{2,0},{3,1},{4,6},{5,7},{6,4},{7,5},{8,10},{9,11},{10,... | collective-permute-start | bytes 147464 | tf_op jit(solution)/shard_map/ppermute | solution.py:424
  58.6 1.4 %collective-permute-start.9 = (bf16[64,384]{1,0:T(8,128)(2,1)S(1)}, bf16[64,384]{1,0:T(8,128)(2,1)S(1)}, u32[]{:S(2)}, u32[]{:S(2)}) collective-permute-start(bf16[64,384]{1,0:T(8,128)(2,1)S(1)} %get-tuple-element.34), channel_id=1, source_target_pairs={{0,3},{1,0},{2,1},{3,2},{4,7},{5,4},{6,5},{7,6},{8,11},{9,8},{10,9... | collective-permute-start | bytes 147464 | tf_op jit(solution)/shard_map/ppermute | solution.py:424
  60.0 0.0 collective-permute-done.7.from_1
  60.0 1.4 %collective-permute-done.8.from_2 = bf16[64,384]{1,0:T(8,128)(2,1)S(1)} collective-permute-done((bf16[64,384]{1,0:T(8,128)(2,1)S(1)}, bf16[64,384]{1,0:T(8,128)(2,1)S(1)}, u32[]{:S(2)}, u32[]{:S(2)}) %collective-permute-start.8) | collective-permute-done | bytes 49184 | tf_op jit(solution)/shard_map/ppermute | solution.py:424
  61.5 1.2 %collective-permute-done.9.from_3 = bf16[64,384]{1,0:T(8,128)(2,1)S(1)} collective-permute-done((bf16[64,384]{1,0:T(8,128)(2,1)S(1)}, bf16[64,384]{1,0:T(8,128)(2,1)S(1)}, u32[]{:S(2)}, u32[]{:S(2)}) %collective-permute-start.9) | collective-permute-done | bytes 49184 | tf_op jit(solution)/shard_map/ppermute | solution.py:424
  62.7 0.0 copy-done
  62.7 0.0 copy-done.1
  62.7 2.3 %project.1 = bf16[64,2048]{1,0:T(8,128)(2,1)} custom-call(bf16[64,384]{1,0:T(8,128)(2,1)S(1)} %get-tuple-element.31.own, bf16[64,384]{1,0:T(8,128)(2,1)S(1)} %collective-permute-done.7.from_1, bf16[64,384]{1,0:T(8,128)(2,1)S(1)} %collective-permute-done.8.from_2, bf16[64,384]{1,0:T(8,128)(2,1)S(1)} %collective-permute-done.9.from_3, ...), custom_call_target="tpu_custom_call" | custom-call | tf_op jit(solution)/shard_map/project/pallas_call | solution.py:432
  (18 shorter events, 0.0 us)
Async XLA Ops:
  0.0 1.2 %copy-start.2 = (bf16[256,2048]{1,0:T(8,128)(2,1)S(1)}, bf16[256,2048]{1,0:T(8,128)(2,1)}, u32[]{:S(2)}) copy-start(bf16[256,2048]{1,0:T(8,128)(2,1)} %tokens_hbm.1) | copy-start | bytes 3145732
  1.2 1.2 %copy-start.3 = (bf16[2048,256]{1,0:T(8,128)(2,1)S(1)}, bf16[2048,256]{1,0:T(8,128)(2,1)}, u32[]{:S(2)}) copy-start(bf16[2048,256]{1,0:T(8,128)(2,1)} %key_hbm.1) | copy-start | bytes 3145732
  2.5 1.2 %copy-start.4 = (bf16[2048,256]{1,0:T(8,128)(2,1)S(1)}, bf16[2048,256]{1,0:T(8,128)(2,1)}, u32[]{:S(2)}) copy-start(bf16[2048,256]{1,0:T(8,128)(2,1)} %rate_hbm.1) | copy-start | bytes 3145732
  3.7 1.2 %copy-start.5 = (bf16[2048,256]{1,0:T(8,128)(2,1)S(1)}, bf16[2048,256]{1,0:T(8,128)(2,1)}, u32[]{:S(2)}) copy-start(bf16[2048,256]{1,0:T(8,128)(2,1)} %decay_hbm.1) | copy-start | bytes 3145732
  4.9 1.2 %copy-start.6 = (bf16[2048,256]{1,0:T(8,128)(2,1)S(1)}, bf16[2048,256]{1,0:T(8,128)(2,1)}, u32[]{:S(2)}) copy-start(bf16[2048,256]{1,0:T(8,128)(2,1)} %value_hbm.1) | copy-start | bytes 3145732
  6.1 1.2 %copy-start.7 = (bf16[2048,256]{1,0:T(8,128)(2,1)S(1)}, bf16[2048,256]{1,0:T(8,128)(2,1)}, u32[]{:S(2)}) copy-start(bf16[2048,256]{1,0:T(8,128)(2,1)} %receptance_hbm.1) | copy-start | bytes 3145732
  7.4 1.2 %copy-start.8 = (bf16[2048,256]{1,0:T(8,128)(2,1)S(1)}, bf16[2048,256]{1,0:T(8,128)(2,1)}, u32[]{:S(2)}) copy-start(bf16[2048,256]{1,0:T(8,128)(2,1)} %gate_hbm.1) | copy-start | bytes 3145732
  8.6 1.0 %copy-start.9 = (bf16[2048,128]{1,0:T(8,128)(2,1)S(1)}, bf16[2048,128]{1,0:T(8,128)(2,1)}, u32[]{:S(2)}) copy-start(bf16[2048,128]{1,0:T(8,128)(2,1)} %conv_value_hbm.1) | copy-start | bytes 1572868
  9.6 1.0 %copy-start.10 = (bf16[2048,128]{1,0:T(8,128)(2,1)S(1)}, bf16[2048,128]{1,0:T(8,128)(2,1)}, u32[]{:S(2)}) copy-start(bf16[2048,128]{1,0:T(8,128)(2,1)} %conv_gate_hbm.1) | copy-start | bytes 1572868
  10.7 0.9 %copy-start.11 = (f32[256,256]{1,0:T(8,128)S(1)}, f32[256,256]{1,0:T(8,128)}, u32[]{:S(2)}) copy-start(f32[256,256]{1,0:T(8,128)} %shift.1) | copy-start | bytes 786436
  11.6 0.9 %copy-start.12 = (f32[256,256]{1,0:T(8,128)S(1)}, f32[256,256]{1,0:T(8,128)}, u32[]{:S(2)}) copy-start(f32[256,256]{1,0:T(8,128)} %extra.1) | copy-start | bytes 786436
  12.6 0.7 %copy-start.14 = (f32[2048]{0:T(1024)S(1)}, f32[2048]{0:T(1024)}, u32[]{:S(2)}) copy-start(f32[2048]{0:T(1024)} %param.21) | copy-start | bytes 24580
  13.3 0.7 %copy-start.17 = (f32[256]{0:T(256)S(1)}, f32[256]{0:T(256)}, u32[]{:S(2)}) copy-start(f32[256]{0:T(256)} %param.33) | copy-start | bytes 3076
  13.9 0.7 %copy-start.18 = (f32[256]{0:T(256)S(1)}, f32[256]{0:T(256)}, u32[]{:S(2)}) copy-start(f32[256]{0:T(256)} %param.34) | copy-start | bytes 3076
  14.6 33.2 %copy-start.13 = (f32[31,128]{1,0:T(8,128)S(1)}, f32[31,128]{1,0:T(8,128)}, u32[]{:S(2)}) copy-start(f32[31,128]{1,0:T(8,128)} %taps.3) | copy-start | bytes 47620
  14.6 33.2 %copy-start.15 = (f32[128]{0:T(128)S(1)}, f32[128]{0:T(128)}, u32[]{:S(2)}) copy-start(f32[128]{0:T(128)} %param.25) | copy-start | bytes 1540
  14.6 33.2 %copy-start.16 = (f32[128]{0:T(128)S(1)}, f32[128]{0:T(128)}, u32[]{:S(2)}) copy-start(f32[128]{0:T(128)} %param.26) | copy-start | bytes 1540
  14.6 38.3 %copy-start.19 = (f32[256]{0:T(256)S(1)}, f32[256]{0:T(256)}, u32[]{:S(2)}) copy-start(f32[256]{0:T(256)} %param.37) | copy-start | bytes 3076
  14.6 48.1 %copy-start = (bf16[1024,2048]{1,0:T(8,128)(2,1)S(1)}, bf16[1024,2048]{1,0:T(8,128)(2,1)}, u32[]{:S(2)}) copy-start(bf16[1024,2048]{1,0:T(8,128)(2,1)} %mix_hbm.1) | copy-start | bytes 12582916
  14.6 48.1 %copy-start.1 = (bf16[512,2048]{1,0:T(8,128)(2,1)S(1)}, bf16[512,2048]{1,0:T(8,128)(2,1)}, u32[]{:S(2)}) copy-start(bf16[512,2048]{1,0:T(8,128)(2,1)} %conv_hbm.1) | copy-start | bytes 6291460
  29.6 1.5 %collective-permute-start = (f32[144,256]{1,0:T(8,128)S(1)}, f32[144,256]{1,0:T(8,128)S(1)}, u32[]{:S(2)}, u32[]{:S(2)}) collective-permute-start(f32[144,256]{1,0:T(8,128)S(1)} %get-tuple-element.20.mine), channel_id=1, source_target_pairs={{0,4},{4,0},{1,5},{5,1},{2,6},{6,2},{3,7},{7,3},{8,12},{12,8},{9,1... | collective-permute-start | bytes 442376 | tf_op jit(solution)/shard_map/ppermute | solution.py:424
  31.3 6.6 %collective-permute-start.3 = (bf16[144,256]{1,0:T(8,128)(2,1)S(1)}, bf16[144,256]{1,0:T(8,128)(2,1)S(1)}, u32[]{:S(2)}, u32[]{:S(2)}) collective-permute-start(bf16[144,256]{1,0:T(8,128)(2,1)S(1)} %get-tuple-element.21.own), channel_id=1, source_target_pairs={{0,24},{8,0},{16,8},{24,16},{1,25},{9,1},{17,9},{25,17},{2,26},{10... | collective-permute-start | bytes 221192 | tf_op jit(solution)/shard_map/ppermute | solution.py:424
  34.5 6.3 %collective-permute-start.2 = (bf16[144,256]{1,0:T(8,128)(2,1)S(1)}, bf16[144,256]{1,0:T(8,128)(2,1)S(1)}, u32[]{:S(2)}, u32[]{:S(2)}) collective-permute-start(bf16[144,256]{1,0:T(8,128)(2,1)S(1)} %get-tuple-element.21.own), channel_id=1, source_target_pairs={{0,16},{8,24},{16,0},{24,8},{1,17},{9,25},{17,1},{25,9},{2,18},{10... | collective-permute-start | bytes 221192 | tf_op jit(solution)/shard_map/ppermute | solution.py:424
  35.1 6.5 %collective-permute-start.1 = (bf16[144,256]{1,0:T(8,128)(2,1)S(1)}, bf16[144,256]{1,0:T(8,128)(2,1)S(1)}, u32[]{:S(2)}, u32[]{:S(2)}) collective-permute-start(bf16[144,256]{1,0:T(8,128)(2,1)S(1)} %get-tuple-element.21.own), channel_id=1, source_target_pairs={{0,8},{8,16},{16,24},{24,0},{1,9},{9,17},{17,25},{25,1},{2,10},{10... | collective-permute-start | bytes 221192 | tf_op jit(solution)/shard_map/ppermute | solution.py:424
  42.3 7.2 %collective-permute-start.6 = (bf16[144,256]{1,0:T(8,128)(2,1)S(1)}, bf16[144,256]{1,0:T(8,128)(2,1)S(1)}, u32[]{:S(2)}, u32[]{:S(2)}) collective-permute-start(bf16[144,256]{1,0:T(8,128)(2,1)S(1)} %get-tuple-element.23), channel_id=1, source_target_pairs={{0,96},{32,0},{64,32},{96,64},{1,97},{33,1},{65,33},{97,65},{2,98}... | collective-permute-start | bytes 221192 | tf_op jit(solution)/shard_map/ppermute | solution.py:424
  46.6 5.9 %collective-permute-start.5 = (bf16[144,256]{1,0:T(8,128)(2,1)S(1)}, bf16[144,256]{1,0:T(8,128)(2,1)S(1)}, u32[]{:S(2)}, u32[]{:S(2)}) collective-permute-start(bf16[144,256]{1,0:T(8,128)(2,1)S(1)} %get-tuple-element.23), channel_id=1, source_target_pairs={{0,64},{32,96},{64,0},{96,32},{1,65},{33,97},{65,1},{97,33},{2,66}... | collective-permute-start | bytes 221192 | tf_op jit(solution)/shard_map/ppermute | solution.py:424
  46.6 6.4 %collective-permute-start.4 = (bf16[144,256]{1,0:T(8,128)(2,1)S(1)}, bf16[144,256]{1,0:T(8,128)(2,1)S(1)}, u32[]{:S(2)}, u32[]{:S(2)}) collective-permute-start(bf16[144,256]{1,0:T(8,128)(2,1)S(1)} %get-tuple-element.23), channel_id=1, source_target_pairs={{0,32},{32,64},{64,96},{96,0},{1,33},{33,65},{65,97},{97,1},{2,34}... | collective-permute-start | bytes 221192 | tf_op jit(solution)/shard_map/ppermute | solution.py:424
  54.3 5.7 %collective-permute-start.7 = (bf16[64,384]{1,0:T(8,128)(2,1)S(1)}, bf16[64,384]{1,0:T(8,128)(2,1)S(1)}, u32[]{:S(2)}, u32[]{:S(2)}) collective-permute-start(bf16[64,384]{1,0:T(8,128)(2,1)S(1)} %get-tuple-element.32), channel_id=1, source_target_pairs={{0,1},{1,2},{2,3},{3,0},{4,5},{5,6},{6,7},{7,4},{8,9},{9,10},{10,1... | collective-permute-start | bytes 147464 | tf_op jit(solution)/shard_map/ppermute | solution.py:424
  55.9 5.6 %collective-permute-start.8 = (bf16[64,384]{1,0:T(8,128)(2,1)S(1)}, bf16[64,384]{1,0:T(8,128)(2,1)S(1)}, u32[]{:S(2)}, u32[]{:S(2)}) collective-permute-start(bf16[64,384]{1,0:T(8,128)(2,1)S(1)} %get-tuple-element.33), channel_id=1, source_target_pairs={{0,2},{1,3},{2,0},{3,1},{4,6},{5,7},{6,4},{7,5},{8,10},{9,11},{10,... | collective-permute-start | bytes 147464 | tf_op jit(solution)/shard_map/ppermute | solution.py:424
  58.6 4.1 %collective-permute-start.9 = (bf16[64,384]{1,0:T(8,128)(2,1)S(1)}, bf16[64,384]{1,0:T(8,128)(2,1)S(1)}, u32[]{:S(2)}, u32[]{:S(2)}) collective-permute-start(bf16[64,384]{1,0:T(8,128)(2,1)S(1)} %get-tuple-element.34), channel_id=1, source_target_pairs={{0,3},{1,0},{2,1},{3,2},{4,7},{5,4},{6,5},{7,6},{8,11},{9,8},{10,9... | collective-permute-start | bytes 147464 | tf_op jit(solution)/shard_map/ppermute | solution.py:424

commit v2 on v1

--- a/solution.py
+++ b/solution.py
@@ -1,3 +1,5 @@
+import functools
+
 import jax
 import jax.numpy as jnp
 from jax import lax
@@ -30,7 +32,7 @@
 NT = (((1,), (1,)), ((), ()))
 TN = (((0,), (0,)), ((), ()))
 VMEM = pl.BlockSpec(memory_space=pltpu.VMEM)
-ANY = pl.BlockSpec(memory_space=pl.ANY)
+HBM = pl.BlockSpec(memory_space=pltpu.HBM)
 
 
 def mm(left, right, dims=NN):
@@ -100,103 +102,77 @@
     return pltpu.roll(value, HEAD, 1)
 
 
-def local_kernel(
-    tokens_hbm,
-    gain,
-    key_hbm,
-    rate_hbm,
-    decay_hbm,
-    value_hbm,
-    conv_value_hbm,
-    conv_gate_hbm,
-    receptance_hbm,
-    gate_hbm,
-    key_gain,
-    bias,
-    shift,
-    extra,
-    pack_out,
-    prior_out,
-    local_out,
-    query_out,
-    gate_out,
-    conv_out,
-    tokens,
-    w_key,
-    w_rate,
-    w_decay,
-    w_value,
-    w_conv_value,
-    w_conv_gate,
-    w_receptance,
-    w_gate,
-    sems,
-):
-    pairs = (
-        (tokens_hbm, tokens),
-        (key_hbm, w_key),
-        (rate_hbm, w_rate),
-        (decay_hbm, w_decay),
-        (value_hbm, w_value),
-        (conv_value_hbm, w_conv_value),
-        (conv_gate_hbm, w_conv_gate),
-        (receptance_hbm, w_receptance),
-        (gate_hbm, w_gate),
-    )
+def local_kernel(*refs):
+    sources = refs[:12]
+    pack_out, prior_out, conv_out, normed_out, fall_out, start_out = refs[12:18]
+    erase_out, key_out, value_out, solved_out = refs[18:22]
+    targets = refs[22:34]
+    sems = refs[34]
     copies = [
         pltpu.make_async_copy(source, target, sems.at[n])
-        for n, (source, target) in enumerate(pairs)
+        for n, (source, target) in enumerate(zip(sources, targets))
     ]
     for copy in copies:
         copy.start()
+    tokens, gain, key_gain, bias, shift, extra = targets[:6]
     copies[0].wait()
+    copies[1].wait()
     rows = tokens[...].astype(F32)
     scale = lax.rsqrt(jnp.mean(rows * rows, axis=-1, keepdims=True) + NORM_EPS)
     normed = (rows * scale * gain[...]).astype(BF16)
+    normed_out[...] = normed
 
     def project(n):
         copies[n].wait()
-        return (
-            jnp.dot(normed, pairs[n][1][...], preferred_element_type=F32)
-            .astype(BF16)
-            .astype(F32)
-        )
+        return rounded_product(normed, targets[n][...])
 
     square = (ROWS, LANES)
     row_at, lane_at = iota(square, 0), iota(square, 1)
     same_chunk = row_at // SPAN == lane_at // SPAN
     ones = block_ones(LANES)
 
-    key = project(1)
+    key = project(6)
+    copies[2].wait()
     key_scaled = key * key_gain[...]
     unit = key_scaled * lax.rsqrt(group_sum(key_scaled * key_scaled, ones) + KEY_EPS)
-    erase = unit * jax.nn.sigmoid(project(2))
-    logits = project(3) + bias[...] + shift[...]
+    erase = unit * jax.nn.sigmoid(project(7))
+    decay = project(8)
+    for n in (3, 4, 5):
+        copies[n].wait()
+    logits = decay + bias[...] + shift[...]
     log_decay = extra[...] - EXP_HALF * jax.nn.sigmoid(logits)
     lower = jnp.where(same_chunk & (lane_at <= row_at), 1.0, 0.0).astype(BF16)
-    part_high, rest = halves(log_decay)
-    part_mid = rest
-    part_low = (log_decay - part_high.astype(F32) - rest.astype(F32)).astype(BF16)
+    part_high, part_mid = halves(log_decay)
+    part_low = (log_decay - part_high.astype(F32) - part_mid.astype(F32)).astype(BF16)
     cumulate = mm(lower, part_high) + (mm(lower, part_mid) + mm(lower, part_low))
     before = cumulate - log_decay
     mids = [cumulate[SPAN * c + 31 : SPAN * c + 32] for c in range(CHUNKS)]
     finals = [cumulate[SPAN * c + 63 : SPAN * c + 64] for c in range(CHUNKS)]
     mid = per_chunk(mids)
     rise = jnp.exp(mid - cumulate)
-    fall_read = jnp.exp(cumulate - mid)
+    fall_out[...] = jnp.exp(cumulate - mid)
     unit_s = unit * jnp.exp(before - mid)
     erase_s = erase * rise
     key_s = key * rise
-    from_start = per_chunk([jnp.exp(m) for m in mids])
+    starts = [jnp.exp(m) for m in mids]
+    for c in range(CHUNKS):
+        start_out[c : c + 1] = starts[c]
     to_end = per_chunk([jnp.exp(f - m) for f, m in zip(finals, mids)])
-    unit_q = unit_s * from_start
+    unit_q = unit_s * per_chunk(starts)
     kept_erase = (erase_s * to_end).astype(BF16)
     kept_key = (key_s * to_end).astype(BF16)
     erase_b = erase_s.astype(BF16)
     key_b = key_s.astype(BF16)
-    value = project(4)
+    value = project(9)
     value_b = value.astype(BF16)
-    value_swapped = [swap_pair(value[:, :128]), swap_pair(value[:, 128:])]
+    value_swapped = [
+        swap_pair(value[:, :128]).astype(BF16),
+        swap_pair(value[:, 128:]).astype(BF16),
+    ]
+    erase_out[...] = erase_b
+    key_out[...] = key_b
+    value_out[:, :128] = value_swapped[0]
+    value_out[:, 128:] = value_swapped[1]
 
     strict = same_chunk & (lane_at < row_at)
     near = strict & (row_at // 8 == lane_at // 8)
@@ -225,6 +201,7 @@
         y = y + mm(p2, y)
         y = mm(p1, y) - y
         solved.append(y)
+        solved_out[h] = y.astype(BF16)
     weave = []
     removed = []
     for pair in range(2):
@@ -250,23 +227,51 @@
         state = jnp.concatenate([moved[:HEAD], moved[HEAD:] + base], axis=0)
     pack_out[: 2 * HEAD] = state
 
-    conv_input = (project(5) * jax.nn.sigmoid(project(6))).astype(BF16).astype(F32)
+    conv_input = rounded(project(10) * jax.nn.sigmoid(project(11)))
     conv_out[...] = conv_input
     pack_out[2 * HEAD :, :128] = conv_input[ROWS - 32 : ROWS - 16]
     pack_out[2 * HEAD :, 128:] = conv_input[ROWS - 16 :]
 
-    receptance = project(7)
-    gate_out[...] = jax.nn.sigmoid(project(8))
-    read_s = receptance * fall_read
-    read_q = read_s * from_start
-    inclusive = same_chunk & (lane_at <= row_at)
+
+def rounded(value):
+    return value.astype(BF16).astype(F32)
+
+
+def rounded_product(left, right):
+    return rounded(jnp.dot(left, right, preferred_element_type=F32))
+
+
+def read_kernel(
+    normed,
+    w_receptance,
+    w_gate,
+    fall,
+    start,
+    erase,
+    key,
+    value_swapped,
+    solved,
+    priors,
+    local_out,
+    query_out,
+    gate_out,
+):
+    square = (ROWS, LANES)
+    row_at, lane_at = iota(square, 0), iota(square, 1)
+    low_half = iota((ROWS, 128), 1) < HEAD
+    receptance = rounded_product(normed[...], w_receptance[...])
+    gate_out[...] = jax.nn.sigmoid(rounded_product(normed[...], w_gate[...]))
+    read_s = receptance * fall[...]
+    read_q = read_s * per_chunk([start[c : c + 1] for c in range(CHUNKS)])
+    inclusive = (row_at // SPAN == lane_at // SPAN) & (lane_at <= row_at)
     found = []
     for h in range(4):
         pair, own = h // 2, (low_half if h % 2 == 0 else ~low_half)
+        span = slice(128 * pair, 128 * pair + 128)
         left = jnp.where(head_lanes(square, h), read_s, 0.0).astype(BF16)
-        read_erase = jnp.where(inclusive, mm(left, erase_b, NT), 0.0)
-        read_key = jnp.where(inclusive, mm(left, key_b, NT), 0.0)
-        mine = jnp.where(own, 0.0, value_swapped[pair])
+        read_erase = jnp.where(inclusive, mm(left, erase[...], NT), 0.0)
+        read_key = jnp.where(inclusive, mm(left, key[...], NT), 0.0)
+        mine = jnp.where(own, 0.0, value_swapped[:, span].astype(F32))
         found.append(mm(read_erase, solved[h]) + mm(read_key, mine))
     query, local = [], []
     for pair in range(2):
@@ -281,7 +286,7 @@
             local_out[here] = local[here]
             query_out[here] = query[here].astype(BF16)
         else:
-            prior = prior_out[c]
+            prior = priors[c]
             local_out[here] = local[here] + mm(query[here], expand(prior[HEAD:]), NT)
             query_out[here] = mm(query[here], expand(prior[:HEAD]), NT).astype(BF16)
 
@@ -304,42 +309,46 @@
     return (scaled * jax.nn.sigmoid(scaled)).astype(BF16)
 
 
-def core_kernel(mine, other, pack_out, prefix_out):
+def joined(lower, upper):
+    return follow(lower[: 2 * HEAD], upper[:HEAD], upper[HEAD : 2 * HEAD])
+
+
+def core_kernel(mine, other, pack_out, total_out, prefix_out):
     first = lax.axis_index("c") == 0
     early = jnp.where(first, mine[...], other[...])
     late = jnp.where(first, other[...], mine[...])
-    joined = follow(early[: 2 * HEAD], late[:HEAD], late[HEAD : 2 * HEAD])
-    pack_out[: 2 * HEAD] = joined.astype(BF16)
+    total = joined(early, late)
+    total_out[...] = total
+    pack_out[: 2 * HEAD] = total.astype(BF16)
     pack_out[2 * HEAD :] = late[2 * HEAD :].astype(BF16)
-    prefix_out[...] = jnp.where(first, unit_state(), early[: 2 * HEAD])
-
-
-def row_kernel(own, from_1, from_2, from_3, prefix, pack_out, prefix_out, slots):
-    me = lax.axis_index("y")
-    for n, ref in enumerate((own, from_1, from_2, from_3)):
-        slots[n] = ref[...].astype(F32)
-    state = unit_state()
-    before = state
-    for n in range(4):
-        before = jnp.where(me == n, state, before)
-        piece = slots[lax.rem(me - n + 4, 4)]
-        if n == 0:
-            state = piece[: 2 * HEAD]
-        else:
-            state = follow(state, piece[:HEAD], piece[HEAD : 2 * HEAD])
-        if n == 3:
-            pack_out[2 * HEAD :] = piece[2 * HEAD :].astype(BF16)
-    pack_out[: 2 * HEAD] = state.astype(BF16)
-    prefix_out[...] = follow(before, prefix[:HEAD], prefix[HEAD:])
+    prefix_out[: 2 * HEAD] = jnp.where(first, unit_state(), early[: 2 * HEAD])
+    prefix_out[2 * HEAD :] = jnp.where(first, 0.0, early[2 * HEAD :])
+
+
+def pair_kernel(axis, far, sent, mine, total, other, prefix, pack_out, total_out, prefix_out):
+    at = lax.axis_index(axis)
+    upper = (at >= 2) if far else (lax.rem(at, 2) == 1)
+    got = other[...].astype(F32)
+    states = got[: 2 * HEAD]
+    early = jnp.where(upper, states, total[...])
+    late = jnp.where(upper, total[...], states)
+    result = joined(early, late)
+    total_out[...] = result
+    pack_out[: HEAD * sent] = result[HEAD * (2 - sent) :].astype(BF16)
+    tail = other if far else mine
+    pack_out[HEAD * sent :] = tail[2 * HEAD :]
+    behind = joined(states, prefix[...])
+    prefix_out[: 2 * HEAD] = jnp.where(upper, behind, prefix[: 2 * HEAD])
+    takes = (at == 2) if far else upper
+    takes = takes & (lax.axis_index("c") == 0)
+    if axis == "z":
+        takes = takes & (lax.axis_index("y") == 0)
+    prefix_out[2 * HEAD :] = jnp.where(takes, got[2 * HEAD :], prefix[2 * HEAD :])
 
 
 def last_kernel(
-    from_1,
-    from_2,
-    from_3,
+    other,
     prefix,
-    side_core,
-    side_row,
     local,
     query,
     gate,
@@ -353,23 +362,13 @@
     out_1,
     out_2,
     out_3,
-    slots,
     ready,
     padded,
 ):
     z, y, c, x = (lax.axis_index(name) for name in SP_TP)
-    for n, ref in enumerate((from_1, from_2, from_3)):
-        slots[n] = ref[: 2 * HEAD].astype(F32)
-    state = jnp.zeros((HEAD, LANES), F32)
-    for n in range(3):
-        piece = slots[lax.rem(z - n + 3, 4)] if n else slots[jnp.maximum(z - 1, 0)]
-        if n:
-            piece = slots[jnp.clip(z - n - 1, 0, 2)]
-            moved = mm3(state, expand(piece[:HEAD])) + piece[HEAD:]
-        else:
-            moved = piece[HEAD:]
-        state = jnp.where(n < z, moved, state)
-    state = mm3(state, expand(prefix[:HEAD])) + prefix[HEAD:]
+    got = other[...].astype(F32)
+    entering = jnp.where(z >= 2, got[:HEAD], 0.0)
+    state = mm3(entering, expand(prefix[:HEAD])) + prefix[HEAD : 2 * HEAD]
     readout = local[...] + mm(query[...], expand(state), NT)
     ones = block_ones(LANES)
     centred = readout - group_sum(readout, ones) * (1.0 / HEAD)
@@ -378,9 +377,8 @@
     ready[:, CONV:] = mixed.astype(BF16)
     ready[:, :CONV] = conv_done[...]
 
-    far = jnp.where(y > 0, side_row[2 * HEAD :].astype(F32), from_1[2 * HEAD :].astype(F32))
-    far = jnp.where((y == 0) & (z == 0), 0.0, far)
-    side = jnp.where(c == 1, side_core[2 * HEAD :], far)
+    takes = (z == 2) & (y == 0) & (c == 0)
+    side = jnp.where(takes, got[HEAD:], prefix[2 * HEAD :])
     padded[:16] = side[:, :128]
     padded[16:32] = side[:, 128:]
     padded[32:] = jnp.zeros((HALO, CONV), F32)
@@ -393,16 +391,8 @@
         out[...] = ready[pl.ds(pl.multiple_of(to * SPAN, SPAN), SPAN)]
 
 
-def project_kernel(own, from_1, from_2, from_3, conv_hbm, mix_hbm, out, conv_w, mix_w, sems):
+def project_kernel(own, from_1, from_2, from_3, conv_w, mix_w, out):
     x = lax.axis_index("x")
-    copies = [
-        pltpu.make_async_copy(conv_hbm, conv_w, sems.at[0]),
-        pltpu.make_async_copy(mix_hbm, mix_w, sems.at[1]),
-    ]
-    for copy in copies:
-        copy.start()
-    for copy in copies:
-        copy.wait()
     total = jnp.zeros((SPAN, 2048), F32)
     for n, ref in enumerate((own, from_1, from_2, from_3)):
         of = lax.rem(x - n + 4, 4)
@@ -422,6 +412,11 @@
 def shifted(value, axis, steps):
     count = lax.axis_size(axis)
     return lax.ppermute(value, axis, [(s, (s + steps) % count) for s in range(count)])
+
+
+def swapped(value, axis, bits):
+    count = lax.axis_size(axis)
+    return lax.ppermute(value, axis, [(s, s ^ bits) for s in range(count)])
 
 
 def params():
@@ -466,43 +461,69 @@
         return value.reshape(1, value.shape[0])
 
     conv_gain, conv_shift = as_row(convolution_group_gain), as_row(convolution_group_shift)
-    wide = (2048, LANES)
-    thin = (2048, CONV)
-    pack, _, local_read, query, gate, conv_input = call(
+    wide = pltpu.VMEM((2048, LANES), BF16)
+    thin = pltpu.VMEM((2048, CONV), BF16)
+    row = pltpu.VMEM((1, LANES), F32)
+    square = ((ROWS, LANES), F32)
+    square_b = ((ROWS, LANES), BF16)
+    state = ((2 * HEAD, LANES), F32)
+    packed = ((PACK, LANES), F32)
+    packed_b = ((PACK, LANES), BF16)
+    pack, priors, conv_input, normed, fall, start, erase, key, value_swapped, solved = call(
         local_kernel,
         "local",
         [
-            ((PACK, LANES), F32),
+            packed,
             ((CHUNKS, 2 * HEAD, LANES), F32),
-            ((ROWS, LANES), F32),
-            ((ROWS, LANES), BF16),
-            ((ROWS, LANES), F32),
             ((ROWS, CONV), F32),
+            ((ROWS, 2048), BF16),
+            square,
+            ((8, LANES), F32),
+            square_b,
+            square_b,
+            square_b,
+            ((4, ROWS, CONV), BF16),
         ],
         (
             tokens,
             as_row(input_norm_gain),
+            as_row(key_prenorm_gain),
+            as_row(decay_offset_bias),
+            position_decay_shift,
+            extra_log_decay,
             key_weight,
             correction_rate_weight,
             decay_weight,
             value_weight,
             convolution_value_weight,
             convolution_gate_weight,
+        ),
+        specs=[HBM] * 12,
+        scratch=[pltpu.VMEM((ROWS, 2048), BF16), pltpu.VMEM((1, 2048), F32), row, row]
+        + [pltpu.VMEM((ROWS, LANES), F32)] * 2
+        + [wide] * 4
+        + [thin] * 2
+        + [pltpu.SemaphoreType.DMA((12,))],
+    )
+    other = swapped(pack, "c", 1)
+    pack, total, prefix = call(core_kernel, "core", [packed_b, state, packed], (pack, other))
+    local_read, query, gate = call(
+        read_kernel,
+        "read",
+        [square, square_b, square],
+        (
+            normed,
             receptance_weight,
             output_gate_weight,
-            as_row(key_prenorm_gain),
-            as_row(decay_offset_bias),
-            position_decay_shift,
-            extra_log_decay,
+            fall,
+            start,
+            erase,
+            key,
+            value_swapped,
+            solved,
+            priors,
         ),
-        specs=[ANY, VMEM] + [ANY] * 8 + [VMEM] * 4,
-        scratch=[pltpu.VMEM((ROWS, 2048), BF16)]
-        + [pltpu.VMEM(wide, BF16)] * 4
-        + [pltpu.VMEM(thin, BF16)] * 2
-        + [pltpu.VMEM(wide, BF16)] * 2
-        + [pltpu.SemaphoreType.DMA((9,))],
-    )
-    other = shifted(pack, "c", 1)
+    )
     conv_done, conv_part = call(
         conv_kernel,
         "conv",
@@ -510,30 +531,23 @@
         (conv_input, depthwise_taps_weight, conv_gain, conv_shift),
         scratch=[pltpu.VMEM((HALO + ROWS, CONV), F32)],
     )
-    pack_y, prefix_c = call(
-        core_kernel,
-        "core",
-        [((PACK, LANES), BF16), ((2 * HEAD, LANES), F32)],
-        (pack, other),
-    )
-    rows = [shifted(pack_y, "y", n) for n in (1, 2, 3)]
-    pack_z, prefix = call(
-        row_kernel,
-        "row",
-        [((PACK, LANES), BF16), ((2 * HEAD, LANES), F32)],
-        (pack_y, *rows, prefix_c),
-        scratch=[pltpu.VMEM((4, PACK, LANES), F32)],
-    )
-    planes = [shifted(pack_z, "z", n) for n in (1, 2, 3)]
+    for axis, far in (("y", False), ("y", True), ("z", False)):
+        other = swapped(pack, axis, 3 if far else 1)
+        sent = 1 if axis == "z" else 2
+        pack, total, prefix = call(
+            functools.partial(pair_kernel, axis, far, sent),
+            f"pair_{axis}{3 if far else 1}",
+            [((HEAD * sent + HALO // 2, LANES), BF16), state, packed],
+            (pack, total, other, prefix),
+        )
+    other = swapped(pack, "z", 3)
     sends = call(
         last_kernel,
         "last",
         [((SPAN, CONV + LANES), BF16)] * 4,
         (
-            *planes,
+            other,
             prefix,
-            other,
-            rows[0],
             local_read,
             query,
             gate,
@@ -545,7 +559,6 @@
             conv_shift,
         ),
         scratch=[
-            pltpu.VMEM((3, 2 * HEAD, LANES), F32),
             pltpu.VMEM((ROWS, CONV + LANES), BF16),
             pltpu.VMEM((2 * HALO, CONV), F32),
         ],
@@ -556,12 +569,6 @@
         "project",
         [((SPAN, 2048), BF16)],
         (sends[0], *arrived, convolution_output_weight, attention_output_weight),
-        specs=[VMEM] * 4 + [ANY] * 2,
-        scratch=[
-            pltpu.VMEM((512, 2048), BF16),
-            pltpu.VMEM((1024, 2048), BF16),
-            pltpu.SemaphoreType.DMA((2,)),
-        ],
     )
     return mixed
 

time: 65.8 us -> 61.3 us (0.932)
  waiting for transfers between devices: 14 us -> 11.4 us
  local copies, waits for them, and re-layouts: 14.6 us -> 12.2 us
  starting transfers between devices: 16.2 us -> 17 us
    ppermute x10 -> x3, waiting for transfers between devices: 14 us -> 2.65 us  [shifted(): lax.ppermute(value, axis, [(s, (s + steps) % count) for s in range(count)])]
    ppermute x0 -> x5, starting transfers between devices: none -> 11.3 us  [swapped(): return lax.ppermute(value, axis, [(s, s ^ bits) for s in range(count)])]
    ppermute x10 -> x3, starting transfers between devices: 16.2 us -> 5.72 us  [shifted(): lax.ppermute(value, axis, [(s, (s + steps) % count) for s in range(count)])]
    ppermute x0 -> x5, waiting for transfers between devices: none -> 8.8 us  [swapped(): return lax.ppermute(value, axis, [(s, s ^ bits) for s in range(count)])]
    unnamed x40, local copies, waits for them, and re-layouts: 14.6 us -> 12.2 us
    pallas_call x6 -> x9, Pallas kernels: 20.2 us -> 19.9 us  [call(): pl.pallas_call(kernel, name=name, out_shape=[jax.ShapeDtypeStruct(*o) for...]
  transfers between devices with their start and end apart: 10 -> 8, of which waited for: 9 -> 6; matrix products, arithmetic and copies ran while one was open for 0% -> 0% of each run, Pallas kernels for 1% -> 4%
where the time goes in v2:
time: 61.3 us; the launch traced here: 60.7 us
  Pallas kernels  19.9 us (32%)
  starting transfers between devices  17 us (28%)
  local copies, waits for them, and re-layouts  12.2 us (20%)
  waiting for transfers between devices  11.4 us (19%)
    pallas_call x9, Pallas kernels, call(): pl.pallas_call(kernel, name=name, out_shape=[jax.ShapeDtypeStruct(*o) for...  19.9 us
    unnamed x40, local copies, waits for them, and re-layouts  12.2 us
    ppermute x5, starting transfers between devices, swapped(): return lax.ppermute(value, axis, [(s, s ^ bits) for s in range(count)])  11.3 us
    ppermute x5, waiting for transfers between devices, swapped(): return lax.ppermute(value, axis, [(s, s ^ bits) for s in range(count)])  8.8 us
    ppermute x3, starting transfers between devices, shifted(): lax.ppermute(value, axis, [(s, (s + steps) % count) for s in range(count)])  5.72 us
    ppermute x3, waiting for transfers between devices, shifted(): lax.ppermute(value, axis, [(s, (s + steps) % count) for s in range(count)])  2.65 us
  transfers between devices with their start and end apart: 8, of which 6 were waited for; matrix products, arithmetic and copies ran while one was open for 0% of the time, Pallas kernels for 4%

profile of v2, /device:TPU:0, one launch (start us, length us, event | category | flops | bytes accessed | tf_op | source)
XLA Modules:
  0.0 60.7 jit_solution(17700310174543986699)
XLA Ops:
  0.0 1.2 %copy-done.2 = bf16[256,2048]{1,0:T(8,128)(2,1)S(1)} copy-done((bf16[256,2048]{1,0:T(8,128)(2,1)S(1)}, bf16[256,2048]{1,0:T(8,128)(2,1)}, u32[]{:S(2)}) %copy-start.2) | copy-done | bytes 1048600
  1.2 1.2 %copy-done.3 = bf16[2048,256]{1,0:T(8,128)(2,1)S(1)} copy-done((bf16[2048,256]{1,0:T(8,128)(2,1)S(1)}, bf16[2048,256]{1,0:T(8,128)(2,1)}, u32[]{:S(2)}) %copy-start.3) | copy-done | bytes 1048600
  2.5 1.2 %copy-done.4 = bf16[2048,256]{1,0:T(8,128)(2,1)S(1)} copy-done((bf16[2048,256]{1,0:T(8,128)(2,1)S(1)}, bf16[2048,256]{1,0:T(8,128)(2,1)}, u32[]{:S(2)}) %copy-start.4) | copy-done | bytes 1048600
  3.7 1.2 %copy-done.5 = bf16[2048,256]{1,0:T(8,128)(2,1)S(1)} copy-done((bf16[2048,256]{1,0:T(8,128)(2,1)S(1)}, bf16[2048,256]{1,0:T(8,128)(2,1)}, u32[]{:S(2)}) %copy-start.5) | copy-done | bytes 1048600
  4.9 1.2 %copy-done.6 = bf16[2048,256]{1,0:T(8,128)(2,1)S(1)} copy-done((bf16[2048,256]{1,0:T(8,128)(2,1)S(1)}, bf16[2048,256]{1,0:T(8,128)(2,1)}, u32[]{:S(2)}) %copy-start.6) | copy-done | bytes 1048600
  6.1 1.0 %copy-done.9 = bf16[2048,128]{1,0:T(8,128)(2,1)S(1)} copy-done((bf16[2048,128]{1,0:T(8,128)(2,1)S(1)}, bf16[2048,128]{1,0:T(8,128)(2,1)}, u32[]{:S(2)}) %copy-start.9) | copy-done | bytes 524312
  7.2 1.0 %copy-done.10 = bf16[2048,128]{1,0:T(8,128)(2,1)S(1)} copy-done((bf16[2048,128]{1,0:T(8,128)(2,1)S(1)}, bf16[2048,128]{1,0:T(8,128)(2,1)}, u32[]{:S(2)}) %copy-start.10) | copy-done | bytes 524312
  8.2 0.9 %copy-done.11 = f32[256,256]{1,0:T(8,128)S(1)} copy-done((f32[256,256]{1,0:T(8,128)S(1)}, f32[256,256]{1,0:T(8,128)}, u32[]{:S(2)}) %copy-start.11) | copy-done | bytes 262168
  9.2 0.9 %copy-done.12 = f32[256,256]{1,0:T(8,128)S(1)} copy-done((f32[256,256]{1,0:T(8,128)S(1)}, f32[256,256]{1,0:T(8,128)}, u32[]{:S(2)}) %copy-start.12) | copy-done | bytes 262168
  10.1 0.7 %copy-done.14 = f32[2048]{0:T(1024)S(1)} copy-done((f32[2048]{0:T(1024)S(1)}, f32[2048]{0:T(1024)}, u32[]{:S(2)}) %copy-start.14) | copy-done | bytes 8216
  10.8 0.7 %copy-done.17 = f32[256]{0:T(256)S(1)} copy-done((f32[256]{0:T(256)S(1)}, f32[256]{0:T(256)}, u32[]{:S(2)}) %copy-start.17) | copy-done | bytes 1048
  11.5 0.7 %copy-done.18 = f32[256]{0:T(256)S(1)} copy-done((f32[256]{0:T(256)S(1)}, f32[256]{0:T(256)}, u32[]{:S(2)}) %copy-start.18) | copy-done | bytes 1048
  12.2 0.0 copy-start.8
  12.2 12.7 %local.1 = (f32[144,256]{1,0:T(8,128)S(1)}, f32[4,128,256]{2,1,0:T(8,128)S(1)}, f32[256,128]{1,0:T(8,128)S(1)}, bf16[256,2048]{1,0:T(8,128)(2,1)S(1)}, f32[256,2...) custom-call(bf16[256,2048]{1,0:T(8,128)(2,1)S(1)} %copy-done.2, ...), custom_call_target="tpu_custom_call" | custom-call | tf_op jit(solution)/shard_map/local/pallas_call | solution.py:427
  24.9 0.0 copy-start.19
  24.9 0.0 copy-start
  24.9 0.0 copy-start.1
  24.9 0.1 collective-permute-start
  25.0 1.4 %collective-permute-done.other = f32[144,256]{1,0:T(8,128)S(1)} collective-permute-done((f32[144,256]{1,0:T(8,128)S(1)}, f32[144,256]{1,0:T(8,128)S(1)}, u32[]{:S(2)}, u32[]{:S(2)}) %collective-permute-start) | collective-permute-done | bytes 147488 | tf_op jit(solution)/shard_map/ppermute | solution.py:419
  26.4 0.3 core.1
  26.6 1.8 %collective-permute-start.1 = (bf16[144,256]{1,0:T(8,128)(2,1)S(1)}, bf16[144,256]{1,0:T(8,128)(2,1)S(1)}, u32[]{:S(2)}, u32[]{:S(2)}) collective-permute-start(bf16[144,256]{1,0:T(8,128)(2,1)S(1)} %get-tuple-element.36.mine), channel_id=1, source_target_pairs={{0,8},{8,0},{16,24},{24,16},{1,9},{9,1},{17,25},{25,17},{2,10},{10... | collective-permute-start | bytes 221192 | tf_op jit(solution)/shard_map/ppermute | solution.py:419
  28.4 2.7 %collective-permute-done.1.other = bf16[144,256]{1,0:T(8,128)(2,1)S(1)} collective-permute-done((bf16[144,256]{1,0:T(8,128)(2,1)S(1)}, bf16[144,256]{1,0:T(8,128)(2,1)S(1)}, u32[]{:S(2)}, u32[]{:S(2)}) %collective-permute-start.1) | collective-permute-done | bytes 73760 | tf_op jit(solution)/shard_map/ppermute | solution.py:419
  31.1 0.3 pair_y1.1
  31.4 3.2 %collective-permute-start.2 = (bf16[144,256]{1,0:T(8,128)(2,1)S(1)}, bf16[144,256]{1,0:T(8,128)(2,1)S(1)}, u32[]{:S(2)}, u32[]{:S(2)}) collective-permute-start(bf16[144,256]{1,0:T(8,128)(2,1)S(1)} %get-tuple-element.39.mine), channel_id=1, source_target_pairs={{0,24},{8,16},{16,8},{24,0},{1,25},{9,17},{17,9},{25,1},{2,26},{10... | collective-permute-start | bytes 221192 | tf_op jit(solution)/shard_map/ppermute | solution.py:419
  34.6 2.4 %collective-permute-done.2.other = bf16[144,256]{1,0:T(8,128)(2,1)S(1)} collective-permute-done((bf16[144,256]{1,0:T(8,128)(2,1)S(1)}, bf16[144,256]{1,0:T(8,128)(2,1)S(1)}, u32[]{:S(2)}, u32[]{:S(2)}) %collective-permute-start.2) | collective-permute-done | bytes 73760 | tf_op jit(solution)/shard_map/ppermute | solution.py:419
  37.0 0.3 pair_y3.1
  37.4 2.1 %collective-permute-start.3 = (bf16[144,256]{1,0:T(8,128)(2,1)S(1)}, bf16[144,256]{1,0:T(8,128)(2,1)S(1)}, u32[]{:S(2)}, u32[]{:S(2)}) collective-permute-start(bf16[144,256]{1,0:T(8,128)(2,1)S(1)} %get-tuple-element.42.mine), channel_id=1, source_target_pairs={{0,32},{32,0},{64,96},{96,64},{1,33},{33,1},{65,97},{97,65},{2,34}... | collective-permute-start | bytes 221192 | tf_op jit(solution)/shard_map/ppermute | solution.py:419
  39.5 2.3 %collective-permute-done.3.other = bf16[144,256]{1,0:T(8,128)(2,1)S(1)} collective-permute-done((bf16[144,256]{1,0:T(8,128)(2,1)S(1)}, bf16[144,256]{1,0:T(8,128)(2,1)S(1)}, u32[]{:S(2)}, u32[]{:S(2)}) %collective-permute-start.3) | collective-permute-done | bytes 73760 | tf_op jit(solution)/shard_map/ppermute | solution.py:419
  41.8 1.0 %pair_z1.1 = (bf16[80,256]{1,0:T(8,128)(2,1)S(1)}, f32[128,256]{1,0:T(8,128)}, f32[144,256]{1,0:T(8,128)S(1)}) custom-call(bf16[144,256]{1,0:T(8,128)(2,1)S(1)} %get-tuple-element.42.mine, f32[128,256]{1,0:T(8,128)S(1)} %get-tuple-element.43.total, bf16[144,256]{1,0:T(8,128)(2,1)S(1)} %collective-permute-done.3.other, f32[144,256]{1,0:T(8,128)S(1)} %get-tuple-element.44.prefix), custom_call_target="tpu_custom_call" | custom-call | tf_op jit(solution)/shard_map/pair_z1/pallas_call | solution.py:427
  42.8 4.1 %collective-permute-start.4 = (bf16[80,256]{1,0:T(8,128)(2,1)S(1)}, bf16[80,256]{1,0:T(8,128)(2,1)S(1)}, u32[]{:S(2)}, u32[]{:S(2)}) collective-permute-start(bf16[80,256]{1,0:T(8,128)(2,1)S(1)} %get-tuple-element.45), channel_id=1, source_target_pairs={{0,96},{32,64},{64,32},{96,0},{1,97},{33,65},{65,33},{97,1},{2,98}... | collective-permute-start | bytes 122888 | tf_op jit(solution)/shard_map/ppermute | solution.py:419
  46.9 0.0 copy-done.13
  46.9 0.0 copy-done.15
  46.9 0.0 copy-done.16
  47.0 0.6 %conv.1 = (bf16[256,128]{1,0:T(8,128)(2,1)S(1)}, f32[32,128]{1,0:T(8,128)S(1)}) custom-call(f32[256,128]{1,0:T(8,128)S(1)} %get-tuple-element.58.conv_in, f32[31,128]{1,0:T(8,128)S(1)} %copy-done.13, f32[1,128]{1,0:T(1,128)S(1)} %bitcast.7, f32[1,128]{1,0:T(1,128)S(1)} %bitcast.9), custom_call_target="tpu_custom_call" | custom-call | tf_op jit(solution)/shard_map/conv/pallas_call | solution.py:427
  47.6 0.0 copy-done.7
  47.6 0.0 copy-done.8
  47.6 1.9 %read.1 = (f32[256,256]{1,0:T(8,128)S(1)}, bf16[256,256]{1,0:T(8,128)(2,1)S(1)}, f32[256,256]{1,0:T(8,128)S(1)}) custom-call(bf16[256,2048]{1,0:T(8,128)(2,1)S(1)} %get-tuple-element.47.normed, bf16[2048,256]{1,0:T(8,128)(2,1)S(1)} %copy-done.7, bf16[2048,256]{1,0:T(8,128)(2,1)S(1)} %copy-done.8, f32[256,256]{1,0:T(8,128)S(1)} %get-tuple-element.48.fall, ...), custom_call_target="tpu_custom_call" | custom-call | tf_op jit(solution)/shard_map/read/pallas_call | solution.py:427
  49.5 0.0 collective-permute-done.4.other
  49.5 0.0 copy-done.19
  49.5 0.9 %last.1 = (bf16[64,384]{1,0:T(8,128)(2,1)S(1)}, bf16[64,384]{1,0:T(8,128)(2,1)S(1)}, bf16[64,384]{1,0:T(8,128)(2,1)S(1)}, bf16[64,384]{1,0:T(8,128)(2,1)S(1)}) custom-call(bf16[80,256]{1,0:T(8,128)(2,1)S(1)} %collective-permute-done.4.other, f32[144,256]{1,0:T(8,128)S(1)} %get-tuple-element.46.prefix, f32[256,256]{1,0:T(8,128)S(1)} %get-tuple-element.55.local, ...), custom_call_target="tpu_custom_call" | custom-call | tf_op jit(solution)/shard_map/last/pallas_call | solution.py:427
  50.4 1.6 %collective-permute-start.5 = (bf16[64,384]{1,0:T(8,128)(2,1)S(1)}, bf16[64,384]{1,0:T(8,128)(2,1)S(1)}, u32[]{:S(2)}, u32[]{:S(2)}) collective-permute-start(bf16[64,384]{1,0:T(8,128)(2,1)S(1)} %get-tuple-element.62), channel_id=1, source_target_pairs={{0,1},{1,2},{2,3},{3,0},{4,5},{5,6},{6,7},{7,4},{8,9},{9,10},{10,1... | collective-permute-start | bytes 147464 | tf_op jit(solution)/shard_map/ppermute | solution.py:414
  52.0 2.7 %collective-permute-start.6 = (bf16[64,384]{1,0:T(8,128)(2,1)S(1)}, bf16[64,384]{1,0:T(8,128)(2,1)S(1)}, u32[]{:S(2)}, u32[]{:S(2)}) collective-permute-start(bf16[64,384]{1,0:T(8,128)(2,1)S(1)} %get-tuple-element.63), channel_id=1, source_target_pairs={{0,2},{1,3},{2,0},{3,1},{4,6},{5,7},{6,4},{7,5},{8,10},{9,11},{10,... | collective-permute-start | bytes 147464 | tf_op jit(solution)/shard_map/ppermute | solution.py:414
  54.7 1.4 %collective-permute-start.7 = (bf16[64,384]{1,0:T(8,128)(2,1)S(1)}, bf16[64,384]{1,0:T(8,128)(2,1)S(1)}, u32[]{:S(2)}, u32[]{:S(2)}) collective-permute-start(bf16[64,384]{1,0:T(8,128)(2,1)S(1)} %get-tuple-element.64), channel_id=1, source_target_pairs={{0,3},{1,0},{2,1},{3,2},{4,7},{5,4},{6,5},{7,6},{8,11},{9,8},{10,9... | collective-permute-start | bytes 147464 | tf_op jit(solution)/shard_map/ppermute | solution.py:414
  56.2 0.0 collective-permute-done.5.from_1
  56.2 1.4 %collective-permute-done.6.from_2 = bf16[64,384]{1,0:T(8,128)(2,1)S(1)} collective-permute-done((bf16[64,384]{1,0:T(8,128)(2,1)S(1)}, bf16[64,384]{1,0:T(8,128)(2,1)S(1)}, u32[]{:S(2)}, u32[]{:S(2)}) %collective-permute-start.6) | collective-permute-done | bytes 49184 | tf_op jit(solution)/shard_map/ppermute | solution.py:414
  57.6 1.2 %collective-permute-done.7.from_3 = bf16[64,384]{1,0:T(8,128)(2,1)S(1)} collective-permute-done((bf16[64,384]{1,0:T(8,128)(2,1)S(1)}, bf16[64,384]{1,0:T(8,128)(2,1)S(1)}, u32[]{:S(2)}, u32[]{:S(2)}) %collective-permute-start.7) | collective-permute-done | bytes 49184 | tf_op jit(solution)/shard_map/ppermute | solution.py:414
  58.8 0.0 copy-done
  58.8 1.9 %project.1 = bf16[64,2048]{1,0:T(8,128)(2,1)} custom-call(bf16[64,384]{1,0:T(8,128)(2,1)S(1)} %get-tuple-element.61.own, bf16[64,384]{1,0:T(8,128)(2,1)S(1)} %collective-permute-done.5.from_1, bf16[64,384]{1,0:T(8,128)(2,1)S(1)} %collective-permute-done.6.from_2, bf16[64,384]{1,0:T(8,128)(2,1)S(1)} %collective-permute-done.7.from_3, ...), custom_call_target="tpu_custom_call" | custom-call | tf_op jit(solution)/shard_map/project/pallas_call | solution.py:427
  (17 shorter events, 0.0 us)
Async XLA Ops:
  0.0 1.2 %copy-start.2 = (bf16[256,2048]{1,0:T(8,128)(2,1)S(1)}, bf16[256,2048]{1,0:T(8,128)(2,1)}, u32[]{:S(2)}) copy-start(bf16[256,2048]{1,0:T(8,128)(2,1)} %refs_0_.1) | copy-start | bytes 3145732
  1.2 1.2 %copy-start.3 = (bf16[2048,256]{1,0:T(8,128)(2,1)S(1)}, bf16[2048,256]{1,0:T(8,128)(2,1)}, u32[]{:S(2)}) copy-start(bf16[2048,256]{1,0:T(8,128)(2,1)} %refs_6_.1) | copy-start | bytes 3145732
  2.5 1.2 %copy-start.4 = (bf16[2048,256]{1,0:T(8,128)(2,1)S(1)}, bf16[2048,256]{1,0:T(8,128)(2,1)}, u32[]{:S(2)}) copy-start(bf16[2048,256]{1,0:T(8,128)(2,1)} %refs_7_.1) | copy-start | bytes 3145732
  3.7 1.2 %copy-start.5 = (bf16[2048,256]{1,0:T(8,128)(2,1)S(1)}, bf16[2048,256]{1,0:T(8,128)(2,1)}, u32[]{:S(2)}) copy-start(bf16[2048,256]{1,0:T(8,128)(2,1)} %refs_8_.1) | copy-start | bytes 3145732
  4.9 1.2 %copy-start.6 = (bf16[2048,256]{1,0:T(8,128)(2,1)S(1)}, bf16[2048,256]{1,0:T(8,128)(2,1)}, u32[]{:S(2)}) copy-start(bf16[2048,256]{1,0:T(8,128)(2,1)} %refs_9_.1) | copy-start | bytes 3145732
  6.1 1.0 %copy-start.9 = (bf16[2048,128]{1,0:T(8,128)(2,1)S(1)}, bf16[2048,128]{1,0:T(8,128)(2,1)}, u32[]{:S(2)}) copy-start(bf16[2048,128]{1,0:T(8,128)(2,1)} %refs_10_.1) | copy-start | bytes 1572868
  7.2 1.0 %copy-start.10 = (bf16[2048,128]{1,0:T(8,128)(2,1)S(1)}, bf16[2048,128]{1,0:T(8,128)(2,1)}, u32[]{:S(2)}) copy-start(bf16[2048,128]{1,0:T(8,128)(2,1)} %refs_11_.1) | copy-start | bytes 1572868
  8.2 0.9 %copy-start.11 = (f32[256,256]{1,0:T(8,128)S(1)}, f32[256,256]{1,0:T(8,128)}, u32[]{:S(2)}) copy-start(f32[256,256]{1,0:T(8,128)} %refs_4_.1) | copy-start | bytes 786436
  9.2 0.9 %copy-start.12 = (f32[256,256]{1,0:T(8,128)S(1)}, f32[256,256]{1,0:T(8,128)}, u32[]{:S(2)}) copy-start(f32[256,256]{1,0:T(8,128)} %refs_5_.1) | copy-start | bytes 786436
  10.1 0.7 %copy-start.14 = (f32[2048]{0:T(1024)S(1)}, f32[2048]{0:T(1024)}, u32[]{:S(2)}) copy-start(f32[2048]{0:T(1024)} %param.21) | copy-start | bytes 24580
  10.8 0.7 %copy-start.17 = (f32[256]{0:T(256)S(1)}, f32[256]{0:T(256)}, u32[]{:S(2)}) copy-start(f32[256]{0:T(256)} %param.33) | copy-start | bytes 3076
  11.5 0.7 %copy-start.18 = (f32[256]{0:T(256)S(1)}, f32[256]{0:T(256)}, u32[]{:S(2)}) copy-start(f32[256]{0:T(256)} %param.34) | copy-start | bytes 3076
  12.2 34.8 %copy-start.13 = (f32[31,128]{1,0:T(8,128)S(1)}, f32[31,128]{1,0:T(8,128)}, u32[]{:S(2)}) copy-start(f32[31,128]{1,0:T(8,128)} %taps.3) | copy-start | bytes 47620
  12.2 34.8 %copy-start.15 = (f32[128]{0:T(128)S(1)}, f32[128]{0:T(128)}, u32[]{:S(2)}) copy-start(f32[128]{0:T(128)} %param.25) | copy-start | bytes 1540
  12.2 34.8 %copy-start.16 = (f32[128]{0:T(128)S(1)}, f32[128]{0:T(128)}, u32[]{:S(2)}) copy-start(f32[128]{0:T(128)} %param.26) | copy-start | bytes 1540
  12.2 35.4 %copy-start.7 = (bf16[2048,256]{1,0:T(8,128)(2,1)S(1)}, bf16[2048,256]{1,0:T(8,128)(2,1)}, u32[]{:S(2)}) copy-start(bf16[2048,256]{1,0:T(8,128)(2,1)} %w_receptance.1) | copy-start | bytes 3145732
  12.2 35.4 %copy-start.8 = (bf16[2048,256]{1,0:T(8,128)(2,1)S(1)}, bf16[2048,256]{1,0:T(8,128)(2,1)}, u32[]{:S(2)}) copy-start(bf16[2048,256]{1,0:T(8,128)(2,1)} %w_gate.1) | copy-start | bytes 3145732
  24.9 24.6 %copy-start.19 = (f32[256]{0:T(256)S(1)}, f32[256]{0:T(256)}, u32[]{:S(2)}) copy-start(f32[256]{0:T(256)} %param.37) | copy-start | bytes 3076
  24.9 33.9 %copy-start = (bf16[1024,2048]{1,0:T(8,128)(2,1)S(1)}, bf16[1024,2048]{1,0:T(8,128)(2,1)}, u32[]{:S(2)}) copy-start(bf16[1024,2048]{1,0:T(8,128)(2,1)} %mix_w.1) | copy-start | bytes 12582916
  24.9 33.9 %copy-start.1 = (bf16[512,2048]{1,0:T(8,128)(2,1)S(1)}, bf16[512,2048]{1,0:T(8,128)(2,1)}, u32[]{:S(2)}) copy-start(bf16[512,2048]{1,0:T(8,128)(2,1)} %conv_w.1) | copy-start | bytes 6291460
  24.9 1.5 %collective-permute-start = (f32[144,256]{1,0:T(8,128)S(1)}, f32[144,256]{1,0:T(8,128)S(1)}, u32[]{:S(2)}, u32[]{:S(2)}) collective-permute-start(f32[144,256]{1,0:T(8,128)S(1)} %get-tuple-element.35.mine), channel_id=1, source_target_pairs={{0,4},{4,0},{1,5},{5,1},{2,6},{6,2},{3,7},{7,3},{8,12},{12,8},{9,1... | collective-permute-start | bytes 442376 | tf_op jit(solution)/shard_map/ppermute | solution.py:419
  26.6 4.4 %collective-permute-start.1 = (bf16[144,256]{1,0:T(8,128)(2,1)S(1)}, bf16[144,256]{1,0:T(8,128)(2,1)S(1)}, u32[]{:S(2)}, u32[]{:S(2)}) collective-permute-start(bf16[144,256]{1,0:T(8,128)(2,1)S(1)} %get-tuple-element.36.mine), channel_id=1, source_target_pairs={{0,8},{8,0},{16,24},{24,16},{1,9},{9,1},{17,25},{25,17},{2,10},{10... | collective-permute-start | bytes 221192 | tf_op jit(solution)/shard_map/ppermute | solution.py:419
  31.4 5.6 %collective-permute-start.2 = (bf16[144,256]{1,0:T(8,128)(2,1)S(1)}, bf16[144,256]{1,0:T(8,128)(2,1)S(1)}, u32[]{:S(2)}, u32[]{:S(2)}) collective-permute-start(bf16[144,256]{1,0:T(8,128)(2,1)S(1)} %get-tuple-element.39.mine), channel_id=1, source_target_pairs={{0,24},{8,16},{16,8},{24,0},{1,25},{9,17},{17,9},{25,1},{2,26},{10... | collective-permute-start | bytes 221192 | tf_op jit(solution)/shard_map/ppermute | solution.py:419
  37.4 4.4 %collective-permute-start.3 = (bf16[144,256]{1,0:T(8,128)(2,1)S(1)}, bf16[144,256]{1,0:T(8,128)(2,1)S(1)}, u32[]{:S(2)}, u32[]{:S(2)}) collective-permute-start(bf16[144,256]{1,0:T(8,128)(2,1)S(1)} %get-tuple-element.42.mine), channel_id=1, source_target_pairs={{0,32},{32,0},{64,96},{96,64},{1,33},{33,1},{65,97},{97,65},{2,34}... | collective-permute-start | bytes 221192 | tf_op jit(solution)/shard_map/ppermute | solution.py:419
  42.8 6.7 %collective-permute-start.4 = (bf16[80,256]{1,0:T(8,128)(2,1)S(1)}, bf16[80,256]{1,0:T(8,128)(2,1)S(1)}, u32[]{:S(2)}, u32[]{:S(2)}) collective-permute-start(bf16[80,256]{1,0:T(8,128)(2,1)S(1)} %get-tuple-element.45), channel_id=1, source_target_pairs={{0,96},{32,64},{64,32},{96,0},{1,97},{33,65},{65,33},{97,1},{2,98}... | collective-permute-start | bytes 122888 | tf_op jit(solution)/shard_map/ppermute | solution.py:419
  50.4 5.7 %collective-permute-start.5 = (bf16[64,384]{1,0:T(8,128)(2,1)S(1)}, bf16[64,384]{1,0:T(8,128)(2,1)S(1)}, u32[]{:S(2)}, u32[]{:S(2)}) collective-permute-start(bf16[64,384]{1,0:T(8,128)(2,1)S(1)} %get-tuple-element.62), channel_id=1, source_target_pairs={{0,1},{1,2},{2,3},{3,0},{4,5},{5,6},{6,7},{7,4},{8,9},{9,10},{10,1... | collective-permute-start | bytes 147464 | tf_op jit(solution)/shard_map/ppermute | solution.py:414
  52.0 5.6 %collective-permute-start.6 = (bf16[64,384]{1,0:T(8,128)(2,1)S(1)}, bf16[64,384]{1,0:T(8,128)(2,1)S(1)}, u32[]{:S(2)}, u32[]{:S(2)}) collective-permute-start(bf16[64,384]{1,0:T(8,128)(2,1)S(1)} %get-tuple-element.63), channel_id=1, source_target_pairs={{0,2},{1,3},{2,0},{3,1},{4,6},{5,7},{6,4},{7,5},{8,10},{9,11},{10,... | collective-permute-start | bytes 147464 | tf_op jit(solution)/shard_map/ppermute | solution.py:414
  54.7 4.1 %collective-permute-start.7 = (bf16[64,384]{1,0:T(8,128)(2,1)S(1)}, bf16[64,384]{1,0:T(8,128)(2,1)S(1)}, u32[]{:S(2)}, u32[]{:S(2)}) collective-permute-start(bf16[64,384]{1,0:T(8,128)(2,1)S(1)} %get-tuple-element.64), channel_id=1, source_target_pairs={{0,3},{1,0},{2,1},{3,2},{4,7},{5,4},{6,5},{7,6},{8,11},{9,8},{10,9... | collective-permute-start | bytes 147464 | tf_op jit(solution)/shard_map/ppermute | solution.py:414

commit v3 on v2

--- a/solution.py
+++ b/solution.py
@@ -33,6 +33,7 @@
 TN = (((0,), (0,)), ((), ()))
 VMEM = pl.BlockSpec(memory_space=pltpu.VMEM)
 HBM = pl.BlockSpec(memory_space=pltpu.HBM)
+ANY = pl.BlockSpec(memory_space=pl.ANY)
 
 
 def mm(left, right, dims=NN):
@@ -241,10 +242,13 @@
     return rounded(jnp.dot(left, right, preferred_element_type=F32))
 
 
+def gate_kernel(normed, w_receptance, w_gate, receptance_out, gate_out):
+    receptance_out[...] = rounded_product(normed[...], w_receptance[...])
+    gate_out[...] = jax.nn.sigmoid(rounded_product(normed[...], w_gate[...]))
+
+
 def read_kernel(
-    normed,
-    w_receptance,
-    w_gate,
+    receptance,
     fall,
     start,
     erase,
@@ -254,14 +258,11 @@
     priors,
     local_out,
     query_out,
-    gate_out,
 ):
     square = (ROWS, LANES)
     row_at, lane_at = iota(square, 0), iota(square, 1)
     low_half = iota((ROWS, 128), 1) < HEAD
-    receptance = rounded_product(normed[...], w_receptance[...])
-    gate_out[...] = jax.nn.sigmoid(rounded_product(normed[...], w_gate[...]))
-    read_s = receptance * fall[...]
+    read_s = receptance[...] * fall[...]
     read_q = read_s * per_chunk([start[c : c + 1] for c in range(CHUNKS)])
     inclusive = (row_at // SPAN == lane_at // SPAN) & (lane_at <= row_at)
     found = []
@@ -313,7 +314,7 @@
     return follow(lower[: 2 * HEAD], upper[:HEAD], upper[HEAD : 2 * HEAD])
 
 
-def core_kernel(mine, other, pack_out, total_out, prefix_out):
+def core_kernel(mine, other, pack_out, prefix_out, total_out):
     first = lax.axis_index("c") == 0
     early = jnp.where(first, mine[...], other[...])
     late = jnp.where(first, other[...], mine[...])
@@ -325,7 +326,7 @@
     prefix_out[2 * HEAD :] = jnp.where(first, 0.0, early[2 * HEAD :])
 
 
-def pair_kernel(axis, far, sent, mine, total, other, prefix, pack_out, total_out, prefix_out):
+def pair_kernel(axis, far, sent, mine, total, other, prefix, _, pack_out, prefix_out, *total_out):
     at = lax.axis_index(axis)
     upper = (at >= 2) if far else (lax.rem(at, 2) == 1)
     got = other[...].astype(F32)
@@ -333,7 +334,8 @@
     early = jnp.where(upper, states, total[...])
     late = jnp.where(upper, total[...], states)
     result = joined(early, late)
-    total_out[...] = result
+    for out in total_out:
+        out[...] = result
     pack_out[: HEAD * sent] = result[HEAD * (2 - sent) :].astype(BF16)
     tail = other if far else mine
     pack_out[HEAD * sent :] = tail[2 * HEAD :]
@@ -391,21 +393,14 @@
         out[...] = ready[pl.ds(pl.multiple_of(to * SPAN, SPAN), SPAN)]
 
 
-def project_kernel(own, from_1, from_2, from_3, conv_w, mix_w, out):
+def project_kernel(own, from_1, from_2, from_3, conv_w, mix_w, out, conv_rows, mix_rows):
     x = lax.axis_index("x")
-    total = jnp.zeros((SPAN, 2048), F32)
     for n, ref in enumerate((own, from_1, from_2, from_3)):
         of = lax.rem(x - n + 4, 4)
-        total = total + jnp.dot(
-            ref[:, :CONV],
-            conv_w[pl.ds(pl.multiple_of(of * CONV, CONV), CONV)],
-            preferred_element_type=F32,
-        )
-        total = total + jnp.dot(
-            ref[:, CONV:],
-            mix_w[pl.ds(pl.multiple_of(of * LANES, LANES), LANES)],
-            preferred_element_type=F32,
-        )
+        conv_rows[:, pl.ds(pl.multiple_of(of * CONV, CONV), CONV)] = ref[:, :CONV]
+        mix_rows[:, pl.ds(pl.multiple_of(of * LANES, LANES), LANES)] = ref[:, CONV:]
+    total = jnp.dot(conv_rows[...], conv_w[...], preferred_element_type=F32)
+    total = total + jnp.dot(mix_rows[...], mix_w[...], preferred_element_type=F32)
     out[...] = total.astype(BF16)
 
 
@@ -423,7 +418,9 @@
     return pltpu.CompilerParams(vmem_limit_bytes=40 * 1024 * 1024)
 
 
-def call(kernel, name, outs, arguments, specs=None, scratch=()):
+def call(kernel, name, outs, arguments, specs=None, scratch=(), pinned=False):
+    if pinned:
+        arguments = [pltpu.with_memory_space_constraint(a, pltpu.HBM) for a in arguments]
     return pl.pallas_call(
         kernel,
         name=name,
@@ -499,6 +496,7 @@
             convolution_gate_weight,
         ),
         specs=[HBM] * 12,
+        pinned=True,
         scratch=[pltpu.VMEM((ROWS, 2048), BF16), pltpu.VMEM((1, 2048), F32), row, row]
         + [pltpu.VMEM((ROWS, LANES), F32)] * 2
         + [wide] * 4
@@ -506,23 +504,18 @@
         + [pltpu.SemaphoreType.DMA((12,))],
     )
     other = swapped(pack, "c", 1)
-    pack, total, prefix = call(core_kernel, "core", [packed_b, state, packed], (pack, other))
-    local_read, query, gate = call(
+    pack, prefix, *total = call(core_kernel, "core", [packed_b, packed, state], (pack, other))
+    receptance, gate = call(
+        gate_kernel,
+        "gate",
+        [square, square],
+        (normed, receptance_weight, output_gate_weight),
+    )
+    local_read, query = call(
         read_kernel,
         "read",
-        [square, square_b, square],
-        (
-            normed,
-            receptance_weight,
-            output_gate_weight,
-            fall,
-            start,
-            erase,
-            key,
-            value_swapped,
-            solved,
-            priors,
-        ),
+        [square, square_b],
+        (receptance, fall, start, erase, key, value_swapped, solved, priors),
     )
     conv_done, conv_part = call(
         conv_kernel,
@@ -531,14 +524,16 @@
         (conv_input, depthwise_taps_weight, conv_gain, conv_shift),
         scratch=[pltpu.VMEM((HALO + ROWS, CONV), F32)],
     )
-    for axis, far in (("y", False), ("y", True), ("z", False)):
+    beside = (conv_done, receptance, local_read)
+    for (axis, far), side in zip((("y", False), ("y", True), ("z", False)), beside):
         other = swapped(pack, axis, 3 if far else 1)
         sent = 1 if axis == "z" else 2
-        pack, total, prefix = call(
+        pack, prefix, *total = call(
             functools.partial(pair_kernel, axis, far, sent),
             f"pair_{axis}{3 if far else 1}",
-            [((HEAD * sent + HALO // 2, LANES), BF16), state, packed],
-            (pack, total, other, prefix),
+            [((HEAD * sent + HALO // 2, LANES), BF16), packed] + [state] * (sent - 1),
+            (pack, total[0], other, prefix, side),
+            specs=[VMEM] * 4 + [ANY],
         )
     other = swapped(pack, "z", 3)
     sends = call(
@@ -569,6 +564,7 @@
         "project",
         [((SPAN, 2048), BF16)],
         (sends[0], *arrived, convolution_output_weight, attention_output_weight),
+        scratch=[pltpu.VMEM((SPAN, 512), BF16), pltpu.VMEM((SPAN, 1024), BF16)],
     )
     return mixed
 

time: 61.3 us -> 48.6 us (0.79)
  local copies, waits for them, and re-layouts: 12.2 us -> 0.04 us
  waiting for transfers between devices: 11.4 us -> 10.7 us
    unnamed x40 -> x16, local copies, waits for them, and re-layouts: 12.2 us -> 0.04 us
    ppermute x5, waiting for transfers between devices: 8.8 us -> 8.07 us  [swapped(): return lax.ppermute(value, axis, [(s, s ^ bits) for s in range(count)])]
    pallas_call x9 -> x10, Pallas kernels: 19.9 us -> 20.3 us  [call(): pl.pallas_call(kernel, name=name, out_shape=[jax.ShapeDtypeStruct(*o) for...]
  transfers between devices with their start and end apart: 8 -> 8, of which waited for: 6 -> 7; matrix products, arithmetic and copies ran while one was open for 0% -> 0% of each run, Pallas kernels for 4% -> 5%
where the time goes in v3:
time: 48.6 us; the launch traced here: 48.5 us
  Pallas kernels  20.3 us (42%)
  starting transfers between devices  17.3 us (36%)
  waiting for transfers between devices  10.7 us (22%)
    pallas_call x10, Pallas kernels, call(): pl.pallas_call(kernel, name=name, out_shape=[jax.ShapeDtypeStruct(*o) for...  20.3 us
    ppermute x5, starting transfers between devices, swapped(): return lax.ppermute(value, axis, [(s, s ^ bits) for s in range(count)])  11.6 us
    ppermute x5, waiting for transfers between devices, swapped(): return lax.ppermute(value, axis, [(s, s ^ bits) for s in range(count)])  8.07 us
    ppermute x3, starting transfers between devices, shifted(): lax.ppermute(value, axis, [(s, (s + steps) % count) for s in range(count)])  5.73 us
    ppermute x3, waiting for transfers between devices, shifted(): lax.ppermute(value, axis, [(s, (s + steps) % count) for s in range(count)])  2.65 us
  transfers between devices with their start and end apart: 8, of which 7 were waited for; matrix products, arithmetic and copies ran while one was open for 0% of the time, Pallas kernels for 5%

profile of v3, /device:TPU:0, one launch (start us, length us, event | category | flops | bytes accessed | tf_op | source)
XLA Modules:
  0.0 48.5 jit_solution(5086604334865963916)
XLA Ops:
  0.0 0.0 copy-start.4
  0.0 0.0 copy-start.6
  0.0 0.0 copy-start.5
  0.0 0.0 copy-start.3
  0.0 0.0 copy-start.2
  0.0 13.6 %local.1 = (f32[144,256]{1,0:T(8,128)S(1)}, f32[4,128,256]{2,1,0:T(8,128)S(1)}, f32[256,128]{1,0:T(8,128)S(1)}, bf16[256,2048]{1,0:T(8,128)(2,1)S(1)}, f32[256,2...) custom-call(bf16[256,2048]{1,0:T(8,128)(2,1)} %refs_0_.1, ...), custom_call_target="tpu_custom_call" | custom-call | tf_op jit(solution)/shard_map/local/pallas_call | solution.py:424
  13.6 0.0 copy-start.7
  13.7 0.0 copy-start
  13.7 0.0 copy-start.1
  13.7 0.1 collective-permute-start
  13.8 1.4 %collective-permute-done.other = f32[144,256]{1,0:T(8,128)S(1)} collective-permute-done((f32[144,256]{1,0:T(8,128)S(1)}, f32[144,256]{1,0:T(8,128)S(1)}, u32[]{:S(2)}, u32[]{:S(2)}) %collective-permute-start) | collective-permute-done | bytes 147488 | tf_op jit(solution)/shard_map/ppermute | solution.py:414
  15.1 0.3 core.1
  15.4 1.8 %collective-permute-start.1 = (bf16[144,256]{1,0:T(8,128)(2,1)S(1)}, bf16[144,256]{1,0:T(8,128)(2,1)S(1)}, u32[]{:S(2)}, u32[]{:S(2)}) collective-permute-start(bf16[144,256]{1,0:T(8,128)(2,1)S(1)} %get-tuple-element.37.mine), channel_id=1, source_target_pairs={{0,8},{8,0},{16,24},{24,16},{1,9},{9,1},{17,25},{25,17},{2,10},{10... | collective-permute-start | bytes 221192 | tf_op jit(solution)/shard_map/ppermute | solution.py:414
  17.2 0.0 copy-done.4
  17.2 0.0 copy-done.6
  17.2 0.0 copy-done.5
  17.2 0.6 %conv.1 = (bf16[256,128]{1,0:T(8,128)(2,1)S(1)}, f32[32,128]{1,0:T(8,128)S(1)}) custom-call(f32[256,128]{1,0:T(8,128)S(1)} %get-tuple-element.40.conv_in, f32[31,128]{1,0:T(8,128)S(1)} %copy-done.4, f32[1,128]{1,0:T(1,128)S(1)} %bitcast.6, f32[1,128]{1,0:T(1,128)S(1)} %bitcast.8), custom_call_target="tpu_custom_call" | custom-call | tf_op jit(solution)/shard_map/conv/pallas_call | solution.py:424
  17.8 2.0 %collective-permute-done.1.other = bf16[144,256]{1,0:T(8,128)(2,1)S(1)} collective-permute-done((bf16[144,256]{1,0:T(8,128)(2,1)S(1)}, bf16[144,256]{1,0:T(8,128)(2,1)S(1)}, u32[]{:S(2)}, u32[]{:S(2)}) %collective-permute-start.1) | collective-permute-done | bytes 73760 | tf_op jit(solution)/shard_map/ppermute | solution.py:414
  19.8 0.3 pair_y1.1
  20.1 3.2 %collective-permute-start.2 = (bf16[144,256]{1,0:T(8,128)(2,1)S(1)}, bf16[144,256]{1,0:T(8,128)(2,1)S(1)}, u32[]{:S(2)}, u32[]{:S(2)}) collective-permute-start(bf16[144,256]{1,0:T(8,128)(2,1)S(1)} %get-tuple-element.42.mine), channel_id=1, source_target_pairs={{0,24},{8,16},{16,8},{24,0},{1,25},{9,17},{17,9},{25,1},{2,26},{10... | collective-permute-start | bytes 221192 | tf_op jit(solution)/shard_map/ppermute | solution.py:414
  23.4 0.0 copy-done.3
  23.4 0.0 copy-done.2
  23.4 0.7 %gate.1 = (f32[256,256]{1,0:T(8,128)S(1)}, f32[256,256]{1,0:T(8,128)S(1)}) custom-call(bf16[256,2048]{1,0:T(8,128)(2,1)S(1)} %get-tuple-element.45.normed, bf16[2048,256]{1,0:T(8,128)(2,1)S(1)} %copy-done.2, bf16[2048,256]{1,0:T(8,128)(2,1)S(1)} %copy-done.3), custom_call_target="tpu_custom_call" | custom-call | tf_op jit(solution)/shard_map/gate/pallas_call | solution.py:424
  24.1 1.7 %collective-permute-done.2.other = bf16[144,256]{1,0:T(8,128)(2,1)S(1)} collective-permute-done((bf16[144,256]{1,0:T(8,128)(2,1)S(1)}, bf16[144,256]{1,0:T(8,128)(2,1)S(1)}, u32[]{:S(2)}, u32[]{:S(2)}) %collective-permute-start.2) | collective-permute-done | bytes 73760 | tf_op jit(solution)/shard_map/ppermute | solution.py:414
  25.8 0.3 pair_y3.1
  26.1 2.1 %collective-permute-start.3 = (bf16[144,256]{1,0:T(8,128)(2,1)S(1)}, bf16[144,256]{1,0:T(8,128)(2,1)S(1)}, u32[]{:S(2)}, u32[]{:S(2)}) collective-permute-start(bf16[144,256]{1,0:T(8,128)(2,1)S(1)} %get-tuple-element.47.mine), channel_id=1, source_target_pairs={{0,32},{32,0},{64,96},{96,64},{1,33},{33,1},{65,97},{97,65},{2,34}... | collective-permute-start | bytes 221192 | tf_op jit(solution)/shard_map/ppermute | solution.py:414
  28.2 1.3 %read.1 = (f32[256,256]{1,0:T(8,128)S(1)}, bf16[256,256]{1,0:T(8,128)(2,1)S(1)}) custom-call(f32[256,256]{1,0:T(8,128)S(1)} %get-tuple-element.46._.receptance, f32[256,256]{1,0:T(8,128)S(1)} %get-tuple-element.50.fall, f32[8,256]{1,0:T(8,128)S(1)} %get-tuple-element.51.start, bf16[256,256]{1,0:T(8,128)(2,1)S(1)} %get-tuple-element.52.erase, ...), custom_call_target="tpu_custom_call" | custom-call | tf_op jit(solution)/shard_map/read/pallas_call | solution.py:424
  29.5 1.0 %collective-permute-done.3.other = bf16[144,256]{1,0:T(8,128)(2,1)S(1)} collective-permute-done((bf16[144,256]{1,0:T(8,128)(2,1)S(1)}, bf16[144,256]{1,0:T(8,128)(2,1)S(1)}, u32[]{:S(2)}, u32[]{:S(2)}) %collective-permute-start.3) | collective-permute-done | bytes 73760 | tf_op jit(solution)/shard_map/ppermute | solution.py:414
  30.6 0.3 pair_z1.1
  30.9 4.4 %collective-permute-start.4 = (bf16[80,256]{1,0:T(8,128)(2,1)S(1)}, bf16[80,256]{1,0:T(8,128)(2,1)S(1)}, u32[]{:S(2)}, u32[]{:S(2)}) collective-permute-start(bf16[80,256]{1,0:T(8,128)(2,1)S(1)} %get-tuple-element.58), channel_id=1, source_target_pairs={{0,96},{32,64},{64,32},{96,0},{1,97},{33,65},{65,33},{97,1},{2,98}... | collective-permute-start | bytes 122888 | tf_op jit(solution)/shard_map/ppermute | solution.py:414
  35.3 2.0 %collective-permute-done.4.other = bf16[80,256]{1,0:T(8,128)(2,1)S(1)} collective-permute-done((bf16[80,256]{1,0:T(8,128)(2,1)S(1)}, bf16[80,256]{1,0:T(8,128)(2,1)S(1)}, u32[]{:S(2)}, u32[]{:S(2)}) %collective-permute-start.4) | collective-permute-done | bytes 40992 | tf_op jit(solution)/shard_map/ppermute | solution.py:414
  37.3 0.0 copy-done.7
  37.3 0.9 %last.1 = (bf16[64,384]{1,0:T(8,128)(2,1)S(1)}, bf16[64,384]{1,0:T(8,128)(2,1)S(1)}, bf16[64,384]{1,0:T(8,128)(2,1)S(1)}, bf16[64,384]{1,0:T(8,128)(2,1)S(1)}) custom-call(bf16[80,256]{1,0:T(8,128)(2,1)S(1)} %collective-permute-done.4.other, f32[144,256]{1,0:T(8,128)S(1)} %get-tuple-element.59.prefix, f32[256,256]{1,0:T(8,128)S(1)} %get-tuple-element.57._.local, ...), custom_call_target="tpu_custom_call" | custom-call | tf_op jit(solution)/shard_map/last/pallas_call | solution.py:424
  38.2 1.6 %collective-permute-start.5 = (bf16[64,384]{1,0:T(8,128)(2,1)S(1)}, bf16[64,384]{1,0:T(8,128)(2,1)S(1)}, u32[]{:S(2)}, u32[]{:S(2)}) collective-permute-start(bf16[64,384]{1,0:T(8,128)(2,1)S(1)} %get-tuple-element.64), channel_id=1, source_target_pairs={{0,1},{1,2},{2,3},{3,0},{4,5},{5,6},{6,7},{7,4},{8,9},{9,10},{10,1... | collective-permute-start | bytes 147464 | tf_op jit(solution)/shard_map/ppermute | solution.py:409
  39.8 2.7 %collective-permute-start.6 = (bf16[64,384]{1,0:T(8,128)(2,1)S(1)}, bf16[64,384]{1,0:T(8,128)(2,1)S(1)}, u32[]{:S(2)}, u32[]{:S(2)}) collective-permute-start(bf16[64,384]{1,0:T(8,128)(2,1)S(1)} %get-tuple-element.65), channel_id=1, source_target_pairs={{0,2},{1,3},{2,0},{3,1},{4,6},{5,7},{6,4},{7,5},{8,10},{9,11},{10,... | collective-permute-start | bytes 147464 | tf_op jit(solution)/shard_map/ppermute | solution.py:409
  42.5 1.4 %collective-permute-start.7 = (bf16[64,384]{1,0:T(8,128)(2,1)S(1)}, bf16[64,384]{1,0:T(8,128)(2,1)S(1)}, u32[]{:S(2)}, u32[]{:S(2)}) collective-permute-start(bf16[64,384]{1,0:T(8,128)(2,1)S(1)} %get-tuple-element.66), channel_id=1, source_target_pairs={{0,3},{1,0},{2,1},{3,2},{4,7},{5,4},{6,5},{7,6},{8,11},{9,8},{10,9... | collective-permute-start | bytes 147464 | tf_op jit(solution)/shard_map/ppermute | solution.py:409
  43.9 0.0 collective-permute-done.5.from_1
  44.0 1.4 %collective-permute-done.6.from_2 = bf16[64,384]{1,0:T(8,128)(2,1)S(1)} collective-permute-done((bf16[64,384]{1,0:T(8,128)(2,1)S(1)}, bf16[64,384]{1,0:T(8,128)(2,1)S(1)}, u32[]{:S(2)}, u32[]{:S(2)}) %collective-permute-start.6) | collective-permute-done | bytes 49184 | tf_op jit(solution)/shard_map/ppermute | solution.py:409
  45.4 1.2 %collective-permute-done.7.from_3 = bf16[64,384]{1,0:T(8,128)(2,1)S(1)} collective-permute-done((bf16[64,384]{1,0:T(8,128)(2,1)S(1)}, bf16[64,384]{1,0:T(8,128)(2,1)S(1)}, u32[]{:S(2)}, u32[]{:S(2)}) %collective-permute-start.7) | collective-permute-done | bytes 49184 | tf_op jit(solution)/shard_map/ppermute | solution.py:409
  46.6 0.0 copy-done
  46.6 0.0 copy-done.1
  46.6 1.9 %project.1 = bf16[64,2048]{1,0:T(8,128)(2,1)} custom-call(bf16[64,384]{1,0:T(8,128)(2,1)S(1)} %get-tuple-element.63.own, bf16[64,384]{1,0:T(8,128)(2,1)S(1)} %collective-permute-done.5.from_1, bf16[64,384]{1,0:T(8,128)(2,1)S(1)} %collective-permute-done.6.from_2, bf16[64,384]{1,0:T(8,128)(2,1)S(1)} %collective-permute-done.7.from_3, ...), custom_call_target="tpu_custom_call" | custom-call | tf_op jit(solution)/shard_map/project/pallas_call | solution.py:424
Async XLA Ops:
  0.0 17.2 %copy-start.4 = (f32[31,128]{1,0:T(8,128)S(1)}, f32[31,128]{1,0:T(8,128)}, u32[]{:S(2)}) copy-start(f32[31,128]{1,0:T(8,128)} %taps.3) | copy-start | bytes 47620
  0.0 17.2 %copy-start.6 = (f32[128]{0:T(128)S(1)}, f32[128]{0:T(128)}, u32[]{:S(2)}) copy-start(f32[128]{0:T(128)} %param.26) | copy-start | bytes 1540
  0.0 17.2 %copy-start.5 = (f32[128]{0:T(128)S(1)}, f32[128]{0:T(128)}, u32[]{:S(2)}) copy-start(f32[128]{0:T(128)} %param.25) | copy-start | bytes 1540
  0.0 23.4 %copy-start.3 = (bf16[2048,256]{1,0:T(8,128)(2,1)S(1)}, bf16[2048,256]{1,0:T(8,128)(2,1)}, u32[]{:S(2)}) copy-start(bf16[2048,256]{1,0:T(8,128)(2,1)} %w_gate.1) | copy-start | bytes 3145732
  0.0 23.4 %copy-start.2 = (bf16[2048,256]{1,0:T(8,128)(2,1)S(1)}, bf16[2048,256]{1,0:T(8,128)(2,1)}, u32[]{:S(2)}) copy-start(bf16[2048,256]{1,0:T(8,128)(2,1)} %w_receptance.1) | copy-start | bytes 3145732
  13.6 23.6 %copy-start.7 = (f32[256]{0:T(256)S(1)}, f32[256]{0:T(256)}, u32[]{:S(2)}) copy-start(f32[256]{0:T(256)} %param.37) | copy-start | bytes 3076
  13.7 33.0 %copy-start = (bf16[1024,2048]{1,0:T(8,128)(2,1)S(1)}, bf16[1024,2048]{1,0:T(8,128)(2,1)}, u32[]{:S(2)}) copy-start(bf16[1024,2048]{1,0:T(8,128)(2,1)} %mix_w.1) | copy-start | bytes 12582916
  13.7 32.9 %copy-start.1 = (bf16[512,2048]{1,0:T(8,128)(2,1)S(1)}, bf16[512,2048]{1,0:T(8,128)(2,1)}, u32[]{:S(2)}) copy-start(bf16[512,2048]{1,0:T(8,128)(2,1)} %conv_w.1) | copy-start | bytes 6291460
  13.7 1.5 %collective-permute-start = (f32[144,256]{1,0:T(8,128)S(1)}, f32[144,256]{1,0:T(8,128)S(1)}, u32[]{:S(2)}, u32[]{:S(2)}) collective-permute-start(f32[144,256]{1,0:T(8,128)S(1)} %get-tuple-element.36.mine), channel_id=1, source_target_pairs={{0,4},{4,0},{1,5},{5,1},{2,6},{6,2},{3,7},{7,3},{8,12},{12,8},{9,1... | collective-permute-start | bytes 442376 | tf_op jit(solution)/shard_map/ppermute | solution.py:414
  15.4 4.4 %collective-permute-start.1 = (bf16[144,256]{1,0:T(8,128)(2,1)S(1)}, bf16[144,256]{1,0:T(8,128)(2,1)S(1)}, u32[]{:S(2)}, u32[]{:S(2)}) collective-permute-start(bf16[144,256]{1,0:T(8,128)(2,1)S(1)} %get-tuple-element.37.mine), channel_id=1, source_target_pairs={{0,8},{8,0},{16,24},{24,16},{1,9},{9,1},{17,25},{25,17},{2,10},{10... | collective-permute-start | bytes 221192 | tf_op jit(solution)/shard_map/ppermute | solution.py:414
  20.1 5.6 %collective-permute-start.2 = (bf16[144,256]{1,0:T(8,128)(2,1)S(1)}, bf16[144,256]{1,0:T(8,128)(2,1)S(1)}, u32[]{:S(2)}, u32[]{:S(2)}) collective-permute-start(bf16[144,256]{1,0:T(8,128)(2,1)S(1)} %get-tuple-element.42.mine), channel_id=1, source_target_pairs={{0,24},{8,16},{16,8},{24,0},{1,25},{9,17},{17,9},{25,1},{2,26},{10... | collective-permute-start | bytes 221192 | tf_op jit(solution)/shard_map/ppermute | solution.py:414
  26.1 4.5 %collective-permute-start.3 = (bf16[144,256]{1,0:T(8,128)(2,1)S(1)}, bf16[144,256]{1,0:T(8,128)(2,1)S(1)}, u32[]{:S(2)}, u32[]{:S(2)}) collective-permute-start(bf16[144,256]{1,0:T(8,128)(2,1)S(1)} %get-tuple-element.47.mine), channel_id=1, source_target_pairs={{0,32},{32,0},{64,96},{96,64},{1,33},{33,1},{65,97},{97,65},{2,34}... | collective-permute-start | bytes 221192 | tf_op jit(solution)/shard_map/ppermute | solution.py:414
  30.9 6.4 %collective-permute-start.4 = (bf16[80,256]{1,0:T(8,128)(2,1)S(1)}, bf16[80,256]{1,0:T(8,128)(2,1)S(1)}, u32[]{:S(2)}, u32[]{:S(2)}) collective-permute-start(bf16[80,256]{1,0:T(8,128)(2,1)S(1)} %get-tuple-element.58), channel_id=1, source_target_pairs={{0,96},{32,64},{64,32},{96,0},{1,97},{33,65},{65,33},{97,1},{2,98}... | collective-permute-start | bytes 122888 | tf_op jit(solution)/shard_map/ppermute | solution.py:414
  38.2 5.7 %collective-permute-start.5 = (bf16[64,384]{1,0:T(8,128)(2,1)S(1)}, bf16[64,384]{1,0:T(8,128)(2,1)S(1)}, u32[]{:S(2)}, u32[]{:S(2)}) collective-permute-start(bf16[64,384]{1,0:T(8,128)(2,1)S(1)} %get-tuple-element.64), channel_id=1, source_target_pairs={{0,1},{1,2},{2,3},{3,0},{4,5},{5,6},{6,7},{7,4},{8,9},{9,10},{10,1... | collective-permute-start | bytes 147464 | tf_op jit(solution)/shard_map/ppermute | solution.py:409
  39.8 5.6 %collective-permute-start.6 = (bf16[64,384]{1,0:T(8,128)(2,1)S(1)}, bf16[64,384]{1,0:T(8,128)(2,1)S(1)}, u32[]{:S(2)}, u32[]{:S(2)}) collective-permute-start(bf16[64,384]{1,0:T(8,128)(2,1)S(1)} %get-tuple-element.65), channel_id=1, source_target_pairs={{0,2},{1,3},{2,0},{3,1},{4,6},{5,7},{6,4},{7,5},{8,10},{9,11},{10,... | collective-permute-start | bytes 147464 | tf_op jit(solution)/shard_map/ppermute | solution.py:409
  42.5 4.1 %collective-permute-start.7 = (bf16[64,384]{1,0:T(8,128)(2,1)S(1)}, bf16[64,384]{1,0:T(8,128)(2,1)S(1)}, u32[]{:S(2)}, u32[]{:S(2)}) collective-permute-start(bf16[64,384]{1,0:T(8,128)(2,1)S(1)} %get-tuple-element.66), channel_id=1, source_target_pairs={{0,3},{1,0},{2,1},{3,2},{4,7},{5,4},{6,5},{7,6},{8,11},{9,8},{10,9... | collective-permute-start | bytes 147464 | tf_op jit(solution)/shard_map/ppermute | solution.py:409

commit v4 on v3

--- a/solution.py
+++ b/solution.py
@@ -104,32 +104,46 @@
 
 
 def local_kernel(*refs):
-    sources = refs[:12]
-    pack_out, prior_out, conv_out, normed_out, fall_out, start_out = refs[12:18]
-    erase_out, key_out, value_out, solved_out = refs[18:22]
-    targets = refs[22:34]
-    sems = refs[34]
+    sources = refs[:14]
+    pack_out, prior_out, conv_out, normed, fall_out, start_out = refs[14:20]
+    erase_out, key_out, value_out, weave_out, removed_out = refs[20:25]
+    late_weights = refs[25:27]
+    tokens, gain, key_gain, bias, shift, extra = refs[27:33]
+    weights = refs[33:37]
+    conv_weights = refs[37]
+    sems = refs[38]
+    targets = (
+        tokens,
+        gain,
+        key_gain,
+        bias,
+        shift,
+        extra,
+        *weights,
+        conv_weights.at[:, :CONV],
+        conv_weights.at[:, CONV:],
+        *late_weights,
+    )
     copies = [
         pltpu.make_async_copy(source, target, sems.at[n])
         for n, (source, target) in enumerate(zip(sources, targets))
     ]
-    for copy in copies:
-        copy.start()
-    tokens, gain, key_gain, bias, shift, extra = targets[:6]
+    for n in (0, 1, 6, 2, 7, 8, 3, 4, 5, 9, 10, 11, 12, 13):
+        copies[n].start()
     copies[0].wait()
     copies[1].wait()
-    rows = tokens[...].astype(F32)
-    scale = lax.rsqrt(jnp.mean(rows * rows, axis=-1, keepdims=True) + NORM_EPS)
-    normed = (rows * scale * gain[...]).astype(BF16)
-    normed_out[...] = normed
+    for n in range(ROWS // 16):
+        here = slice(16 * n, 16 * n + 16)
+        rows = tokens[here].astype(F32)
+        scale = lax.rsqrt(jnp.mean(rows * rows, axis=-1, keepdims=True) + NORM_EPS)
+        normed[here] = (rows * scale * gain[...]).astype(BF16)
 
     def project(n):
         copies[n].wait()
-        return rounded_product(normed, targets[n][...])
+        return rounded_product(normed[...], targets[n][...])
 
     square = (ROWS, LANES)
     row_at, lane_at = iota(square, 0), iota(square, 1)
-    same_chunk = row_at // SPAN == lane_at // SPAN
     ones = block_ones(LANES)
 
     key = project(6)
@@ -142,10 +156,18 @@
         copies[n].wait()
     logits = decay + bias[...] + shift[...]
     log_decay = extra[...] - EXP_HALF * jax.nn.sigmoid(logits)
-    lower = jnp.where(same_chunk & (lane_at <= row_at), 1.0, 0.0).astype(BF16)
+    small = (SPAN, SPAN)
+    lower = jnp.where(iota(small, 1) <= iota(small, 0), 1.0, 0.0).astype(BF16)
     part_high, part_mid = halves(log_decay)
     part_low = (log_decay - part_high.astype(F32) - part_mid.astype(F32)).astype(BF16)
-    cumulate = mm(lower, part_high) + (mm(lower, part_mid) + mm(lower, part_low))
+    chunks = [slice(SPAN * c, SPAN * c + SPAN) for c in range(CHUNKS)]
+    cumulate = jnp.concatenate(
+        [
+            mm(lower, part_high[at]) + (mm(lower, part_mid[at]) + mm(lower, part_low[at]))
+            for at in chunks
+        ],
+        axis=0,
+    )
     before = cumulate - log_decay
     mids = [cumulate[SPAN * c + 31 : SPAN * c + 32] for c in range(CHUNKS)]
     finals = [cumulate[SPAN * c + 63 : SPAN * c + 64] for c in range(CHUNKS)]
@@ -164,74 +186,83 @@
     kept_key = (key_s * to_end).astype(BF16)
     erase_b = erase_s.astype(BF16)
     key_b = key_s.astype(BF16)
-    value = project(9)
-    value_b = value.astype(BF16)
-    value_swapped = [
-        swap_pair(value[:, :128]).astype(BF16),
-        swap_pair(value[:, 128:]).astype(BF16),
-    ]
+    unit_b = unit_s.astype(BF16)
+    value_b = project(9).astype(BF16)
     erase_out[...] = erase_b
     key_out[...] = key_b
-    value_out[:, :128] = value_swapped[0]
-    value_out[:, 128:] = value_swapped[1]
-
-    strict = same_chunk & (lane_at < row_at)
-    near = strict & (row_at // 8 == lane_at // 8)
-    far = strict & (row_at // 8 != lane_at // 8)
-    low_half = iota((ROWS, 128), 1) < HEAD
-    solved = []
-    for h in range(4):
-        pair, own = h // 2, (low_half if h % 2 == 0 else ~low_half)
-        span = slice(128 * pair, 128 * pair + 128)
-        left = jnp.where(head_lanes(square, h), unit_s, 0.0).astype(BF16)
-        erase_mix = mm(left, erase_b, NT)
-        key_mix = jnp.where(strict, mm(left, key_b, NT), 0.0)
-        d1 = jnp.where(near, erase_mix, 0.0)
-        n1 = jnp.where(far, erase_mix, 0.0)
-        d2 = mm(d1, d1)
-        d4 = mm(d2, d2)
-        g = d2 - d1 - mm(d1, d2)
-        dinv = g + d4 + mm(g, d4)
-        p1 = n1 + mm(dinv, n1)
-        p2 = mm(p1, p1)
-        p4 = mm(p2, p2)
-        key_value = mm(key_mix, value_swapped[pair])
-        right = jnp.where(own, unit_q[:, span], key_value)
-        y = right + mm(dinv, right)
-        y = y + mm(p4, y)
-        y = y + mm(p2, y)
-        y = mm(p1, y) - y
-        solved.append(y)
-        solved_out[h] = y.astype(BF16)
-    weave = []
-    removed = []
-    for pair in range(2):
-        even, odd = solved[2 * pair], solved[2 * pair + 1]
-        weave.append(jnp.where(low_half, even, odd))
-        removed.append(swap_pair(jnp.where(low_half, odd, even)))
-    weave = jnp.concatenate(weave, axis=1).astype(BF16)
-    removed = jnp.concatenate(removed, axis=1).astype(BF16)
+    value_out[...] = value_b
+
+    copies[10].wait()
+    copies[11].wait()
+    both = rounded_product(normed[...], conv_weights[...])
+    conv_input = rounded(both[:, :CONV] * jax.nn.sigmoid(both[:, CONV:]))
+    conv_out[...] = conv_input
+    pack_out[2 * HEAD :, :128] = conv_input[ROWS - 32 : ROWS - 16]
+    pack_out[2 * HEAD :, 128:] = conv_input[ROWS - 16 :]
+
+    flat = (SPAN, LANES)
+    row_in, lane_in = iota(flat, 0), iota(flat, 1) % HEAD
+    strict = lane_in < row_in
+    near = strict & (row_in // 8 == lane_in // 8)
+    far = strict & (row_in // 8 != lane_in // 8)
+
+    def spread(value):
+        return jnp.concatenate([value.astype(BF16)] * 4, axis=0) * ones
+
+    def times(left, right):
+        return [mm(x, spread(y)) for x, y in zip(left, right)]
+
+    def add(*terms):
+        return [functools.reduce(lambda p, q: p + q, group) for group in zip(*terms)]
+
+    erase_mix = [mm(unit_b[at], spread(erase_b[at]), NT) for at in chunks]
+    key_mix = [
+        jnp.where(strict, mm(unit_b[at], spread(key_b[at]), NT), 0.0) for at in chunks
+    ]
+    d1 = [jnp.where(near, a, 0.0) for a in erase_mix]
+    n1 = [jnp.where(far, a, 0.0) for a in erase_mix]
+    d2 = times(d1, d1)
+    key_value = times(key_mix, [value_b[at] for at in chunks])
+    stacked = times([jnp.concatenate([p, q], axis=0) for p, q in zip(d1, d2)], d2)
+    d4 = [m[SPAN:] for m in stacked]
+    g = [q - p - m[:SPAN] for p, q, m in zip(d1, d2, stacked)]
+    dinv = add(g, d4, times(g, d4))
+    p1 = add(n1, times(dinv, n1))
+    p2 = times(p1, p1)
+    m1 = [d - p - r for d, p, r in zip(dinv, p1, times(p1, dinv))]
+    p4 = times(p2, p2)
+    m2 = add(m1, p2, times(p2, m1))
+    m3 = add(m2, p4, times(p4, m2))
+    start_unit = [unit_q[at] for at in chunks]
+    weave = [-x for x in add(start_unit, times(m3, start_unit))]
+    removed = [-x for x in add(key_value, times(m3, key_value))]
+    weave = [x.astype(BF16) for x in weave]
+    removed = [x.astype(BF16) for x in removed]
 
     same_head = row_at // HEAD == lane_at // HEAD
     eye = row_at == lane_at
     state = unit_state()
-    for c in range(CHUNKS):
-        here = slice(SPAN * c, SPAN * c + SPAN)
+    for c, at in enumerate(chunks):
+        weave_out[at] = weave[c]
+        removed_out[at] = removed[c]
         prior_out[c] = state
-        full = mm(weave[here], kept_erase[here], TN)
-        trans = jnp.where(same_head, full, 0.0) + jnp.where(
+        trans = jnp.where(same_head, mm(weave[c], kept_erase[at], TN), 0.0) + jnp.where(
             eye, jnp.broadcast_to(jnp.exp(finals[c]), square), 0.0
         )
-        base = mm(removed[here], kept_erase[here], TN) + mm(value_b[here], kept_key[here], TN)
+        base = mm(
+            jnp.concatenate([removed[c], value_b[at]], axis=0),
+            jnp.concatenate([kept_erase[at], kept_key[at]], axis=0),
+            TN,
+        )
         base = shrink(jnp.where(same_head, base, 0.0))
-        moved = mm3(state, trans)
-        state = jnp.concatenate([moved[:HEAD], moved[HEAD:] + base], axis=0)
+        if c == 0:
+            state = jnp.concatenate([shrink(trans), base], axis=0)
+        else:
+            moved = mm3(state, trans)
+            state = jnp.concatenate([moved[:HEAD], moved[HEAD:] + base], axis=0)
     pack_out[: 2 * HEAD] = state
-
-    conv_input = rounded(project(10) * jax.nn.sigmoid(project(11)))
-    conv_out[...] = conv_input
-    pack_out[2 * HEAD :, :128] = conv_input[ROWS - 32 : ROWS - 16]
-    pack_out[2 * HEAD :, 128:] = conv_input[ROWS - 16 :]
+    copies[12].wait()
+    copies[13].wait()
 
 
 def rounded(value):
@@ -253,43 +284,34 @@
     start,
     erase,
     key,
-    value_swapped,
-    solved,
+    value,
+    weave,
+    removed,
     priors,
     local_out,
     query_out,
 ):
-    square = (ROWS, LANES)
-    row_at, lane_at = iota(square, 0), iota(square, 1)
-    low_half = iota((ROWS, 128), 1) < HEAD
-    read_s = receptance[...] * fall[...]
-    read_q = read_s * per_chunk([start[c : c + 1] for c in range(CHUNKS)])
-    inclusive = (row_at // SPAN == lane_at // SPAN) & (lane_at <= row_at)
-    found = []
-    for h in range(4):
-        pair, own = h // 2, (low_half if h % 2 == 0 else ~low_half)
-        span = slice(128 * pair, 128 * pair + 128)
-        left = jnp.where(head_lanes(square, h), read_s, 0.0).astype(BF16)
-        read_erase = jnp.where(inclusive, mm(left, erase[...], NT), 0.0)
-        read_key = jnp.where(inclusive, mm(left, key[...], NT), 0.0)
-        mine = jnp.where(own, 0.0, value_swapped[:, span].astype(F32))
-        found.append(mm(read_erase, solved[h]) + mm(read_key, mine))
-    query, local = [], []
-    for pair in range(2):
-        even, odd = found[2 * pair], found[2 * pair + 1]
-        query.append(jnp.where(low_half, even, odd))
-        local.append(swap_pair(jnp.where(low_half, odd, even)))
-    query = jnp.concatenate(query, axis=1) + read_q
-    local = jnp.concatenate(local, axis=1)
+    ones = block_ones(LANES)
+    flat = (SPAN, LANES)
+    inclusive = iota(flat, 1) % HEAD <= iota(flat, 0)
+
+    def spread(part):
+        return jnp.concatenate([part.astype(BF16)] * 4, axis=0) * ones
+
     for c in range(CHUNKS):
         here = slice(SPAN * c, SPAN * c + SPAN)
-        if c == 0:
-            local_out[here] = local[here]
-            query_out[here] = query[here].astype(BF16)
-        else:
+        read_s = receptance[here] * fall[here]
+        read_b = read_s.astype(BF16)
+        read_erase = jnp.where(inclusive, mm(read_b, spread(erase[here]), NT), 0.0)
+        read_key = jnp.where(inclusive, mm(read_b, spread(key[here]), NT), 0.0)
+        query = read_s * start[c : c + 1] + mm(read_erase, spread(weave[here]))
+        local = mm(read_erase, spread(removed[here])) + mm(read_key, spread(value[here]))
+        if c:
             prior = priors[c]
-            local_out[here] = local[here] + mm(query[here], expand(prior[HEAD:]), NT)
-            query_out[here] = mm(query[here], expand(prior[:HEAD]), NT).astype(BF16)
+            local = local + mm(query, spread(prior[HEAD:]), NT)
+            query = mm(query, spread(prior[:HEAD]), NT)
+        local_out[here] = local
+        query_out[here] = query.astype(BF16)
 
 
 def conv_kernel(conv_in, taps, gain, shift, done_out, part_out, padded):
@@ -459,14 +481,27 @@
 
     conv_gain, conv_shift = as_row(convolution_group_gain), as_row(convolution_group_shift)
     wide = pltpu.VMEM((2048, LANES), BF16)
-    thin = pltpu.VMEM((2048, CONV), BF16)
     row = pltpu.VMEM((1, LANES), F32)
     square = ((ROWS, LANES), F32)
     square_b = ((ROWS, LANES), BF16)
     state = ((2 * HEAD, LANES), F32)
     packed = ((PACK, LANES), F32)
     packed_b = ((PACK, LANES), BF16)
-    pack, priors, conv_input, normed, fall, start, erase, key, value_swapped, solved = call(
+    (
+        pack,
+        priors,
+        conv_input,
+        normed,
+        fall,
+        start,
+        erase,
+        key,
+        value,
+        weave,
+        removed,
+        w_receptance,
+        w_gate,
+    ) = call(
         local_kernel,
         "local",
         [
@@ -476,11 +511,9 @@
             ((ROWS, 2048), BF16),
             square,
             ((8, LANES), F32),
-            square_b,
-            square_b,
-            square_b,
-            ((4, ROWS, CONV), BF16),
-        ],
+        ]
+        + [square_b] * 5
+        + [((2048, LANES), BF16)] * 2,
         (
             tokens,
             as_row(input_norm_gain),
@@ -494,14 +527,15 @@
             value_weight,
             convolution_value_weight,
             convolution_gate_weight,
+            receptance_weight,
+            output_gate_weight,
         ),
-        specs=[HBM] * 12,
+        specs=[HBM] * 14,
         pinned=True,
         scratch=[pltpu.VMEM((ROWS, 2048), BF16), pltpu.VMEM((1, 2048), F32), row, row]
         + [pltpu.VMEM((ROWS, LANES), F32)] * 2
-        + [wide] * 4
-        + [thin] * 2
-        + [pltpu.SemaphoreType.DMA((12,))],
+        + [wide] * 5
+        + [pltpu.SemaphoreType.DMA((14,))],
     )
     other = swapped(pack, "c", 1)
     pack, prefix, *total = call(core_kernel, "core", [packed_b, packed, state], (pack, other))
@@ -509,13 +543,13 @@
         gate_kernel,
         "gate",
         [square, square],
-        (normed, receptance_weight, output_gate_weight),
+        (normed, w_receptance, w_gate),
     )
     local_read, query = call(
         read_kernel,
         "read",
         [square, square_b],
-        (receptance, fall, start, erase, key, value_swapped, solved, priors),
+        (receptance, fall, start, erase, key, value, weave, removed, priors),
     )
     conv_done, conv_part = call(
         conv_kernel,

time: 48.6 us -> 43.2 us (0.89)
  Pallas kernels: 20.3 us -> 15.1 us
    pallas_call x10, Pallas kernels: 20.3 us -> 15.1 us  [call(): pl.pallas_call(kernel, name=name, out_shape=[jax.ShapeDtypeStruct(*o) for...]
  transfers between devices with their start and end apart: 8 -> 8, of which waited for: 7 -> 7; matrix products, arithmetic and copies ran while one was open for 0% -> 0% of each run, Pallas kernels for 5% -> 6%
where the time goes in v4:
time: 43.2 us; the launch traced here: 43.1 us
  starting transfers between devices  17.1 us (40%)
  Pallas kernels  15.1 us (35%)
  waiting for transfers between devices  10.7 us (25%)
    pallas_call x10, Pallas kernels, call(): pl.pallas_call(kernel, name=name, out_shape=[jax.ShapeDtypeStruct(*o) for...  15.1 us
    ppermute x5, starting transfers between devices, swapped(): return lax.ppermute(value, axis, [(s, s ^ bits) for s in range(count)])  11.4 us
    ppermute x5, waiting for transfers between devices, swapped(): return lax.ppermute(value, axis, [(s, s ^ bits) for s in range(count)])  8.09 us
    ppermute x3, starting transfers between devices, shifted(): lax.ppermute(value, axis, [(s, (s + steps) % count) for s in range(count)])  5.72 us
    ppermute x3, waiting for transfers between devices, shifted(): lax.ppermute(value, axis, [(s, (s + steps) % count) for s in range(count)])  2.65 us
  transfers between devices with their start and end apart: 8, of which 7 were waited for; matrix products, arithmetic and copies ran while one was open for 0% of the time, Pallas kernels for 6%

profile of v4, /device:TPU:0, one launch (start us, length us, event | category | flops | bytes accessed | tf_op | source)
XLA Modules:
  0.0 43.1 jit_solution(16898097528010900433)
XLA Ops:
  0.0 0.0 copy-start.2
  0.0 0.0 copy-start.3
  0.0 0.0 copy-start.4
  0.0 8.4 %local.1 = (f32[144,256]{1,0:T(8,128)S(1)}, f32[4,128,256]{2,1,0:T(8,128)S(1)}, f32[256,128]{1,0:T(8,128)S(1)}, bf16[256,2048]{1,0:T(8,128)(2,1)S(1)}, f32[256,2...) custom-call(bf16[256,2048]{1,0:T(8,128)(2,1)} %refs_0_.1, ...), custom_call_target="tpu_custom_call" | custom-call | tf_op jit(solution)/shard_map/local/pallas_call | solution.py:446
  8.4 0.0 copy-start.5
  8.4 0.0 copy-start
  8.4 0.0 copy-start.1
  8.4 0.1 collective-permute-start
  8.5 1.4 %collective-permute-done.other = f32[144,256]{1,0:T(8,128)S(1)} collective-permute-done((f32[144,256]{1,0:T(8,128)S(1)}, f32[144,256]{1,0:T(8,128)S(1)}, u32[]{:S(2)}, u32[]{:S(2)}) %collective-permute-start) | collective-permute-done | bytes 147488 | tf_op jit(solution)/shard_map/ppermute | solution.py:436
  9.9 0.2 core.1
  10.1 1.8 %collective-permute-start.1 = (bf16[144,256]{1,0:T(8,128)(2,1)S(1)}, bf16[144,256]{1,0:T(8,128)(2,1)S(1)}, u32[]{:S(2)}, u32[]{:S(2)}) collective-permute-start(bf16[144,256]{1,0:T(8,128)(2,1)S(1)} %get-tuple-element.40.mine), channel_id=1, source_target_pairs={{0,8},{8,0},{16,24},{24,16},{1,9},{9,1},{17,25},{25,17},{2,10},{10... | collective-permute-start | bytes 221192 | tf_op jit(solution)/shard_map/ppermute | solution.py:436
  11.9 0.0 copy-done.2
  11.9 0.0 copy-done.3
  11.9 0.0 copy-done.4
  11.9 0.6 %conv.1 = (bf16[256,128]{1,0:T(8,128)(2,1)S(1)}, f32[32,128]{1,0:T(8,128)S(1)}) custom-call(f32[256,128]{1,0:T(8,128)S(1)} %get-tuple-element.43.conv_in, f32[31,128]{1,0:T(8,128)S(1)} %copy-done.2, f32[1,128]{1,0:T(1,128)S(1)} %bitcast.6, f32[1,128]{1,0:T(1,128)S(1)} %bitcast.8), custom_call_target="tpu_custom_call" | custom-call | tf_op jit(solution)/shard_map/conv/pallas_call | solution.py:446
  12.6 2.0 %collective-permute-done.1.other = bf16[144,256]{1,0:T(8,128)(2,1)S(1)} collective-permute-done((bf16[144,256]{1,0:T(8,128)(2,1)S(1)}, bf16[144,256]{1,0:T(8,128)(2,1)S(1)}, u32[]{:S(2)}, u32[]{:S(2)}) %collective-permute-start.1) | collective-permute-done | bytes 73760 | tf_op jit(solution)/shard_map/ppermute | solution.py:436
  14.6 0.3 pair_y1.1
  14.9 3.2 %collective-permute-start.2 = (bf16[144,256]{1,0:T(8,128)(2,1)S(1)}, bf16[144,256]{1,0:T(8,128)(2,1)S(1)}, u32[]{:S(2)}, u32[]{:S(2)}) collective-permute-start(bf16[144,256]{1,0:T(8,128)(2,1)S(1)} %get-tuple-element.45.mine), channel_id=1, source_target_pairs={{0,24},{8,16},{16,8},{24,0},{1,25},{9,17},{17,9},{25,1},{2,26},{10... | collective-permute-start | bytes 221192 | tf_op jit(solution)/shard_map/ppermute | solution.py:436
  18.1 0.7 %gate.1 = (f32[256,256]{1,0:T(8,128)S(1)}, f32[256,256]{1,0:T(8,128)S(1)}) custom-call(bf16[256,2048]{1,0:T(8,128)(2,1)S(1)} %get-tuple-element.48.normed, bf16[2048,256]{1,0:T(8,128)(2,1)S(1)} %get-tuple-element.49.w_receptance, bf16[2048,256]{1,0:T(8,128)(2,1)S(1)} %get-tuple-element.50.w_gate), custom_call_target="tpu_custom_call" | custom-call | tf_op jit(solution)/shard_map/gate/pallas_call | solution.py:446
  18.8 1.7 %collective-permute-done.2.other = bf16[144,256]{1,0:T(8,128)(2,1)S(1)} collective-permute-done((bf16[144,256]{1,0:T(8,128)(2,1)S(1)}, bf16[144,256]{1,0:T(8,128)(2,1)S(1)}, u32[]{:S(2)}, u32[]{:S(2)}) %collective-permute-start.2) | collective-permute-done | bytes 73760 | tf_op jit(solution)/shard_map/ppermute | solution.py:436
  20.5 0.3 pair_y3.1
  20.9 2.1 %collective-permute-start.3 = (bf16[144,256]{1,0:T(8,128)(2,1)S(1)}, bf16[144,256]{1,0:T(8,128)(2,1)S(1)}, u32[]{:S(2)}, u32[]{:S(2)}) collective-permute-start(bf16[144,256]{1,0:T(8,128)(2,1)S(1)} %get-tuple-element.52.mine), channel_id=1, source_target_pairs={{0,32},{32,0},{64,96},{96,64},{1,33},{33,1},{65,97},{97,65},{2,34}... | collective-permute-start | bytes 221192 | tf_op jit(solution)/shard_map/ppermute | solution.py:436
  23.0 1.3 %read.1 = (f32[256,256]{1,0:T(8,128)S(1)}, bf16[256,256]{1,0:T(8,128)(2,1)S(1)}) custom-call(f32[256,256]{1,0:T(8,128)S(1)} %get-tuple-element.51._.receptance, f32[256,256]{1,0:T(8,128)S(1)} %get-tuple-element.55.fall, f32[8,256]{1,0:T(8,128)S(1)} %get-tuple-element.56.start, bf16[256,256]{1,0:T(8,128)(2,1)S(1)} %get-tuple-element.57.erase, ...), custom_call_target="tpu_custom_call" | custom-call | tf_op jit(solution)/shard_map/read/pallas_call | solution.py:446
  24.3 1.0 %collective-permute-done.3.other = bf16[144,256]{1,0:T(8,128)(2,1)S(1)} collective-permute-done((bf16[144,256]{1,0:T(8,128)(2,1)S(1)}, bf16[144,256]{1,0:T(8,128)(2,1)S(1)}, u32[]{:S(2)}, u32[]{:S(2)}) %collective-permute-start.3) | collective-permute-done | bytes 73760 | tf_op jit(solution)/shard_map/ppermute | solution.py:436
  25.3 0.3 pair_z1.1
  25.7 4.2 %collective-permute-start.4 = (bf16[80,256]{1,0:T(8,128)(2,1)S(1)}, bf16[80,256]{1,0:T(8,128)(2,1)S(1)}, u32[]{:S(2)}, u32[]{:S(2)}) collective-permute-start(bf16[80,256]{1,0:T(8,128)(2,1)S(1)} %get-tuple-element.64), channel_id=1, source_target_pairs={{0,96},{32,64},{64,32},{96,0},{1,97},{33,65},{65,33},{97,1},{2,98}... | collective-permute-start | bytes 122888 | tf_op jit(solution)/shard_map/ppermute | solution.py:436
  29.9 2.0 %collective-permute-done.4.other = bf16[80,256]{1,0:T(8,128)(2,1)S(1)} collective-permute-done((bf16[80,256]{1,0:T(8,128)(2,1)S(1)}, bf16[80,256]{1,0:T(8,128)(2,1)S(1)}, u32[]{:S(2)}, u32[]{:S(2)}) %collective-permute-start.4) | collective-permute-done | bytes 40992 | tf_op jit(solution)/shard_map/ppermute | solution.py:436
  31.9 0.0 copy-done.5
  31.9 0.9 %last.1 = (bf16[64,384]{1,0:T(8,128)(2,1)S(1)}, bf16[64,384]{1,0:T(8,128)(2,1)S(1)}, bf16[64,384]{1,0:T(8,128)(2,1)S(1)}, bf16[64,384]{1,0:T(8,128)(2,1)S(1)}) custom-call(bf16[80,256]{1,0:T(8,128)(2,1)S(1)} %collective-permute-done.4.other, f32[144,256]{1,0:T(8,128)S(1)} %get-tuple-element.65.prefix, f32[256,256]{1,0:T(8,128)S(1)} %get-tuple-element.63._.local, ...), custom_call_target="tpu_custom_call" | custom-call | tf_op jit(solution)/shard_map/last/pallas_call | solution.py:446
  32.8 1.6 %collective-permute-start.5 = (bf16[64,384]{1,0:T(8,128)(2,1)S(1)}, bf16[64,384]{1,0:T(8,128)(2,1)S(1)}, u32[]{:S(2)}, u32[]{:S(2)}) collective-permute-start(bf16[64,384]{1,0:T(8,128)(2,1)S(1)} %get-tuple-element.70), channel_id=1, source_target_pairs={{0,1},{1,2},{2,3},{3,0},{4,5},{5,6},{6,7},{7,4},{8,9},{9,10},{10,1... | collective-permute-start | bytes 147464 | tf_op jit(solution)/shard_map/ppermute | solution.py:431
  34.3 2.7 %collective-permute-start.6 = (bf16[64,384]{1,0:T(8,128)(2,1)S(1)}, bf16[64,384]{1,0:T(8,128)(2,1)S(1)}, u32[]{:S(2)}, u32[]{:S(2)}) collective-permute-start(bf16[64,384]{1,0:T(8,128)(2,1)S(1)} %get-tuple-element.71), channel_id=1, source_target_pairs={{0,2},{1,3},{2,0},{3,1},{4,6},{5,7},{6,4},{7,5},{8,10},{9,11},{10,... | collective-permute-start | bytes 147464 | tf_op jit(solution)/shard_map/ppermute | solution.py:431
  37.1 1.4 %collective-permute-start.7 = (bf16[64,384]{1,0:T(8,128)(2,1)S(1)}, bf16[64,384]{1,0:T(8,128)(2,1)S(1)}, u32[]{:S(2)}, u32[]{:S(2)}) collective-permute-start(bf16[64,384]{1,0:T(8,128)(2,1)S(1)} %get-tuple-element.72), channel_id=1, source_target_pairs={{0,3},{1,0},{2,1},{3,2},{4,7},{5,4},{6,5},{7,6},{8,11},{9,8},{10,9... | collective-permute-start | bytes 147464 | tf_op jit(solution)/shard_map/ppermute | solution.py:431
  38.5 0.0 collective-permute-done.5.from_1
  38.5 1.4 %collective-permute-done.6.from_2 = bf16[64,384]{1,0:T(8,128)(2,1)S(1)} collective-permute-done((bf16[64,384]{1,0:T(8,128)(2,1)S(1)}, bf16[64,384]{1,0:T(8,128)(2,1)S(1)}, u32[]{:S(2)}, u32[]{:S(2)}) %collective-permute-start.6) | collective-permute-done | bytes 49184 | tf_op jit(solution)/shard_map/ppermute | solution.py:431
  39.9 1.2 %collective-permute-done.7.from_3 = bf16[64,384]{1,0:T(8,128)(2,1)S(1)} collective-permute-done((bf16[64,384]{1,0:T(8,128)(2,1)S(1)}, bf16[64,384]{1,0:T(8,128)(2,1)S(1)}, u32[]{:S(2)}, u32[]{:S(2)}) %collective-permute-start.7) | collective-permute-done | bytes 49184 | tf_op jit(solution)/shard_map/ppermute | solution.py:431
  41.2 0.0 copy-done
  41.2 0.0 copy-done.1
  41.2 1.9 %project.1 = bf16[64,2048]{1,0:T(8,128)(2,1)} custom-call(bf16[64,384]{1,0:T(8,128)(2,1)S(1)} %get-tuple-element.69.own, bf16[64,384]{1,0:T(8,128)(2,1)S(1)} %collective-permute-done.5.from_1, bf16[64,384]{1,0:T(8,128)(2,1)S(1)} %collective-permute-done.6.from_2, bf16[64,384]{1,0:T(8,128)(2,1)S(1)} %collective-permute-done.7.from_3, ...), custom_call_target="tpu_custom_call" | custom-call | tf_op jit(solution)/shard_map/project/pallas_call | solution.py:446
Async XLA Ops:
  0.0 11.9 %copy-start.2 = (f32[31,128]{1,0:T(8,128)S(1)}, f32[31,128]{1,0:T(8,128)}, u32[]{:S(2)}) copy-start(f32[31,128]{1,0:T(8,128)} %taps.3) | copy-start | bytes 47620
  0.0 11.9 %copy-start.3 = (f32[128]{0:T(128)S(1)}, f32[128]{0:T(128)}, u32[]{:S(2)}) copy-start(f32[128]{0:T(128)} %param.25) | copy-start | bytes 1540
  0.0 11.9 %copy-start.4 = (f32[128]{0:T(128)S(1)}, f32[128]{0:T(128)}, u32[]{:S(2)}) copy-start(f32[128]{0:T(128)} %param.26) | copy-start | bytes 1540
  8.4 23.5 %copy-start.5 = (f32[256]{0:T(256)S(1)}, f32[256]{0:T(256)}, u32[]{:S(2)}) copy-start(f32[256]{0:T(256)} %param.37) | copy-start | bytes 3076
  8.4 32.8 %copy-start = (bf16[1024,2048]{1,0:T(8,128)(2,1)S(1)}, bf16[1024,2048]{1,0:T(8,128)(2,1)}, u32[]{:S(2)}) copy-start(bf16[1024,2048]{1,0:T(8,128)(2,1)} %mix_w.1) | copy-start | bytes 12582916
  8.4 32.7 %copy-start.1 = (bf16[512,2048]{1,0:T(8,128)(2,1)S(1)}, bf16[512,2048]{1,0:T(8,128)(2,1)}, u32[]{:S(2)}) copy-start(bf16[512,2048]{1,0:T(8,128)(2,1)} %conv_w.1) | copy-start | bytes 6291460
  8.4 1.5 %collective-permute-start = (f32[144,256]{1,0:T(8,128)S(1)}, f32[144,256]{1,0:T(8,128)S(1)}, u32[]{:S(2)}, u32[]{:S(2)}) collective-permute-start(f32[144,256]{1,0:T(8,128)S(1)} %get-tuple-element.39.mine), channel_id=1, source_target_pairs={{0,4},{4,0},{1,5},{5,1},{2,6},{6,2},{3,7},{7,3},{8,12},{12,8},{9,1... | collective-permute-start | bytes 442376 | tf_op jit(solution)/shard_map/ppermute | solution.py:436
  10.1 4.4 %collective-permute-start.1 = (bf16[144,256]{1,0:T(8,128)(2,1)S(1)}, bf16[144,256]{1,0:T(8,128)(2,1)S(1)}, u32[]{:S(2)}, u32[]{:S(2)}) collective-permute-start(bf16[144,256]{1,0:T(8,128)(2,1)S(1)} %get-tuple-element.40.mine), channel_id=1, source_target_pairs={{0,8},{8,0},{16,24},{24,16},{1,9},{9,1},{17,25},{25,17},{2,10},{10... | collective-permute-start | bytes 221192 | tf_op jit(solution)/shard_map/ppermute | solution.py:436
  14.9 5.6 %collective-permute-start.2 = (bf16[144,256]{1,0:T(8,128)(2,1)S(1)}, bf16[144,256]{1,0:T(8,128)(2,1)S(1)}, u32[]{:S(2)}, u32[]{:S(2)}) collective-permute-start(bf16[144,256]{1,0:T(8,128)(2,1)S(1)} %get-tuple-element.45.mine), channel_id=1, source_target_pairs={{0,24},{8,16},{16,8},{24,0},{1,25},{9,17},{17,9},{25,1},{2,26},{10... | collective-permute-start | bytes 221192 | tf_op jit(solution)/shard_map/ppermute | solution.py:436
  20.9 4.4 %collective-permute-start.3 = (bf16[144,256]{1,0:T(8,128)(2,1)S(1)}, bf16[144,256]{1,0:T(8,128)(2,1)S(1)}, u32[]{:S(2)}, u32[]{:S(2)}) collective-permute-start(bf16[144,256]{1,0:T(8,128)(2,1)S(1)} %get-tuple-element.52.mine), channel_id=1, source_target_pairs={{0,32},{32,0},{64,96},{96,64},{1,33},{33,1},{65,97},{97,65},{2,34}... | collective-permute-start | bytes 221192 | tf_op jit(solution)/shard_map/ppermute | solution.py:436
  25.7 6.2 %collective-permute-start.4 = (bf16[80,256]{1,0:T(8,128)(2,1)S(1)}, bf16[80,256]{1,0:T(8,128)(2,1)S(1)}, u32[]{:S(2)}, u32[]{:S(2)}) collective-permute-start(bf16[80,256]{1,0:T(8,128)(2,1)S(1)} %get-tuple-element.64), channel_id=1, source_target_pairs={{0,96},{32,64},{64,32},{96,0},{1,97},{33,65},{65,33},{97,1},{2,98}... | collective-permute-start | bytes 122888 | tf_op jit(solution)/shard_map/ppermute | solution.py:436
  32.8 5.7 %collective-permute-start.5 = (bf16[64,384]{1,0:T(8,128)(2,1)S(1)}, bf16[64,384]{1,0:T(8,128)(2,1)S(1)}, u32[]{:S(2)}, u32[]{:S(2)}) collective-permute-start(bf16[64,384]{1,0:T(8,128)(2,1)S(1)} %get-tuple-element.70), channel_id=1, source_target_pairs={{0,1},{1,2},{2,3},{3,0},{4,5},{5,6},{6,7},{7,4},{8,9},{9,10},{10,1... | collective-permute-start | bytes 147464 | tf_op jit(solution)/shard_map/ppermute | solution.py:431
  34.3 5.6 %collective-permute-start.6 = (bf16[64,384]{1,0:T(8,128)(2,1)S(1)}, bf16[64,384]{1,0:T(8,128)(2,1)S(1)}, u32[]{:S(2)}, u32[]{:S(2)}) collective-permute-start(bf16[64,384]{1,0:T(8,128)(2,1)S(1)} %get-tuple-element.71), channel_id=1, source_target_pairs={{0,2},{1,3},{2,0},{3,1},{4,6},{5,7},{6,4},{7,5},{8,10},{9,11},{10,... | collective-permute-start | bytes 147464 | tf_op jit(solution)/shard_map/ppermute | solution.py:431
  37.1 4.1 %collective-permute-start.7 = (bf16[64,384]{1,0:T(8,128)(2,1)S(1)}, bf16[64,384]{1,0:T(8,128)(2,1)S(1)}, u32[]{:S(2)}, u32[]{:S(2)}) collective-permute-start(bf16[64,384]{1,0:T(8,128)(2,1)S(1)} %get-tuple-element.72), channel_id=1, source_target_pairs={{0,3},{1,0},{2,1},{3,2},{4,7},{5,4},{6,5},{7,6},{8,11},{9,8},{10,9... | collective-permute-start | bytes 147464 | tf_op jit(solution)/shard_map/ppermute | solution.py:431

commit v5 on v4

--- a/solution.py
+++ b/solution.py
@@ -348,30 +348,31 @@
     prefix_out[2 * HEAD :] = jnp.where(first, 0.0, early[2 * HEAD :])
 
 
-def pair_kernel(axis, far, sent, mine, total, other, prefix, _, pack_out, prefix_out, *total_out):
-    at = lax.axis_index(axis)
-    upper = (at >= 2) if far else (lax.rem(at, 2) == 1)
-    got = other[...].astype(F32)
-    states = got[: 2 * HEAD]
-    early = jnp.where(upper, states, total[...])
-    late = jnp.where(upper, total[...], states)
-    result = joined(early, late)
-    for out in total_out:
-        out[...] = result
-    pack_out[: HEAD * sent] = result[HEAD * (2 - sent) :].astype(BF16)
-    tail = other if far else mine
-    pack_out[HEAD * sent :] = tail[2 * HEAD :]
-    behind = joined(states, prefix[...])
-    prefix_out[: 2 * HEAD] = jnp.where(upper, behind, prefix[: 2 * HEAD])
-    takes = (at == 2) if far else upper
-    takes = takes & (lax.axis_index("c") == 0)
-    if axis == "z":
-        takes = takes & (lax.axis_index("y") == 0)
-    prefix_out[2 * HEAD :] = jnp.where(takes, got[2 * HEAD :], prefix[2 * HEAD :])
+def row_kernel(own, total, from_1, from_2, from_3, prefix, *refs):
+    pack_out, prefix_out, slots = refs[-3:]
+    me, core = lax.axis_index("y"), lax.axis_index("c")
+    slots[0, : 2 * HEAD] = total[...]
+    slots[0, 2 * HEAD :] = own[2 * HEAD :].astype(F32)
+    for n, ref in enumerate((from_1, from_2, from_3)):
+        slots[n + 1] = ref[...].astype(F32)
+    state = slots[me ^ 0][: 2 * HEAD]
+    before = unit_state()
+    for n in range(1, 4):
+        before = jnp.where(me == n, state, before)
+        piece = slots[me ^ n]
+        state = follow(state, piece[:HEAD], piece[HEAD : 2 * HEAD])
+    pack_out[: 2 * HEAD] = state.astype(BF16)
+    pack_out[2 * HEAD :] = slots[me ^ 3, 2 * HEAD :].astype(BF16)
+    prefix_out[: 2 * HEAD] = follow(before, prefix[:HEAD], prefix[HEAD : 2 * HEAD])
+    behind = slots[me ^ jnp.maximum(me - 1, 0), 2 * HEAD :]
+    takes = (me > 0) & (core == 0)
+    prefix_out[2 * HEAD :] = jnp.where(takes, behind, prefix[2 * HEAD :])
 
 
 def last_kernel(
-    other,
+    from_1,
+    from_2,
+    from_3,
     prefix,
     local,
     query,
@@ -386,13 +387,20 @@
     out_1,
     out_2,
     out_3,
+    slots,
     ready,
     padded,
 ):
     z, y, c, x = (lax.axis_index(name) for name in SP_TP)
-    got = other[...].astype(F32)
-    entering = jnp.where(z >= 2, got[:HEAD], 0.0)
-    state = mm3(entering, expand(prefix[:HEAD])) + prefix[HEAD : 2 * HEAD]
+    for n, ref in enumerate((from_1, from_2, from_3)):
+        slots[n + 1] = ref[...].astype(F32)
+    slots[0] = slots[1]
+    state = jnp.where(z > 0, slots[z ^ 0, HEAD : 2 * HEAD], 0.0)
+    for n in range(1, 3):
+        piece = slots[z ^ n]
+        moved = mm3(state, expand(piece[:HEAD])) + piece[HEAD : 2 * HEAD]
+        state = jnp.where(n < z, moved, state)
+    state = mm3(state, expand(prefix[:HEAD])) + prefix[HEAD : 2 * HEAD]
     readout = local[...] + mm(query[...], expand(state), NT)
     ones = block_ones(LANES)
     centred = readout - group_sum(readout, ones) * (1.0 / HEAD)
@@ -401,8 +409,9 @@
     ready[:, CONV:] = mixed.astype(BF16)
     ready[:, :CONV] = conv_done[...]
 
-    takes = (z == 2) & (y == 0) & (c == 0)
-    side = jnp.where(takes, got[HEAD:], prefix[2 * HEAD :])
+    behind = slots[z ^ jnp.maximum(z - 1, 0), 2 * HEAD :]
+    takes = (z > 0) & (y == 0) & (c == 0)
+    side = jnp.where(takes, behind, prefix[2 * HEAD :])
     padded[:16] = side[:, :128]
     padded[16:32] = side[:, 128:]
     padded[32:] = jnp.zeros((HALO, CONV), F32)
@@ -411,14 +420,14 @@
         total = total + taps[j : j + 1] * padded[2 + j : 2 + j + HALO]
     ready[:HALO, :CONV] = finish_conv(total, conv_gain[...], conv_shift[...])
     for n, out in enumerate((out_0, out_1, out_2, out_3)):
-        to = lax.rem(x + n, 4)
+        to = x ^ n
         out[...] = ready[pl.ds(pl.multiple_of(to * SPAN, SPAN), SPAN)]
 
 
 def project_kernel(own, from_1, from_2, from_3, conv_w, mix_w, out, conv_rows, mix_rows):
     x = lax.axis_index("x")
     for n, ref in enumerate((own, from_1, from_2, from_3)):
-        of = lax.rem(x - n + 4, 4)
+        of = x ^ n
         conv_rows[:, pl.ds(pl.multiple_of(of * CONV, CONV), CONV)] = ref[:, :CONV]
         mix_rows[:, pl.ds(pl.multiple_of(of * LANES, LANES), LANES)] = ref[:, CONV:]
     total = jnp.dot(conv_rows[...], conv_w[...], preferred_element_type=F32)
@@ -426,14 +435,9 @@
     out[...] = total.astype(BF16)
 
 
-def shifted(value, axis, steps):
-    count = lax.axis_size(axis)
-    return lax.ppermute(value, axis, [(s, (s + steps) % count) for s in range(count)])
-
-
-def swapped(value, axis, bits):
-    count = lax.axis_size(axis)
-    return lax.ppermute(value, axis, [(s, s ^ bits) for s in range(count)])
+def swapped(value, axes, bits):
+    count = lax.axis_size(axes)
+    return lax.ppermute(value, axes, [(s, s ^ bits) for s in range(count)])
 
 
 def params():
@@ -538,7 +542,7 @@
         + [pltpu.SemaphoreType.DMA((14,))],
     )
     other = swapped(pack, "c", 1)
-    pack, prefix, *total = call(core_kernel, "core", [packed_b, packed, state], (pack, other))
+    pack, prefix, total = call(core_kernel, "core", [packed_b, packed, state], (pack, other))
     receptance, gate = call(
         gate_kernel,
         "gate",
@@ -558,24 +562,22 @@
         (conv_input, depthwise_taps_weight, conv_gain, conv_shift),
         scratch=[pltpu.VMEM((HALO + ROWS, CONV), F32)],
     )
-    beside = (conv_done, receptance, local_read)
-    for (axis, far), side in zip((("y", False), ("y", True), ("z", False)), beside):
-        other = swapped(pack, axis, 3 if far else 1)
-        sent = 1 if axis == "z" else 2
-        pack, prefix, *total = call(
-            functools.partial(pair_kernel, axis, far, sent),
-            f"pair_{axis}{3 if far else 1}",
-            [((HEAD * sent + HALO // 2, LANES), BF16), packed] + [state] * (sent - 1),
-            (pack, total[0], other, prefix, side),
-            specs=[VMEM] * 4 + [ANY],
-        )
-    other = swapped(pack, "z", 3)
+    planes = [swapped(pack, ("y", "c"), 2 * n + 1) for n in (1, 2, 3)]
+    pack, prefix = call(
+        row_kernel,
+        "row",
+        [packed_b, packed],
+        (pack, total, *planes, prefix, conv_done, gate),
+        specs=[VMEM] * 6 + [ANY] * 2,
+        scratch=[pltpu.VMEM((4, PACK, LANES), F32)],
+    )
+    planes = [swapped(pack, ("z", "c"), 2 * n + 1) for n in (1, 2, 3)]
     sends = call(
         last_kernel,
         "last",
         [((SPAN, CONV + LANES), BF16)] * 4,
         (
-            other,
+            *planes,
             prefix,
             local_read,
             query,
@@ -588,11 +590,12 @@
             conv_shift,
         ),
         scratch=[
+            pltpu.VMEM((4, PACK, LANES), F32),
             pltpu.VMEM((ROWS, CONV + LANES), BF16),
             pltpu.VMEM((2 * HALO, CONV), F32),
         ],
     )
-    arrived = [shifted(sends[n], "x", n) for n in (1, 2, 3)]
+    arrived = [swapped(sends[n], "x", n) for n in (1, 2, 3)]
     (mixed,) = call(
         project_kernel,
         "project",

time: 43.2 us -> 45.3 us (1.049)
  waiting for transfers between devices: 10.7 us -> 15.2 us
  starting transfers between devices: 17.1 us -> 14.6 us
    ppermute x8 -> x10, waiting for transfers between devices: 10.7 us -> 15.2 us  [swapped(): return lax.ppermute(value, axes, [(s, s ^ bits) for s in range(count)])]
    ppermute x8 -> x10, starting transfers between devices: 17.1 us -> 14.6 us  [swapped(): return lax.ppermute(value, axes, [(s, s ^ bits) for s in range(count)])]
    pallas_call x10 -> x8, Pallas kernels: 15.1 us -> 15.3 us  [call(): pl.pallas_call(kernel, name=name, out_shape=[jax.ShapeDtypeStruct(*o) for...]
  transfers between devices with their start and end apart: 8 -> 10, of which waited for: 7 -> 7; matrix products, arithmetic and copies ran while one was open for 0% -> 0% of each run, Pallas kernels for 6% -> 6%
where the time goes in v5:
time: 45.3 us; the launch traced here: 45.2 us
  Pallas kernels  15.3 us (34%)
  waiting for transfers between devices  15.2 us (34%)
  starting transfers between devices  14.6 us (32%)
    pallas_call x8, Pallas kernels, call(): pl.pallas_call(kernel, name=name, out_shape=[jax.ShapeDtypeStruct(*o) for...  15.3 us
    ppermute x10, waiting for transfers between devices, swapped(): return lax.ppermute(value, axes, [(s, s ^ bits) for s in range(count)])  15.2 us
    ppermute x10, starting transfers between devices, swapped(): return lax.ppermute(value, axes, [(s, s ^ bits) for s in range(count)])  14.6 us
  transfers between devices with their start and end apart: 10, of which 7 were waited for; matrix products, arithmetic and copies ran while one was open for 0% of the time, Pallas kernels for 6%

profile of v5, /device:TPU:0, one launch (start us, length us, event | category | flops | bytes accessed | tf_op | source)
XLA Modules:
  0.0 45.2 jit_solution(1519484251749723939)
XLA Ops:
  0.0 0.0 copy-start.2
  0.0 0.0 copy-start.3
  0.0 0.0 copy-start.4
  0.0 0.0 copy-start.5
  0.0 8.4 %local.1 = (f32[144,256]{1,0:T(8,128)S(1)}, f32[4,128,256]{2,1,0:T(8,128)S(1)}, f32[256,128]{1,0:T(8,128)S(1)}, bf16[256,2048]{1,0:T(8,128)(2,1)S(1)}, f32[256,2...) custom-call(bf16[256,2048]{1,0:T(8,128)(2,1)} %refs_0_.1, ...), custom_call_target="tpu_custom_call" | custom-call | tf_op jit(solution)/shard_map/local/pallas_call | solution.py:450
  8.4 0.0 copy-start
  8.4 0.0 copy-start.1
  8.4 0.1 collective-permute-start
  8.5 1.4 %collective-permute-done.other = f32[144,256]{1,0:T(8,128)S(1)} collective-permute-done((f32[144,256]{1,0:T(8,128)S(1)}, f32[144,256]{1,0:T(8,128)S(1)}, u32[]{:S(2)}, u32[]{:S(2)}) %collective-permute-start) | collective-permute-done | bytes 147488 | tf_op jit(solution)/shard_map/ppermute | solution.py:440
  9.9 0.3 core.1
  10.2 1.5 %collective-permute-start.1 = (bf16[144,256]{1,0:T(8,128)(2,1)S(1)}, bf16[144,256]{1,0:T(8,128)(2,1)S(1)}, u32[]{:S(2)}, u32[]{:S(2)}) collective-permute-start(bf16[144,256]{1,0:T(8,128)(2,1)S(1)} %get-tuple-element.34.own), channel_id=1, source_target_pairs={{0,12},{4,8},{8,4},{12,0},{16,28},{20,24},{24,20},{28,16},{1,13},{... | collective-permute-start | bytes 221192 | tf_op jit(solution)/shard_map/ppermute | solution.py:440
  11.7 2.9 %collective-permute-start.2 = (bf16[144,256]{1,0:T(8,128)(2,1)S(1)}, bf16[144,256]{1,0:T(8,128)(2,1)S(1)}, u32[]{:S(2)}, u32[]{:S(2)}) collective-permute-start(bf16[144,256]{1,0:T(8,128)(2,1)S(1)} %get-tuple-element.34.own), channel_id=1, source_target_pairs={{0,20},{4,16},{8,28},{12,24},{16,4},{20,0},{24,12},{28,8},{1,21},{... | collective-permute-start | bytes 221192 | tf_op jit(solution)/shard_map/ppermute | solution.py:440
  14.5 0.0 collective-permute-start.3
  14.5 0.7 %gate.1 = (f32[256,256]{1,0:T(8,128)S(1)}, f32[256,256]{1,0:T(8,128)S(1)}) custom-call(bf16[256,2048]{1,0:T(8,128)(2,1)S(1)} %get-tuple-element.39.normed, bf16[2048,256]{1,0:T(8,128)(2,1)S(1)} %get-tuple-element.40.w_receptance, bf16[2048,256]{1,0:T(8,128)(2,1)S(1)} %get-tuple-element.41.w_gate), custom_call_target="tpu_custom_call" | custom-call | tf_op jit(solution)/shard_map/gate/pallas_call | solution.py:450
  15.3 0.0 copy-done.2
  15.3 0.0 copy-done.3
  15.3 0.0 copy-done.4
  15.3 0.6 %conv.1 = (bf16[256,128]{1,0:T(8,128)(2,1)S(1)}, f32[32,128]{1,0:T(8,128)S(1)}) custom-call(f32[256,128]{1,0:T(8,128)S(1)} %get-tuple-element.37.conv_in, f32[31,128]{1,0:T(8,128)S(1)} %copy-done.2, f32[1,128]{1,0:T(1,128)S(1)} %bitcast.6, f32[1,128]{1,0:T(1,128)S(1)} %bitcast.8), custom_call_target="tpu_custom_call" | custom-call | tf_op jit(solution)/shard_map/conv/pallas_call | solution.py:450
  15.9 0.0 collective-permute-done.1.from_1
  15.9 2.7 %collective-permute-done.2.from_2 = bf16[144,256]{1,0:T(8,128)(2,1)S(1)} collective-permute-done((bf16[144,256]{1,0:T(8,128)(2,1)S(1)}, bf16[144,256]{1,0:T(8,128)(2,1)S(1)}, u32[]{:S(2)}, u32[]{:S(2)}) %collective-permute-start.2) | collective-permute-done | bytes 73760 | tf_op jit(solution)/shard_map/ppermute | solution.py:440
  18.6 1.8 %collective-permute-done.3.from_3 = bf16[144,256]{1,0:T(8,128)(2,1)S(1)} collective-permute-done((bf16[144,256]{1,0:T(8,128)(2,1)S(1)}, bf16[144,256]{1,0:T(8,128)(2,1)S(1)}, u32[]{:S(2)}, u32[]{:S(2)}) %collective-permute-start.3) | collective-permute-done | bytes 73760 | tf_op jit(solution)/shard_map/ppermute | solution.py:440
  20.4 0.7 %row.1 = (bf16[144,256]{1,0:T(8,128)(2,1)S(1)}, f32[144,256]{1,0:T(8,128)S(1)}) custom-call(bf16[144,256]{1,0:T(8,128)(2,1)S(1)} %get-tuple-element.34.own, f32[128,256]{1,0:T(8,128)S(1)} %get-tuple-element.35.total, bf16[144,256]{1,0:T(8,128)(2,1)S(1)} %collective-permute-done.1.from_1, bf16[144,256]{1,0:T(8,128)(2,1)S(1)} %collective-permute-done.2.from_2, ...), custom_call_target="tpu_custom_call" | custom-call | tf_op jit(solution)/shard_map/row/pallas_call | solution.py:450
  21.1 1.7 %collective-permute-start.4 = (bf16[144,256]{1,0:T(8,128)(2,1)S(1)}, bf16[144,256]{1,0:T(8,128)(2,1)S(1)}, u32[]{:S(2)}, u32[]{:S(2)}) collective-permute-start(bf16[144,256]{1,0:T(8,128)(2,1)S(1)} %get-tuple-element.43), channel_id=1, source_target_pairs={{0,36},{4,32},{32,4},{36,0},{64,100},{68,96},{96,68},{100,64},{1,3... | collective-permute-start | bytes 221192 | tf_op jit(solution)/shard_map/ppermute | solution.py:440
  22.8 3.6 %collective-permute-start.5 = (bf16[144,256]{1,0:T(8,128)(2,1)S(1)}, bf16[144,256]{1,0:T(8,128)(2,1)S(1)}, u32[]{:S(2)}, u32[]{:S(2)}) collective-permute-start(bf16[144,256]{1,0:T(8,128)(2,1)S(1)} %get-tuple-element.43), channel_id=1, source_target_pairs={{0,68},{4,64},{32,100},{36,96},{64,4},{68,0},{96,36},{100,32},{1,6... | collective-permute-start | bytes 221192 | tf_op jit(solution)/shard_map/ppermute | solution.py:440
  26.4 0.0 collective-permute-start.6
  26.4 1.3 %read.1 = (f32[256,256]{1,0:T(8,128)S(1)}, bf16[256,256]{1,0:T(8,128)(2,1)S(1)}) custom-call(f32[256,256]{1,0:T(8,128)S(1)} %get-tuple-element.45.receptance, f32[256,256]{1,0:T(8,128)S(1)} %get-tuple-element.46.fall, f32[8,256]{1,0:T(8,128)S(1)} %get-tuple-element.47.start, bf16[256,256]{1,0:T(8,128)(2,1)S(1)} %get-tuple-element.48.erase, ...), custom_call_target="tpu_custom_call" | custom-call | tf_op jit(solution)/shard_map/read/pallas_call | solution.py:450
  27.7 0.0 collective-permute-done.4.from_1
  27.7 2.8 %collective-permute-done.5.from_2 = bf16[144,256]{1,0:T(8,128)(2,1)S(1)} collective-permute-done((bf16[144,256]{1,0:T(8,128)(2,1)S(1)}, bf16[144,256]{1,0:T(8,128)(2,1)S(1)}, u32[]{:S(2)}, u32[]{:S(2)}) %collective-permute-start.5) | collective-permute-done | bytes 73760 | tf_op jit(solution)/shard_map/ppermute | solution.py:440
  30.5 1.8 %collective-permute-done.6.from_3 = bf16[144,256]{1,0:T(8,128)(2,1)S(1)} collective-permute-done((bf16[144,256]{1,0:T(8,128)(2,1)S(1)}, bf16[144,256]{1,0:T(8,128)(2,1)S(1)}, u32[]{:S(2)}, u32[]{:S(2)}) %collective-permute-start.6) | collective-permute-done | bytes 73760 | tf_op jit(solution)/shard_map/ppermute | solution.py:440
  32.3 0.0 copy-done.5
  32.3 1.4 %last.1 = (bf16[64,384]{1,0:T(8,128)(2,1)S(1)}, bf16[64,384]{1,0:T(8,128)(2,1)S(1)}, bf16[64,384]{1,0:T(8,128)(2,1)S(1)}, bf16[64,384]{1,0:T(8,128)(2,1)S(1)}) custom-call(bf16[144,256]{1,0:T(8,128)(2,1)S(1)} %collective-permute-done.4.from_1, bf16[144,256]{1,0:T(8,128)(2,1)S(1)} %collective-permute-done.5.from_2, ...), custom_call_target="tpu_custom_call" | custom-call | tf_op jit(solution)/shard_map/last/pallas_call | solution.py:450
  33.7 1.6 %collective-permute-start.7 = (bf16[64,384]{1,0:T(8,128)(2,1)S(1)}, bf16[64,384]{1,0:T(8,128)(2,1)S(1)}, u32[]{:S(2)}, u32[]{:S(2)}) collective-permute-start(bf16[64,384]{1,0:T(8,128)(2,1)S(1)} %get-tuple-element.58), channel_id=1, source_target_pairs={{0,1},{1,0},{2,3},{3,2},{4,5},{5,4},{6,7},{7,6},{8,9},{9,8},{10,11... | collective-permute-start | bytes 147464 | tf_op jit(solution)/shard_map/ppermute | solution.py:440
  35.2 2.7 %collective-permute-start.8 = (bf16[64,384]{1,0:T(8,128)(2,1)S(1)}, bf16[64,384]{1,0:T(8,128)(2,1)S(1)}, u32[]{:S(2)}, u32[]{:S(2)}) collective-permute-start(bf16[64,384]{1,0:T(8,128)(2,1)S(1)} %get-tuple-element.59), channel_id=1, source_target_pairs={{0,2},{1,3},{2,0},{3,1},{4,6},{5,7},{6,4},{7,5},{8,10},{9,11},{10,... | collective-permute-start | bytes 147464 | tf_op jit(solution)/shard_map/ppermute | solution.py:440
  38.0 0.5 %collective-permute-start.9 = (bf16[64,384]{1,0:T(8,128)(2,1)S(1)}, bf16[64,384]{1,0:T(8,128)(2,1)S(1)}, u32[]{:S(2)}, u32[]{:S(2)}) collective-permute-start(bf16[64,384]{1,0:T(8,128)(2,1)S(1)} %get-tuple-element.60), channel_id=1, source_target_pairs={{0,3},{1,2},{2,1},{3,0},{4,7},{5,6},{6,5},{7,4},{8,11},{9,10},{10,... | collective-permute-start | bytes 147464 | tf_op jit(solution)/shard_map/ppermute | solution.py:440
  38.5 0.0 collective-permute-done.7.from_1
  38.5 2.4 %collective-permute-done.8.from_2 = bf16[64,384]{1,0:T(8,128)(2,1)S(1)} collective-permute-done((bf16[64,384]{1,0:T(8,128)(2,1)S(1)}, bf16[64,384]{1,0:T(8,128)(2,1)S(1)}, u32[]{:S(2)}, u32[]{:S(2)}) %collective-permute-start.8) | collective-permute-done | bytes 49184 | tf_op jit(solution)/shard_map/ppermute | solution.py:440
  40.8 2.4 %collective-permute-done.9.from_3 = bf16[64,384]{1,0:T(8,128)(2,1)S(1)} collective-permute-done((bf16[64,384]{1,0:T(8,128)(2,1)S(1)}, bf16[64,384]{1,0:T(8,128)(2,1)S(1)}, u32[]{:S(2)}, u32[]{:S(2)}) %collective-permute-start.9) | collective-permute-done | bytes 49184 | tf_op jit(solution)/shard_map/ppermute | solution.py:440
  43.3 0.0 copy-done
  43.3 0.0 copy-done.1
  43.3 1.9 %project.1 = bf16[64,2048]{1,0:T(8,128)(2,1)} custom-call(bf16[64,384]{1,0:T(8,128)(2,1)S(1)} %get-tuple-element.57.own, bf16[64,384]{1,0:T(8,128)(2,1)S(1)} %collective-permute-done.7.from_1, bf16[64,384]{1,0:T(8,128)(2,1)S(1)} %collective-permute-done.8.from_2, bf16[64,384]{1,0:T(8,128)(2,1)S(1)} %collective-permute-done.9.from_3, ...), custom_call_target="tpu_custom_call" | custom-call | tf_op jit(solution)/shard_map/project/pallas_call | solution.py:450
Async XLA Ops:
  0.0 15.3 %copy-start.2 = (f32[31,128]{1,0:T(8,128)S(1)}, f32[31,128]{1,0:T(8,128)}, u32[]{:S(2)}) copy-start(f32[31,128]{1,0:T(8,128)} %taps.3) | copy-start | bytes 47620
  0.0 15.3 %copy-start.3 = (f32[128]{0:T(128)S(1)}, f32[128]{0:T(128)}, u32[]{:S(2)}) copy-start(f32[128]{0:T(128)} %param.25) | copy-start | bytes 1540
  0.0 15.3 %copy-start.4 = (f32[128]{0:T(128)S(1)}, f32[128]{0:T(128)}, u32[]{:S(2)}) copy-start(f32[128]{0:T(128)} %param.26) | copy-start | bytes 1540
  0.0 32.3 %copy-start.5 = (f32[256]{0:T(256)S(1)}, f32[256]{0:T(256)}, u32[]{:S(2)}) copy-start(f32[256]{0:T(256)} %param.37) | copy-start | bytes 3076
  8.4 34.9 %copy-start = (bf16[1024,2048]{1,0:T(8,128)(2,1)S(1)}, bf16[1024,2048]{1,0:T(8,128)(2,1)}, u32[]{:S(2)}) copy-start(bf16[1024,2048]{1,0:T(8,128)(2,1)} %mix_w.1) | copy-start | bytes 12582916
  8.4 34.9 %copy-start.1 = (bf16[512,2048]{1,0:T(8,128)(2,1)S(1)}, bf16[512,2048]{1,0:T(8,128)(2,1)}, u32[]{:S(2)}) copy-start(bf16[512,2048]{1,0:T(8,128)(2,1)} %conv_w.1) | copy-start | bytes 6291460
  8.4 1.5 %collective-permute-start = (f32[144,256]{1,0:T(8,128)S(1)}, f32[144,256]{1,0:T(8,128)S(1)}, u32[]{:S(2)}, u32[]{:S(2)}) collective-permute-start(f32[144,256]{1,0:T(8,128)S(1)} %get-tuple-element.33.mine), channel_id=1, source_target_pairs={{0,4},{4,0},{1,5},{5,1},{2,6},{6,2},{3,7},{7,3},{8,12},{12,8},{9,1... | collective-permute-start | bytes 442376 | tf_op jit(solution)/shard_map/ppermute | solution.py:440
  10.2 5.8 %collective-permute-start.1 = (bf16[144,256]{1,0:T(8,128)(2,1)S(1)}, bf16[144,256]{1,0:T(8,128)(2,1)S(1)}, u32[]{:S(2)}, u32[]{:S(2)}) collective-permute-start(bf16[144,256]{1,0:T(8,128)(2,1)S(1)} %get-tuple-element.34.own), channel_id=1, source_target_pairs={{0,12},{4,8},{8,4},{12,0},{16,28},{20,24},{24,20},{28,16},{1,13},{... | collective-permute-start | bytes 221192 | tf_op jit(solution)/shard_map/ppermute | solution.py:440
  11.7 6.9 %collective-permute-start.2 = (bf16[144,256]{1,0:T(8,128)(2,1)S(1)}, bf16[144,256]{1,0:T(8,128)(2,1)S(1)}, u32[]{:S(2)}, u32[]{:S(2)}) collective-permute-start(bf16[144,256]{1,0:T(8,128)(2,1)S(1)} %get-tuple-element.34.own), channel_id=1, source_target_pairs={{0,20},{4,16},{8,28},{12,24},{16,4},{20,0},{24,12},{28,8},{1,21},{... | collective-permute-start | bytes 221192 | tf_op jit(solution)/shard_map/ppermute | solution.py:440
  14.5 5.9 %collective-permute-start.3 = (bf16[144,256]{1,0:T(8,128)(2,1)S(1)}, bf16[144,256]{1,0:T(8,128)(2,1)S(1)}, u32[]{:S(2)}, u32[]{:S(2)}) collective-permute-start(bf16[144,256]{1,0:T(8,128)(2,1)S(1)} %get-tuple-element.34.own), channel_id=1, source_target_pairs={{0,28},{4,24},{8,20},{12,16},{16,12},{20,8},{24,4},{28,0},{1,29},{... | collective-permute-start | bytes 221192 | tf_op jit(solution)/shard_map/ppermute | solution.py:440
  21.1 6.6 %collective-permute-start.4 = (bf16[144,256]{1,0:T(8,128)(2,1)S(1)}, bf16[144,256]{1,0:T(8,128)(2,1)S(1)}, u32[]{:S(2)}, u32[]{:S(2)}) collective-permute-start(bf16[144,256]{1,0:T(8,128)(2,1)S(1)} %get-tuple-element.43), channel_id=1, source_target_pairs={{0,36},{4,32},{32,4},{36,0},{64,100},{68,96},{96,68},{100,64},{1,3... | collective-permute-start | bytes 221192 | tf_op jit(solution)/shard_map/ppermute | solution.py:440
  22.8 7.7 %collective-permute-start.5 = (bf16[144,256]{1,0:T(8,128)(2,1)S(1)}, bf16[144,256]{1,0:T(8,128)(2,1)S(1)}, u32[]{:S(2)}, u32[]{:S(2)}) collective-permute-start(bf16[144,256]{1,0:T(8,128)(2,1)S(1)} %get-tuple-element.43), channel_id=1, source_target_pairs={{0,68},{4,64},{32,100},{36,96},{64,4},{68,0},{96,36},{100,32},{1,6... | collective-permute-start | bytes 221192 | tf_op jit(solution)/shard_map/ppermute | solution.py:440
  26.4 5.9 %collective-permute-start.6 = (bf16[144,256]{1,0:T(8,128)(2,1)S(1)}, bf16[144,256]{1,0:T(8,128)(2,1)S(1)}, u32[]{:S(2)}, u32[]{:S(2)}) collective-permute-start(bf16[144,256]{1,0:T(8,128)(2,1)S(1)} %get-tuple-element.43), channel_id=1, source_target_pairs={{0,100},{4,96},{32,68},{36,64},{64,36},{68,32},{96,4},{100,0},{1,1... | collective-permute-start | bytes 221192 | tf_op jit(solution)/shard_map/ppermute | solution.py:440
  33.7 4.8 %collective-permute-start.7 = (bf16[64,384]{1,0:T(8,128)(2,1)S(1)}, bf16[64,384]{1,0:T(8,128)(2,1)S(1)}, u32[]{:S(2)}, u32[]{:S(2)}) collective-permute-start(bf16[64,384]{1,0:T(8,128)(2,1)S(1)} %get-tuple-element.58), channel_id=1, source_target_pairs={{0,1},{1,0},{2,3},{3,2},{4,5},{5,4},{6,7},{7,6},{8,9},{9,8},{10,11... | collective-permute-start | bytes 147464 | tf_op jit(solution)/shard_map/ppermute | solution.py:440
  35.2 5.6 %collective-permute-start.8 = (bf16[64,384]{1,0:T(8,128)(2,1)S(1)}, bf16[64,384]{1,0:T(8,128)(2,1)S(1)}, u32[]{:S(2)}, u32[]{:S(2)}) collective-permute-start(bf16[64,384]{1,0:T(8,128)(2,1)S(1)} %get-tuple-element.59), channel_id=1, source_target_pairs={{0,2},{1,3},{2,0},{3,1},{4,6},{5,7},{6,4},{7,5},{8,10},{9,11},{10,... | collective-permute-start | bytes 147464 | tf_op jit(solution)/shard_map/ppermute | solution.py:440
  38.0 5.3 %collective-permute-start.9 = (bf16[64,384]{1,0:T(8,128)(2,1)S(1)}, bf16[64,384]{1,0:T(8,128)(2,1)S(1)}, u32[]{:S(2)}, u32[]{:S(2)}) collective-permute-start(bf16[64,384]{1,0:T(8,128)(2,1)S(1)} %get-tuple-element.60), channel_id=1, source_target_pairs={{0,3},{1,2},{2,1},{3,0},{4,7},{5,6},{6,5},{7,4},{8,11},{9,10},{10,... | collective-permute-start | bytes 147464 | tf_op jit(solution)/shard_map/ppermute | solution.py:440

commit v6 on v5

--- a/solution.py
+++ b/solution.py
@@ -128,15 +128,30 @@
         pltpu.make_async_copy(source, target, sems.at[n])
         for n, (source, target) in enumerate(zip(sources, targets))
     ]
-    for n in (0, 1, 6, 2, 7, 8, 3, 4, 5, 9, 10, 11, 12, 13):
-        copies[n].start()
-    copies[0].wait()
+    blocks = (0, 14, 15, 16)
+    parts = [slice(SPAN * n, SPAN * n + SPAN) for n in range(CHUNKS)]
+    copies[0] = pltpu.make_async_copy(sources[0].at[parts[0]], tokens.at[parts[0]], sems.at[0])
+    for n in range(1, CHUNKS):
+        copies.append(
+            pltpu.make_async_copy(sources[0].at[parts[n]], tokens.at[parts[n]], sems.at[13 + n])
+        )
+
+    def start(*which):
+        for n in which:
+            copies[n].start()
+
+    start(*blocks, 1, 6, 2, 7)
     copies[1].wait()
-    for n in range(ROWS // 16):
-        here = slice(16 * n, 16 * n + 16)
-        rows = tokens[here].astype(F32)
-        scale = lax.rsqrt(jnp.mean(rows * rows, axis=-1, keepdims=True) + NORM_EPS)
-        normed[here] = (rows * scale * gain[...]).astype(BF16)
+    for n in range(CHUNKS):
+        copies[blocks[n]].wait()
+        if n == 0:
+            start(8)
+        for m in range(SPAN // 16):
+            here = slice(SPAN * n + 16 * m, SPAN * n + 16 * m + 16)
+            rows = tokens[here].astype(F32)
+            scale = lax.rsqrt(jnp.mean(rows * rows, axis=-1, keepdims=True) + NORM_EPS)
+            normed[here] = (rows * scale * gain[...]).astype(BF16)
+    start(3, 4, 5, 9)
 
     def project(n):
         copies[n].wait()
@@ -151,7 +166,9 @@
     key_scaled = key * key_gain[...]
     unit = key_scaled * lax.rsqrt(group_sum(key_scaled * key_scaled, ones) + KEY_EPS)
     erase = unit * jax.nn.sigmoid(project(7))
+    start(10, 11)
     decay = project(8)
+    start(12, 13)
     for n in (3, 4, 5):
         copies[n].wait()
     logits = decay + bias[...] + shift[...]
@@ -187,19 +204,8 @@
     erase_b = erase_s.astype(BF16)
     key_b = key_s.astype(BF16)
     unit_b = unit_s.astype(BF16)
-    value_b = project(9).astype(BF16)
     erase_out[...] = erase_b
     key_out[...] = key_b
-    value_out[...] = value_b
-
-    copies[10].wait()
-    copies[11].wait()
-    both = rounded_product(normed[...], conv_weights[...])
-    conv_input = rounded(both[:, :CONV] * jax.nn.sigmoid(both[:, CONV:]))
-    conv_out[...] = conv_input
-    pack_out[2 * HEAD :, :128] = conv_input[ROWS - 32 : ROWS - 16]
-    pack_out[2 * HEAD :, 128:] = conv_input[ROWS - 16 :]
-
     flat = (SPAN, LANES)
     row_in, lane_in = iota(flat, 0), iota(flat, 1) % HEAD
     strict = lane_in < row_in
@@ -222,7 +228,6 @@
     d1 = [jnp.where(near, a, 0.0) for a in erase_mix]
     n1 = [jnp.where(far, a, 0.0) for a in erase_mix]
     d2 = times(d1, d1)
-    key_value = times(key_mix, [value_b[at] for at in chunks])
     stacked = times([jnp.concatenate([p, q], axis=0) for p, q in zip(d1, d2)], d2)
     d4 = [m[SPAN:] for m in stacked]
     g = [q - p - m[:SPAN] for p, q, m in zip(d1, d2, stacked)]
@@ -233,11 +238,22 @@
     p4 = times(p2, p2)
     m2 = add(m1, p2, times(p2, m1))
     m3 = add(m2, p4, times(p4, m2))
+    value_b = project(9).astype(BF16)
+    value_out[...] = value_b
+    key_value = times(key_mix, [value_b[at] for at in chunks])
     start_unit = [unit_q[at] for at in chunks]
     weave = [-x for x in add(start_unit, times(m3, start_unit))]
     removed = [-x for x in add(key_value, times(m3, key_value))]
     weave = [x.astype(BF16) for x in weave]
     removed = [x.astype(BF16) for x in removed]
+
+    copies[10].wait()
+    copies[11].wait()
+    both = rounded_product(normed[...], conv_weights[...])
+    conv_input = rounded(both[:, :CONV] * jax.nn.sigmoid(both[:, CONV:]))
+    conv_out[...] = conv_input
+    pack_out[2 * HEAD :, :128] = conv_input[ROWS - 32 : ROWS - 16]
+    pack_out[2 * HEAD :, 128:] = conv_input[ROWS - 16 :]
 
     same_head = row_at // HEAD == lane_at // HEAD
     eye = row_at == lane_at
@@ -348,31 +364,57 @@
     prefix_out[2 * HEAD :] = jnp.where(first, 0.0, early[2 * HEAD :])
 
 
-def row_kernel(own, total, from_1, from_2, from_3, prefix, *refs):
-    pack_out, prefix_out, slots = refs[-3:]
-    me, core = lax.axis_index("y"), lax.axis_index("c")
+def in_order(own, total, pieces, slots):
+    me = lax.axis_index("y")
     slots[0, : 2 * HEAD] = total[...]
     slots[0, 2 * HEAD :] = own[2 * HEAD :].astype(F32)
-    for n, ref in enumerate((from_1, from_2, from_3)):
+    for n, ref in enumerate(pieces):
         slots[n + 1] = ref[...].astype(F32)
-    state = slots[me ^ 0][: 2 * HEAD]
-    before = unit_state()
-    for n in range(1, 4):
-        before = jnp.where(me == n, state, before)
-        piece = slots[me ^ n]
-        state = follow(state, piece[:HEAD], piece[HEAD : 2 * HEAD])
+    return me
+
+
+def row_kernel(own, total, from_3, from_2, from_1, _, unread, pack_out, total_out, slots):
+    me = in_order(own, total, (from_1, from_2, from_3), slots)
+    low = joined(slots[me], slots[me ^ 1])
+    high = joined(slots[me ^ 2], slots[me ^ 3])
+    state = joined(low, high)
+    total_out[...] = state
     pack_out[: 2 * HEAD] = state.astype(BF16)
     pack_out[2 * HEAD :] = slots[me ^ 3, 2 * HEAD :].astype(BF16)
-    prefix_out[: 2 * HEAD] = follow(before, prefix[:HEAD], prefix[HEAD : 2 * HEAD])
+
+
+def prefix_kernel(own, total, from_3, from_2, from_1, prefix, prefix_out, slots):
+    me = in_order(own, total, (from_1, from_2, from_3), slots)
+    first = slots[me][: 2 * HEAD]
+    two = joined(first, slots[me ^ 1])
+    three = joined(two, slots[me ^ 2])
+    before = jnp.where(me == 1, first, unit_state())
+    before = jnp.where(me == 2, two, before)
+    before = jnp.where(me == 3, three, before)
+    prefix_out[: 2 * HEAD] = joined(before, prefix[...])
     behind = slots[me ^ jnp.maximum(me - 1, 0), 2 * HEAD :]
-    takes = (me > 0) & (core == 0)
+    takes = (me > 0) & (lax.axis_index("c") == 0)
     prefix_out[2 * HEAD :] = jnp.where(takes, behind, prefix[2 * HEAD :])
 
 
+def plane_kernel(mine, total, other, prefix, pack_out, prefix_out):
+    at = lax.axis_index("z")
+    upper = lax.rem(at, 2) == 1
+    got = other[...].astype(F32)
+    states = got[: 2 * HEAD]
+    early = jnp.where(upper, states, total[...])
+    late = jnp.where(upper, total[...], states)
+    base = mm3(early[HEAD:], expand(late[:HEAD])) + late[HEAD:]
+    pack_out[:HEAD] = base.astype(BF16)
+    pack_out[HEAD:] = jnp.where(upper, mine[2 * HEAD :].astype(F32), got[2 * HEAD :]).astype(BF16)
+    behind = joined(states, prefix[...])
+    prefix_out[: 2 * HEAD] = jnp.where(upper, behind, prefix[: 2 * HEAD])
+    takes = upper & (lax.axis_index("c") == 0) & (lax.axis_index("y") == 0)
+    prefix_out[2 * HEAD :] = jnp.where(takes, got[2 * HEAD :], prefix[2 * HEAD :])
+
+
 def last_kernel(
-    from_1,
-    from_2,
-    from_3,
+    other,
     prefix,
     local,
     query,
@@ -387,20 +429,13 @@
     out_1,
     out_2,
     out_3,
-    slots,
     ready,
     padded,
 ):
     z, y, c, x = (lax.axis_index(name) for name in SP_TP)
-    for n, ref in enumerate((from_1, from_2, from_3)):
-        slots[n + 1] = ref[...].astype(F32)
-    slots[0] = slots[1]
-    state = jnp.where(z > 0, slots[z ^ 0, HEAD : 2 * HEAD], 0.0)
-    for n in range(1, 3):
-        piece = slots[z ^ n]
-        moved = mm3(state, expand(piece[:HEAD])) + piece[HEAD : 2 * HEAD]
-        state = jnp.where(n < z, moved, state)
-    state = mm3(state, expand(prefix[:HEAD])) + prefix[HEAD : 2 * HEAD]
+    got = other[...].astype(F32)
+    entering = jnp.where(z >= 2, got[:HEAD], 0.0)
+    state = mm3(entering, expand(prefix[:HEAD])) + prefix[HEAD : 2 * HEAD]
     readout = local[...] + mm(query[...], expand(state), NT)
     ones = block_ones(LANES)
     centred = readout - group_sum(readout, ones) * (1.0 / HEAD)
@@ -409,9 +444,8 @@
     ready[:, CONV:] = mixed.astype(BF16)
     ready[:, :CONV] = conv_done[...]
 
-    behind = slots[z ^ jnp.maximum(z - 1, 0), 2 * HEAD :]
-    takes = (z > 0) & (y == 0) & (c == 0)
-    side = jnp.where(takes, behind, prefix[2 * HEAD :])
+    takes = (z >= 2) & (y == 0) & (c == 0) & (lax.rem(z, 2) == 0)
+    side = jnp.where(takes, got[HEAD:], prefix[2 * HEAD :])
     padded[:16] = side[:, :128]
     padded[16:32] = side[:, 128:]
     padded[32:] = jnp.zeros((HALO, CONV), F32)
@@ -424,15 +458,24 @@
         out[...] = ready[pl.ds(pl.multiple_of(to * SPAN, SPAN), SPAN)]
 
 
-def project_kernel(own, from_1, from_2, from_3, conv_w, mix_w, out, conv_rows, mix_rows):
+def block_product(rows, of, conv_w, mix_w):
+    conv = conv_w[pl.ds(pl.multiple_of(of * CONV, CONV), CONV)]
+    mix = mix_w[pl.ds(pl.multiple_of(of * LANES, LANES), LANES)]
+    return jnp.dot(rows[:, :CONV], conv, preferred_element_type=F32) + jnp.dot(
+        rows[:, CONV:], mix, preferred_element_type=F32
+    )
+
+
+def part_kernel(partners, *refs):
+    blocks = refs[: len(partners)]
+    conv_w, mix_w, *sums, out = refs[len(partners) :]
     x = lax.axis_index("x")
-    for n, ref in enumerate((own, from_1, from_2, from_3)):
-        of = x ^ n
-        conv_rows[:, pl.ds(pl.multiple_of(of * CONV, CONV), CONV)] = ref[:, :CONV]
-        mix_rows[:, pl.ds(pl.multiple_of(of * LANES, LANES), LANES)] = ref[:, CONV:]
-    total = jnp.dot(conv_rows[...], conv_w[...], preferred_element_type=F32)
-    total = total + jnp.dot(mix_rows[...], mix_w[...], preferred_element_type=F32)
-    out[...] = total.astype(BF16)
+    total = block_product(blocks[0], x ^ partners[0], conv_w, mix_w)
+    for n, block in zip(partners[1:], blocks[1:]):
+        total = total + block_product(block, x ^ n, conv_w, mix_w)
+    for part in sums:
+        total = total + part[...]
+    out[...] = total.astype(out.dtype)
 
 
 def swapped(value, axes, bits):
@@ -539,7 +582,7 @@
         scratch=[pltpu.VMEM((ROWS, 2048), BF16), pltpu.VMEM((1, 2048), F32), row, row]
         + [pltpu.VMEM((ROWS, LANES), F32)] * 2
         + [wide] * 5
-        + [pltpu.SemaphoreType.DMA((14,))],
+        + [pltpu.SemaphoreType.DMA((17,))],
     )
     other = swapped(pack, "c", 1)
     pack, prefix, total = call(core_kernel, "core", [packed_b, packed, state], (pack, other))
@@ -562,22 +605,32 @@
         (conv_input, depthwise_taps_weight, conv_gain, conv_shift),
         scratch=[pltpu.VMEM((HALO + ROWS, CONV), F32)],
     )
-    planes = [swapped(pack, ("y", "c"), 2 * n + 1) for n in (1, 2, 3)]
-    pack, prefix = call(
+    planes = [swapped(pack, ("y", "c"), 2 * n + 1) for n in (3, 2, 1)]
+    slots = pltpu.VMEM((4, PACK, LANES), F32)
+    around = (pack, total, *planes)
+    pack, total = call(
         row_kernel,
         "row",
-        [packed_b, packed],
-        (pack, total, *planes, prefix, conv_done, gate),
-        specs=[VMEM] * 6 + [ANY] * 2,
-        scratch=[pltpu.VMEM((4, PACK, LANES), F32)],
-    )
-    planes = [swapped(pack, ("z", "c"), 2 * n + 1) for n in (1, 2, 3)]
+        [packed_b, state],
+        (*around, conv_done, gate),
+        specs=[VMEM] * 5 + [ANY] * 2,
+        scratch=[slots],
+    )
+    other = swapped(pack, ("z", "c"), 3)
+    (prefix,) = call(prefix_kernel, "prefix", [packed], (*around, prefix), scratch=[slots])
+    pack, prefix = call(
+        plane_kernel,
+        "plane",
+        [((HEAD + HALO // 2, LANES), BF16), packed],
+        (pack, total, other, prefix),
+    )
+    other = swapped(pack, ("z", "c"), 7)
     sends = call(
         last_kernel,
         "last",
         [((SPAN, CONV + LANES), BF16)] * 4,
         (
-            *planes,
+            other,
             prefix,
             local_read,
             query,
@@ -590,18 +643,27 @@
             conv_shift,
         ),
         scratch=[
-            pltpu.VMEM((4, PACK, LANES), F32),
             pltpu.VMEM((ROWS, CONV + LANES), BF16),
             pltpu.VMEM((2 * HALO, CONV), F32),
         ],
     )
-    arrived = [swapped(sends[n], "x", n) for n in (1, 2, 3)]
+    from_3, from_2, from_1 = [swapped(sends[n], "x", n) for n in (3, 2, 1)]
+    weights = (convolution_output_weight, attention_output_weight)
+    wide_sum = ((SPAN, 2048), F32)
+    (own_sum,) = call(
+        functools.partial(part_kernel, (0,)), "part_own", [wide_sum], (sends[0], *weights)
+    )
+    (near_sum,) = call(
+        functools.partial(part_kernel, (3, 1)),
+        "part_near",
+        [wide_sum],
+        (from_3, from_1, *weights, own_sum),
+    )
     (mixed,) = call(
-        project_kernel,
-        "project",
+        functools.partial(part_kernel, (2,)),
+        "part_far",
         [((SPAN, 2048), BF16)],
-        (sends[0], *arrived, convolution_output_weight, attention_output_weight),
-        scratch=[pltpu.VMEM((SPAN, 512), BF16), pltpu.VMEM((SPAN, 1024), BF16)],
+        (from_2, *weights, near_sum),
     )
     return mixed
 

time: 45.3 us -> 41.2 us (0.909)
  waiting for transfers between devices: 15.2 us -> 9.85 us
  Pallas kernels: 15.3 us -> 16 us
    ppermute x10 -> x9, waiting for transfers between devices: 15.2 us -> 9.85 us  [swapped(): return lax.ppermute(value, axes, [(s, s ^ bits) for s in range(count)])]
    pallas_call x8 -> x12, Pallas kernels: 15.3 us -> 16 us  [call(): pl.pallas_call(kernel, name=name, out_shape=[jax.ShapeDtypeStruct(*o) for...]
    ppermute x10 -> x9, starting transfers between devices: 14.6 us -> 14.8 us  [swapped(): return lax.ppermute(value, axes, [(s, s ^ bits) for s in range(count)])]
  transfers between devices with their start and end apart: 10 -> 9, of which waited for: 7 -> 8; matrix products, arithmetic and copies ran while one was open for 0% -> 0% of each run, Pallas kernels for 6% -> 11%
where the time goes in v6:
time: 41.2 us; the launch traced here: 40.9 us
  Pallas kernels  16 us (39%)
  starting transfers between devices  14.8 us (36%)
  waiting for transfers between devices  9.85 us (24%)
    pallas_call x12, Pallas kernels, call(): pl.pallas_call(kernel, name=name, out_shape=[jax.ShapeDtypeStruct(*o) for...  16 us
    ppermute x9, starting transfers between devices, swapped(): return lax.ppermute(value, axes, [(s, s ^ bits) for s in range(count)])  14.8 us
    ppermute x9, waiting for transfers between devices, swapped(): return lax.ppermute(value, axes, [(s, s ^ bits) for s in range(count)])  9.85 us
  transfers between devices with their start and end apart: 9, of which 8 were waited for; matrix products, arithmetic and copies ran while one was open for 0% of the time, Pallas kernels for 11%

profile of v6, /device:TPU:0, one launch (start us, length us, event | category | flops | bytes accessed | tf_op | source)
XLA Modules:
  0.0 40.9 jit_solution(7390720428264590921)
XLA Ops:
  0.0 0.0 copy-start.2
  0.0 0.0 copy-start.3
  0.0 0.0 copy-start.4
  0.0 8.5 %local.1 = (f32[144,256]{1,0:T(8,128)S(1)}, f32[4,128,256]{2,1,0:T(8,128)S(1)}, f32[256,128]{1,0:T(8,128)S(1)}, bf16[256,2048]{1,0:T(8,128)(2,1)S(1)}, f32[256,2...) custom-call(bf16[256,2048]{1,0:T(8,128)(2,1)} %refs_0_.1, ...), custom_call_target="tpu_custom_call" | custom-call | tf_op jit(solution)/shard_map/local/pallas_call | solution.py:493
  8.5 0.0 copy-start.5
  8.5 0.0 copy-start
  8.6 0.0 copy-start.1
  8.6 0.1 collective-permute-start
  8.7 1.4 %collective-permute-done.other = f32[144,256]{1,0:T(8,128)S(1)} collective-permute-done((f32[144,256]{1,0:T(8,128)S(1)}, f32[144,256]{1,0:T(8,128)S(1)}, u32[]{:S(2)}, u32[]{:S(2)}) %collective-permute-start) | collective-permute-done | bytes 147488 | tf_op jit(solution)/shard_map/ppermute | solution.py:483
  10.0 0.2 core.1
  10.3 3.0 %collective-permute-start.1 = (bf16[144,256]{1,0:T(8,128)(2,1)S(1)}, bf16[144,256]{1,0:T(8,128)(2,1)S(1)}, u32[]{:S(2)}, u32[]{:S(2)}) collective-permute-start(bf16[144,256]{1,0:T(8,128)(2,1)S(1)} %get-tuple-element.36.own), channel_id=1, source_target_pairs={{0,28},{4,24},{8,20},{12,16},{16,12},{20,8},{24,4},{28,0},{1,29},{... | collective-permute-start | bytes 221192 | tf_op jit(solution)/shard_map/ppermute | solution.py:483
  13.2 0.6 %collective-permute-start.2 = (bf16[144,256]{1,0:T(8,128)(2,1)S(1)}, bf16[144,256]{1,0:T(8,128)(2,1)S(1)}, u32[]{:S(2)}, u32[]{:S(2)}) collective-permute-start(bf16[144,256]{1,0:T(8,128)(2,1)S(1)} %get-tuple-element.36.own), channel_id=1, source_target_pairs={{0,20},{4,16},{8,28},{12,24},{16,4},{20,0},{24,12},{28,8},{1,21},{... | collective-permute-start | bytes 221192 | tf_op jit(solution)/shard_map/ppermute | solution.py:483
  13.8 0.3 collective-permute-start.3
  14.2 0.7 %gate.1 = (f32[256,256]{1,0:T(8,128)S(1)}, f32[256,256]{1,0:T(8,128)S(1)}) custom-call(bf16[256,2048]{1,0:T(8,128)(2,1)S(1)} %get-tuple-element.40.normed, bf16[2048,256]{1,0:T(8,128)(2,1)S(1)} %get-tuple-element.41.w_receptance, bf16[2048,256]{1,0:T(8,128)(2,1)S(1)} %get-tuple-element.42.w_gate), custom_call_target="tpu_custom_call" | custom-call | tf_op jit(solution)/shard_map/gate/pallas_call | solution.py:493
  14.9 0.0 copy-done.2
  14.9 0.0 copy-done.3
  14.9 0.0 copy-done.4
  14.9 0.6 %conv.1 = (bf16[256,128]{1,0:T(8,128)(2,1)S(1)}, f32[32,128]{1,0:T(8,128)S(1)}) custom-call(f32[256,128]{1,0:T(8,128)S(1)} %get-tuple-element.38.conv_in, f32[31,128]{1,0:T(8,128)S(1)} %copy-done.2, f32[1,128]{1,0:T(1,128)S(1)} %bitcast.6, f32[1,128]{1,0:T(1,128)S(1)} %bitcast.8), custom_call_target="tpu_custom_call" | custom-call | tf_op jit(solution)/shard_map/conv/pallas_call | solution.py:493
  15.6 1.6 %collective-permute-done.1.from_3 = bf16[144,256]{1,0:T(8,128)(2,1)S(1)} collective-permute-done((bf16[144,256]{1,0:T(8,128)(2,1)S(1)}, bf16[144,256]{1,0:T(8,128)(2,1)S(1)}, u32[]{:S(2)}, u32[]{:S(2)}) %collective-permute-start.1) | collective-permute-done | bytes 73760 | tf_op jit(solution)/shard_map/ppermute | solution.py:483
  17.2 1.6 %collective-permute-done.2.from_2 = bf16[144,256]{1,0:T(8,128)(2,1)S(1)} collective-permute-done((bf16[144,256]{1,0:T(8,128)(2,1)S(1)}, bf16[144,256]{1,0:T(8,128)(2,1)S(1)}, u32[]{:S(2)}, u32[]{:S(2)}) %collective-permute-start.2) | collective-permute-done | bytes 73760 | tf_op jit(solution)/shard_map/ppermute | solution.py:483
  18.8 0.0 collective-permute-done.3.from_1
  18.8 0.6 %row.1 = (bf16[144,256]{1,0:T(8,128)(2,1)S(1)}, f32[128,256]{1,0:T(8,128)S(1)}) custom-call(bf16[144,256]{1,0:T(8,128)(2,1)S(1)} %get-tuple-element.36.own, f32[128,256]{1,0:T(8,128)S(1)} %get-tuple-element.37.total, bf16[144,256]{1,0:T(8,128)(2,1)S(1)} %collective-permute-done.1.from_3, bf16[144,256]{1,0:T(8,128)(2,1)S(1)} %collective-permute-done.2.from_2, ...), custom_call_target="tpu_custom_call" | custom-call | tf_op jit(solution)/shard_map/row/pallas_call | solution.py:493
  19.4 2.5 %collective-permute-start.4 = (bf16[144,256]{1,0:T(8,128)(2,1)S(1)}, bf16[144,256]{1,0:T(8,128)(2,1)S(1)}, u32[]{:S(2)}, u32[]{:S(2)}) collective-permute-start(bf16[144,256]{1,0:T(8,128)(2,1)S(1)} %get-tuple-element.44.mine), channel_id=1, source_target_pairs={{0,36},{4,32},{32,4},{36,0},{64,100},{68,96},{96,68},{100,64},{1,3... | collective-permute-start | bytes 221192 | tf_op jit(solution)/shard_map/ppermute | solution.py:483
  21.9 0.6 %prefix.1 = f32[144,256]{1,0:T(8,128)S(1)} custom-call(bf16[144,256]{1,0:T(8,128)(2,1)S(1)} %get-tuple-element.36.own, f32[128,256]{1,0:T(8,128)S(1)} %get-tuple-element.37.total, bf16[144,256]{1,0:T(8,128)(2,1)S(1)} %collective-permute-done.1.from_3, bf16[144,256]{1,0:T(8,128)(2,1)S(1)} %collective-permute-done.2.from_2, ...), custom_call_target="tpu_custom_call" | custom-call | tf_op jit(solution)/shard_map/prefix/pallas_call | solution.py:493
  22.5 1.8 %collective-permute-done.4.other = bf16[144,256]{1,0:T(8,128)(2,1)S(1)} collective-permute-done((bf16[144,256]{1,0:T(8,128)(2,1)S(1)}, bf16[144,256]{1,0:T(8,128)(2,1)S(1)}, u32[]{:S(2)}, u32[]{:S(2)}) %collective-permute-start.4) | collective-permute-done | bytes 73760 | tf_op jit(solution)/shard_map/ppermute | solution.py:483
  24.3 0.3 plane.1
  24.6 3.6 %collective-permute-start.5 = (bf16[80,256]{1,0:T(8,128)(2,1)S(1)}, bf16[80,256]{1,0:T(8,128)(2,1)S(1)}, u32[]{:S(2)}, u32[]{:S(2)}) collective-permute-start(bf16[80,256]{1,0:T(8,128)(2,1)S(1)} %get-tuple-element.47), channel_id=1, source_target_pairs={{0,100},{4,96},{32,68},{36,64},{64,36},{68,32},{96,4},{100,0},{1,1... | collective-permute-start | bytes 122888 | tf_op jit(solution)/shard_map/ppermute | solution.py:483
  28.2 1.3 %read.1 = (f32[256,256]{1,0:T(8,128)S(1)}, bf16[256,256]{1,0:T(8,128)(2,1)S(1)}) custom-call(f32[256,256]{1,0:T(8,128)S(1)} %get-tuple-element.49.receptance, f32[256,256]{1,0:T(8,128)S(1)} %get-tuple-element.50.fall, f32[8,256]{1,0:T(8,128)S(1)} %get-tuple-element.51.start, bf16[256,256]{1,0:T(8,128)(2,1)S(1)} %get-tuple-element.52.erase, ...), custom_call_target="tpu_custom_call" | custom-call | tf_op jit(solution)/shard_map/read/pallas_call | solution.py:493
  29.5 0.7 %collective-permute-done.5.other = bf16[80,256]{1,0:T(8,128)(2,1)S(1)} collective-permute-done((bf16[80,256]{1,0:T(8,128)(2,1)S(1)}, bf16[80,256]{1,0:T(8,128)(2,1)S(1)}, u32[]{:S(2)}, u32[]{:S(2)}) %collective-permute-start.5) | collective-permute-done | bytes 40992 | tf_op jit(solution)/shard_map/ppermute | solution.py:483
  30.2 0.0 copy-done.5
  30.2 0.9 %last.1 = (bf16[64,384]{1,0:T(8,128)(2,1)S(1)}, bf16[64,384]{1,0:T(8,128)(2,1)S(1)}, bf16[64,384]{1,0:T(8,128)(2,1)S(1)}, bf16[64,384]{1,0:T(8,128)(2,1)S(1)}) custom-call(bf16[80,256]{1,0:T(8,128)(2,1)S(1)} %collective-permute-done.5.other, f32[144,256]{1,0:T(8,128)S(1)} %get-tuple-element.48.prefix, f32[256,256]{1,0:T(8,128)S(1)} %get-tuple-element.58.local, ...), custom_call_target="tpu_custom_call" | custom-call | tf_op jit(solution)/shard_map/last/pallas_call | solution.py:493
  31.1 2.8 %collective-permute-start.7 = (bf16[64,384]{1,0:T(8,128)(2,1)S(1)}, bf16[64,384]{1,0:T(8,128)(2,1)S(1)}, u32[]{:S(2)}, u32[]{:S(2)}) collective-permute-start(bf16[64,384]{1,0:T(8,128)(2,1)S(1)} %get-tuple-element.62), channel_id=1, source_target_pairs={{0,3},{1,2},{2,1},{3,0},{4,7},{5,6},{6,5},{7,4},{8,11},{9,10},{10,... | collective-permute-start | bytes 147464 | tf_op jit(solution)/shard_map/ppermute | solution.py:483
  33.9 0.2 collective-permute-start.8
  34.2 1.7 %collective-permute-start.6 = (bf16[64,384]{1,0:T(8,128)(2,1)S(1)}, bf16[64,384]{1,0:T(8,128)(2,1)S(1)}, u32[]{:S(2)}, u32[]{:S(2)}) collective-permute-start(bf16[64,384]{1,0:T(8,128)(2,1)S(1)} %get-tuple-element.61), channel_id=1, source_target_pairs={{0,2},{1,3},{2,0},{3,1},{4,6},{5,7},{6,4},{7,5},{8,10},{9,11},{10,... | collective-permute-start | bytes 147464 | tf_op jit(solution)/shard_map/ppermute | solution.py:483
  35.9 0.0 copy-done
  35.9 0.0 copy-done.1
  35.9 0.4 part_own.1.refs_4_
  36.3 0.2 collective-permute-done.7.refs_0_
  36.5 1.5 %collective-permute-done.8.refs_1_ = bf16[64,384]{1,0:T(8,128)(2,1)S(1)} collective-permute-done((bf16[64,384]{1,0:T(8,128)(2,1)S(1)}, bf16[64,384]{1,0:T(8,128)(2,1)S(1)}, u32[]{:S(2)}, u32[]{:S(2)}) %collective-permute-start.8) | collective-permute-done | bytes 49184 | tf_op jit(solution)/shard_map/ppermute | solution.py:483
  38.0 0.7 %part_near.1.refs_3_ = f32[64,2048]{1,0:T(8,128)S(1)} custom-call(bf16[64,384]{1,0:T(8,128)(2,1)S(1)} %collective-permute-done.7.refs_0_, bf16[64,384]{1,0:T(8,128)(2,1)S(1)} %collective-permute-done.8.refs_1_, bf16[512,2048]{1,0:T(8,128)(2,1)S(1)} %copy-done.1, bf16[1024,2048]{1,0:T(8,128)(2,1)S(1)} %copy-done, f32[64,2048]{1,0:T(8,128)S(1)} %part_own.1.refs_4_), custom_call_target="tpu_custom_call" | custom-call | tf_op jit(solution)/shard_map/part_near/pallas_call | solution.py:493
  38.7 1.1 %collective-permute-done.6.refs_0_ = bf16[64,384]{1,0:T(8,128)(2,1)S(1)} collective-permute-done((bf16[64,384]{1,0:T(8,128)(2,1)S(1)}, bf16[64,384]{1,0:T(8,128)(2,1)S(1)}, u32[]{:S(2)}, u32[]{:S(2)}) %collective-permute-start.6) | collective-permute-done | bytes 49184 | tf_op jit(solution)/shard_map/ppermute | solution.py:483
  39.8 1.1 %part_far.1 = bf16[64,2048]{1,0:T(8,128)(2,1)} custom-call(bf16[64,384]{1,0:T(8,128)(2,1)S(1)} %collective-permute-done.6.refs_0_, bf16[512,2048]{1,0:T(8,128)(2,1)S(1)} %copy-done.1, bf16[1024,2048]{1,0:T(8,128)(2,1)S(1)} %copy-done, f32[64,2048]{1,0:T(8,128)S(1)} %part_near.1.refs_3_), custom_call_target="tpu_custom_call" | custom-call | tf_op jit(solution)/shard_map/part_far/pallas_call | solution.py:493
Async XLA Ops:
  0.0 14.9 %copy-start.2 = (f32[31,128]{1,0:T(8,128)S(1)}, f32[31,128]{1,0:T(8,128)}, u32[]{:S(2)}) copy-start(f32[31,128]{1,0:T(8,128)} %taps.3) | copy-start | bytes 47620
  0.0 14.9 %copy-start.3 = (f32[128]{0:T(128)S(1)}, f32[128]{0:T(128)}, u32[]{:S(2)}) copy-start(f32[128]{0:T(128)} %param.25) | copy-start | bytes 1540
  0.0 14.9 %copy-start.4 = (f32[128]{0:T(128)S(1)}, f32[128]{0:T(128)}, u32[]{:S(2)}) copy-start(f32[128]{0:T(128)} %param.26) | copy-start | bytes 1540
  8.5 21.6 %copy-start.5 = (f32[256]{0:T(256)S(1)}, f32[256]{0:T(256)}, u32[]{:S(2)}) copy-start(f32[256]{0:T(256)} %param.37) | copy-start | bytes 3076
  8.5 27.3 %copy-start = (bf16[1024,2048]{1,0:T(8,128)(2,1)S(1)}, bf16[1024,2048]{1,0:T(8,128)(2,1)}, u32[]{:S(2)}) copy-start(bf16[1024,2048]{1,0:T(8,128)(2,1)} %refs_2_.5) | copy-start | bytes 12582916
  8.6 27.3 %copy-start.1 = (bf16[512,2048]{1,0:T(8,128)(2,1)S(1)}, bf16[512,2048]{1,0:T(8,128)(2,1)}, u32[]{:S(2)}) copy-start(bf16[512,2048]{1,0:T(8,128)(2,1)} %refs_1_.3) | copy-start | bytes 6291460
  8.6 1.5 %collective-permute-start = (f32[144,256]{1,0:T(8,128)S(1)}, f32[144,256]{1,0:T(8,128)S(1)}, u32[]{:S(2)}, u32[]{:S(2)}) collective-permute-start(f32[144,256]{1,0:T(8,128)S(1)} %get-tuple-element.35.mine), channel_id=1, source_target_pairs={{0,4},{4,0},{1,5},{5,1},{2,6},{6,2},{3,7},{7,3},{8,12},{12,8},{9,1... | collective-permute-start | bytes 442376 | tf_op jit(solution)/shard_map/ppermute | solution.py:483
  10.3 6.9 %collective-permute-start.1 = (bf16[144,256]{1,0:T(8,128)(2,1)S(1)}, bf16[144,256]{1,0:T(8,128)(2,1)S(1)}, u32[]{:S(2)}, u32[]{:S(2)}) collective-permute-start(bf16[144,256]{1,0:T(8,128)(2,1)S(1)} %get-tuple-element.36.own), channel_id=1, source_target_pairs={{0,28},{4,24},{8,20},{12,16},{16,12},{20,8},{24,4},{28,0},{1,29},{... | collective-permute-start | bytes 221192 | tf_op jit(solution)/shard_map/ppermute | solution.py:483
  13.2 5.5 %collective-permute-start.2 = (bf16[144,256]{1,0:T(8,128)(2,1)S(1)}, bf16[144,256]{1,0:T(8,128)(2,1)S(1)}, u32[]{:S(2)}, u32[]{:S(2)}) collective-permute-start(bf16[144,256]{1,0:T(8,128)(2,1)S(1)} %get-tuple-element.36.own), channel_id=1, source_target_pairs={{0,20},{4,16},{8,28},{12,24},{16,4},{20,0},{24,12},{28,8},{1,21},{... | collective-permute-start | bytes 221192 | tf_op jit(solution)/shard_map/ppermute | solution.py:483
  13.8 4.9 %collective-permute-start.3 = (bf16[144,256]{1,0:T(8,128)(2,1)S(1)}, bf16[144,256]{1,0:T(8,128)(2,1)S(1)}, u32[]{:S(2)}, u32[]{:S(2)}) collective-permute-start(bf16[144,256]{1,0:T(8,128)(2,1)S(1)} %get-tuple-element.36.own), channel_id=1, source_target_pairs={{0,12},{4,8},{8,4},{12,0},{16,28},{20,24},{24,20},{28,16},{1,13},{... | collective-permute-start | bytes 221192 | tf_op jit(solution)/shard_map/ppermute | solution.py:483
  19.4 4.9 %collective-permute-start.4 = (bf16[144,256]{1,0:T(8,128)(2,1)S(1)}, bf16[144,256]{1,0:T(8,128)(2,1)S(1)}, u32[]{:S(2)}, u32[]{:S(2)}) collective-permute-start(bf16[144,256]{1,0:T(8,128)(2,1)S(1)} %get-tuple-element.44.mine), channel_id=1, source_target_pairs={{0,36},{4,32},{32,4},{36,0},{64,100},{68,96},{96,68},{100,64},{1,3... | collective-permute-start | bytes 221192 | tf_op jit(solution)/shard_map/ppermute | solution.py:483
  24.6 5.6 %collective-permute-start.5 = (bf16[80,256]{1,0:T(8,128)(2,1)S(1)}, bf16[80,256]{1,0:T(8,128)(2,1)S(1)}, u32[]{:S(2)}, u32[]{:S(2)}) collective-permute-start(bf16[80,256]{1,0:T(8,128)(2,1)S(1)} %get-tuple-element.47), channel_id=1, source_target_pairs={{0,100},{4,96},{32,68},{36,64},{64,36},{68,32},{96,4},{100,0},{1,1... | collective-permute-start | bytes 122888 | tf_op jit(solution)/shard_map/ppermute | solution.py:483
  31.1 5.4 %collective-permute-start.7 = (bf16[64,384]{1,0:T(8,128)(2,1)S(1)}, bf16[64,384]{1,0:T(8,128)(2,1)S(1)}, u32[]{:S(2)}, u32[]{:S(2)}) collective-permute-start(bf16[64,384]{1,0:T(8,128)(2,1)S(1)} %get-tuple-element.62), channel_id=1, source_target_pairs={{0,3},{1,2},{2,1},{3,0},{4,7},{5,6},{6,5},{7,4},{8,11},{9,10},{10,... | collective-permute-start | bytes 147464 | tf_op jit(solution)/shard_map/ppermute | solution.py:483
  33.9 4.1 %collective-permute-start.8 = (bf16[64,384]{1,0:T(8,128)(2,1)S(1)}, bf16[64,384]{1,0:T(8,128)(2,1)S(1)}, u32[]{:S(2)}, u32[]{:S(2)}) collective-permute-start(bf16[64,384]{1,0:T(8,128)(2,1)S(1)} %get-tuple-element.63), channel_id=1, source_target_pairs={{0,1},{1,0},{2,3},{3,2},{4,5},{5,4},{6,7},{7,6},{8,9},{9,8},{10,11... | collective-permute-start | bytes 147464 | tf_op jit(solution)/shard_map/ppermute | solution.py:483
  34.2 5.6 %collective-permute-start.6 = (bf16[64,384]{1,0:T(8,128)(2,1)S(1)}, bf16[64,384]{1,0:T(8,128)(2,1)S(1)}, u32[]{:S(2)}, u32[]{:S(2)}) collective-permute-start(bf16[64,384]{1,0:T(8,128)(2,1)S(1)} %get-tuple-element.61), channel_id=1, source_target_pairs={{0,2},{1,3},{2,0},{3,1},{4,6},{5,7},{6,4},{7,5},{8,10},{9,11},{10,... | collective-permute-start | bytes 147464 | tf_op jit(solution)/shard_map/ppermute | solution.py:483
